TPU v7x, 512 devices: a whole 4x4x16 slice. The times are simulated.
512 devices in a mesh: kv: 64 (over z, y), tp: 8 (over x, core).
Axes of the slice: x: 4, y: 4, z: 16, core: 2. Of those that a mesh axis runs over, the one named last changes fastest.
Arguments:
- tokens: bfloat16 [16384, 2048], P('kv'), may hold values from -72 to 72
- w_query: bfloat16 [2048, 1024], P(None, 'tp'), may hold values from -0.125 to 0.125
- w_key: bfloat16 [2048, 1024], P(None, 'tp'), may hold values from -0.125 to 0.125
- w_value: bfloat16 [2048, 1024], P(None, 'tp'), may hold values from -0.125 to 0.125
- w_out: bfloat16 [1024, 2048], P('tp'), may hold values from -0.1875 to 0.1875
- chosen: int32 [256, 16], replicated, may hold values from -1 to 255, as said below
Outputs:
- mixed: bfloat16 [16384, 2048], P(('kv', 'tp'))
- log_sums: float32 [16, 16384], P('tp', 'kv')
Inputs may be any that keep to these rules, and one draw needn't show every extreme that they name: `chosen`: row b begins with b itself, then lists distinct key blocks at most b, then holds -1 in its remaining entries. Taken together, the rows of the query blocks of one index of kv list at most 2 distinct blocks of the positions of any other index of kv, and exactly 2 for some pairs of indices in every draw.
All inputs are finite; a program needn't handle non-finite values.
Results may differ from a plain program's by a relative error of at most 0.03.
Values may be sent and summed in bfloat16 or wider, within the bound.
No kernel may reach another device: no remote copies, remote signals or barrier semaphores. Data moves between devices by JAX's collectives and lax.ppermute only.
A program may use at most 64 MiB of HBM per device.

v0:
```python
import jax
import jax.numpy as jnp
from jax import lax
from jax.sharding import PartitionSpec as P

HEAD_DIM = 64
BLK = 64
SEL = 16
CAP = 2


rotary_base = 500000.0
masked_score = -1e30


def in_blocks(value, dim, size):
    before, after = (value.shape[:dim], value.shape[dim + 1 :])
    return jnp.moveaxis(value.reshape(*before, size, -1, *after), dim, 0)


def summed_on_arrival(value, axis, dim):
    size = lax.axis_size(axis)
    tiles = lax.all_to_all(in_blocks(value, dim, size), axis, 0, 0, tiled=True)
    return jnp.sum(tiles.astype(jnp.float32), axis=0)


def rotate(values, positions, head_count, head_size):
    half_size = head_size // 2
    inverse = rotary_base ** (-jnp.arange(half_size, dtype=jnp.float32) / half_size)
    angles = positions.astype(jnp.float32)[:, None, None] * inverse[None, None, :]
    cos_part = jnp.cos(angles)
    sin_part = jnp.sin(angles)
    grouped = values.reshape(values.shape[0], head_count, head_size)
    first_half = grouped[..., :half_size]
    second_half = grouped[..., half_size:]
    turned = jnp.concatenate(
        [
            first_half * cos_part - second_half * sin_part,
            second_half * cos_part + first_half * sin_part,
        ],
        axis=-1,
    )
    return turned.reshape(values.shape)


def local(tokens, w_query, w_key, w_value, w_out, chosen):
    local_rows = tokens.shape[0]
    local_width = w_query.shape[1]
    head_count = local_width // HEAD_DIM
    scaling = HEAD_DIM ** (-0.5)
    device = lax.axis_index("kv")
    positions = device * local_rows + jnp.arange(local_rows)
    query = rotate(
        jnp.dot(tokens, w_query, preferred_element_type=jnp.float32),
        positions,
        head_count,
        HEAD_DIM,
    ).astype(jnp.bfloat16)
    keys_here = rotate(
        jnp.dot(tokens, w_key, preferred_element_type=jnp.float32), positions, head_count, HEAD_DIM
    ).astype(jnp.bfloat16)
    values_here = jnp.dot(tokens, w_value, preferred_element_type=jnp.float32).astype(jnp.bfloat16)
    blocks_here = local_rows // BLK
    own_lists = lax.dynamic_slice_in_dim(chosen, device * blocks_here, blocks_here, 0)
    query_heads = query.reshape(local_rows, head_count, HEAD_DIM)
    devices = lax.axis_size("kv")
    mine_blocks = device * blocks_here + jnp.arange(blocks_here)
    listed_hits = jnp.any(chosen[:, :, None] == mine_blocks[None, None, :], axis=1)
    wanted = jnp.any(listed_hits.reshape(devices, blocks_here, blocks_here), axis=1)
    wanted = wanted & (jnp.arange(devices) != device)[:, None]
    send_slots = jnp.cumsum(wanted.astype(jnp.int32), axis=1) - 1
    placing = (wanted[:, None, :] & (send_slots[:, None, :] == jnp.arange(CAP)[:, None])).astype(
        jnp.bfloat16
    )
    both_here = jnp.concatenate([keys_here, values_here], axis=1).reshape(
        blocks_here, BLK, 2 * local_width
    )
    outgoing = (
        jnp.einsum("dcb,bkf->dckf", placing, both_here, preferred_element_type=jnp.float32)
        .astype(jnp.bfloat16)
        .reshape(devices, CAP * BLK, 2 * local_width)
    )
    incoming = lax.all_to_all(outgoing, "kv", split_axis=0, concat_axis=0, tiled=True)
    every_block = jnp.arange(chosen.shape[0])
    needed = jnp.any(own_lists.reshape(-1)[:, None] == every_block[None, :], axis=0).reshape(
        devices, blocks_here
    )
    my_slots = (jnp.cumsum(needed.astype(jnp.int32), axis=1) - 1).reshape(-1)
    usable = own_lists >= 0
    safe_rows = jnp.maximum(own_lists, 0)
    lookup = jnp.sum(
        jnp.where(safe_rows[:, :, None] == every_block[None, None, :], my_slots[None, None, :], 0),
        axis=-1,
    )
    owner_dev = safe_rows // blocks_here
    source_row = jnp.where(
        owner_dev == device, devices * CAP + safe_rows % blocks_here, owner_dev * CAP + lookup
    )
    key_table = jnp.concatenate(
        [incoming.reshape(devices * CAP, BLK, 2 * local_width), both_here], axis=0
    )
    picked = key_table[source_row]
    picked_keys = picked[..., :local_width].reshape(blocks_here, SEL * BLK, head_count, HEAD_DIM)
    picked_values = picked[..., local_width:].reshape(blocks_here, SEL * BLK, head_count, HEAD_DIM)
    query_blocks = query_heads.reshape(blocks_here, BLK, head_count, HEAD_DIM)
    scores = (
        jnp.einsum("bqhd,bkhd->bhqk", query_blocks, picked_keys, preferred_element_type=jnp.float32)
        * scaling
    )
    key_mask = jnp.broadcast_to(usable[:, :, None], (blocks_here, SEL, BLK)).reshape(
        blocks_here, 1, 1, SEL * BLK
    )
    scores = jnp.where(key_mask, scores, masked_score)
    block_max = jnp.max(scores, axis=-1)
    weights = jnp.where(key_mask, jnp.exp(scores - block_max[..., None]), 0.0)
    block_total = jnp.sum(weights, axis=-1)
    block_sum = jnp.einsum(
        "bhqk,bkhd->bhqd",
        weights.astype(jnp.bfloat16),
        picked_values,
        preferred_element_type=jnp.float32,
    )
    row_max = jnp.transpose(block_max, (1, 0, 2)).reshape(head_count, local_rows)
    totals = jnp.transpose(block_total, (1, 0, 2)).reshape(head_count, local_rows)
    summed = jnp.transpose(block_sum, (1, 0, 2, 3)).reshape(head_count, local_rows, HEAD_DIM)
    mixed_heads = summed / totals[..., None]
    attended = (
        jnp.transpose(mixed_heads, (1, 0, 2)).reshape(local_rows, local_width).astype(jnp.bfloat16)
    )
    log_sums = row_max + jnp.log(totals)
    output = summed_on_arrival(
        jnp.dot(attended, w_out, preferred_element_type=jnp.float32).astype(jnp.bfloat16), "tp", 0
    )
    return (output.astype(jnp.bfloat16), log_sums)


def solution(mesh):
    placed = (P("kv", None), P(None, "tp"), P(None, "tp"), P(None, "tp"), P("tp", None), P())
    return jax.shard_map(
        local,
        mesh=mesh,
        in_specs=placed,
        out_specs=(P(("kv", "tp"), None), P("tp", "kv")),
        check_vma=False,
    )
```

profile of v0, /device:TPU:1, one launch (start us, length us, event | category | flops | bytes accessed | tf_op | source)
XLA Modules:
  0.0 270.5 jit_solution(12492361866420358039)
XLA Ops:
  0.7 1.2 copy-done
  1.9 1.5 fusion.33
  3.4 1.5 fusion.34
  5.0 0.5 convolution_convert_fusion.2
  5.4 0.2 multiply_cosine_fusion
  5.7 0.1 copy.77
  5.9 0.2 reshape.174
  6.1 0.1 reduce_or.28
  6.3 1.3 convolution_convert_fusion
  7.6 4.3 %copy.79 = bf16[64,128,256]{2,1,0:T(8,128)(2,1)} copy(bf16[64,128,256]{2,0,1:T(8,128)(2,1)S(1)} %bitcast.41) | data formatting | bytes 8388608 | tf_op jit(solution)/shard_map/reshape | solution.py:81
  12.0 19.7 %all-to-all-start = ((bf16[64,128,256]{2,1,0:T(8,128)(2,1)}), bf16[64,128,256]{2,1,0:T(8,128)(2,1)}, u32[]{:S(2)}, u32[]{:S(2)}) async-start(bf16[64,128,256]{2,1,0:T(8,128)(2,1)} %copy.79), calls=%async_computation | async-start | bytes 8388608 | tf_op jit(solution)/shard_map/all_to_all | solution.py:83
  32.0 0.1 fusion.19
  32.1 0.1 reshape.184
  32.4 0.1 sub.33
  32.5 0.2 select_reduce_fusion
  32.8 0.1 convert_element_type.55
  33.2 182.2 %all-to-all-done = bf16[64,128,256]{2,1,0:T(8,128)(2,1)} async-done(((bf16[64,128,256]{2,1,0:T(8,128)(2,1)}), bf16[64,128,256]{2,1,0:T(8,128)(2,1)}, u32[]{:S(2)}, u32[]{:S(2)}) %all-to-all-start) | async-done | bytes 4194336 | tf_op jit(solution)/shard_map/all_to_all | solution.py:83
  215.4 4.5 %pad_maximum_fusion = bf16[132,64,256]{2,1,0:T(8,128)(2,1)} fusion(bf16[4,64,256]{2,1,0:T(8,128)(2,1)S(1)} %bitcast.44, bf16[128,64,256]{2,1,0:T(8,128)(2,1)} %bitcast.8), kind=kLoop, calls=%fused_computation.1 | loop fusion | flops 2162688 | bytes 8650752 | tf_op jit(solution)/shard_map/concatenate | solution.py:99
  219.9 2.9 %gather_fusion = bf16[64,64,256]{2,1,0:T(8,128)(2,1)S(1)} fusion(bf16[132,64,256]{2,1,0:T(8,128)(2,1)} %pad_maximum_fusion, s32[1024]{0:T(1024)S(1)} %pad_clamp_fusion), kind=kCustom, calls=%fused_computation | custom fusion | bytes 4194560 | tf_op jit(solution)/shard_map/gather | solution.py:102
  222.8 1.9 fusion.32
  224.7 5.0 %reshape.197 = bf16[4,1024,2,64]{3,2,1,0:T(2,128)(2,1)} reshape(bf16[4,16,64,128]{3,2,1,0:T(8,128)(2,1)} %get-tuple-element.4) | data formatting | bytes 2097152 | tf_op jit(solution)/shard_map/reshape | solution.py:103
  229.8 2.6 fusion.4
  232.3 0.7 fusion.5
  233.1 5.0 %reshape.198 = bf16[4,1024,2,64]{3,2,1,0:T(2,128)(2,1)} reshape(bf16[4,16,64,128]{3,2,1,0:T(8,128)(2,1)} %get-tuple-element.5) | data formatting | bytes 2097152 | tf_op jit(solution)/shard_map/reshape | solution.py:104
  238.1 2.4 fusion.7
  240.5 0.1 copy.85
  240.6 0.2 reshape.181
  240.9 2.5 convolution_convert_fusion.1
  243.4 11.4 %all-to-all-start.1 = ((bf16[8,32,2048]{2,1,0:T(8,128)(2,1)}), bf16[8,32,2048]{2,1,0:T(8,128)(2,1)S(1)}, u32[]{:S(2)}, u32[]{:S(2)}) async-start(bf16[8,32,2048]{2,1,0:T(8,128)(2,1)} %bitcast.14), calls=%async_computation.1 | async-start | bytes 2097152 | tf_op jit(solution)/shard_map/all_to_all | solution.py:23
  254.8 0.6 log_add_fusion
  255.4 14.3 %all-to-all-done.1 = bf16[8,32,2048]{2,1,0:T(8,128)(2,1)S(1)} async-done(((bf16[8,32,2048]{2,1,0:T(8,128)(2,1)}), bf16[8,32,2048]{2,1,0:T(8,128)(2,1)S(1)}, u32[]{:S(2)}, u32[]{:S(2)}) %all-to-all-start.1) | async-done | bytes 1048608 | tf_op jit(solution)/shard_map/all_to_all | solution.py:23
  269.7 0.8 reduce_sum.32
  (36 shorter events, 1.2 us)
Async XLA Ops:
  0.6 1.2 copy-start
  0.6 4.3 %copy-start.1 = (bf16[2048,128]{1,0:T(8,128)(2,1)S(1)}, bf16[2048,128]{1,0:T(8,128)(2,1)}, u32[]{:S(2)}) copy-start(bf16[2048,128]{1,0:T(8,128)(2,1)} %param.9) | copy-start | bytes 1572868
  3.4 2.5 copy-start.2
  12.0 203.4 %all-to-all-start = ((bf16[64,128,256]{2,1,0:T(8,128)(2,1)}), bf16[64,128,256]{2,1,0:T(8,128)(2,1)}, u32[]{:S(2)}, u32[]{:S(2)}) async-start(bf16[64,128,256]{2,1,0:T(8,128)(2,1)} %copy.79), calls=%async_computation | async-start | bytes 8388608 | tf_op jit(solution)/shard_map/all_to_all | solution.py:83
  243.4 26.3 %all-to-all-start.1 = ((bf16[8,32,2048]{2,1,0:T(8,128)(2,1)}), bf16[8,32,2048]{2,1,0:T(8,128)(2,1)S(1)}, u32[]{:S(2)}, u32[]{:S(2)}) async-start(bf16[8,32,2048]{2,1,0:T(8,128)(2,1)} %bitcast.14), calls=%async_computation.1 | async-start | bytes 2097152 | tf_op jit(solution)/shard_map/all_to_all | solution.py:23
where the time goes:
time: 271 us; the launch traced here: 270 us
  waiting for transfers between devices  196 us (72%)
  starting transfers between devices  31.1 us (11%)
  local copies, waits for them, and re-layouts  22.2 us (8%)
  matrix products  12.3 us (5%)
  other arithmetic  7.6 us (3%)
    all_to_all x1, waiting for transfers between devices, local(): lax.all_to_all(outgoing, 'kv', split_axis=0, concat_axis=0, tiled=True)  182 us
    all_to_all x1, starting transfers between devices, local(): lax.all_to_all(outgoing, 'kv', split_axis=0, concat_axis=0, tiled=True)  19.7 us
    all_to_all x1, waiting for transfers between devices, summed_on_arrival(): tiles = lax.all_to_all(in_blocks(value, dim, size), axis, 0, 0, tiled=True)  14.3 us
    all_to_all x1, starting transfers between devices, summed_on_arrival(): tiles = lax.all_to_all(in_blocks(value, dim, size), axis, 0, 0, tiled=True)  11.4 us
  transfers between devices with their start and end apart: 2, of which 2 were waited for; matrix products, arithmetic and copies ran while one was open for 1% of the time, Pallas kernels for 0%

commit v1 on v0

v1 whole, which is shorter than its diff:
```python
import functools

import jax
import jax.numpy as jnp
from jax import lax
from jax.experimental import pallas as pl
from jax.experimental.pallas import tpu as pltpu
from jax.sharding import Mesh
from jax.sharding import PartitionSpec as P

HEAD_DIM = 64
BLK = 64
SEL = 16
ROWS = 256
PER = 4
WIDTH = 128
RING = 8
TEAM = 8
QB = TEAM * PER
MAXP = QB * SEL
UNROLL = 8
STATS = 16

rotary_base = 500000.0
masked_score = -1e30
f32 = jnp.float32
bf16 = jnp.bfloat16


def project_kernel(x_ref, wq_ref, wk_ref, wv_ref, cos_ref, sin_ref, q_ref, kv_ref):
    x = x_ref[...]
    cos = cos_ref[...]
    sin = sin_ref[...]
    lane = lax.broadcasted_iota(jnp.int32, (ROWS, WIDTH), 1)
    first = (lane & (HEAD_DIM - 1)) < HEAD_DIM // 2

    def turned(t):
        partner = jnp.where(first, pltpu.roll(t, WIDTH - HEAD_DIM // 2, 1), pltpu.roll(t, HEAD_DIM // 2, 1))
        return t * cos + partner * sin

    k = jnp.dot(x, wk_ref[...], preferred_element_type=f32)
    kv_ref[:, :WIDTH] = turned(k).astype(bf16)
    v = jnp.dot(x, wv_ref[...], preferred_element_type=f32)
    kv_ref[:, WIDTH:] = v.astype(bf16)
    q = jnp.dot(x, wq_ref[...], preferred_element_type=f32)
    q = (turned(q) * (HEAD_DIM**-0.5)).astype(bf16)
    for i in range(TEAM):
        q_ref[i] = q


def project(x, wq, wk, wv, cos, sin):
    return pl.pallas_call(
        project_kernel,
        out_shape=(
            jax.ShapeDtypeStruct((TEAM, ROWS, WIDTH), bf16),
            jax.ShapeDtypeStruct((ROWS, 2 * WIDTH), bf16),
        ),
        name="project",
    )(x, wq, wk, wv, cos, sin)


def attend_kernel(pairs_ref, count_ref, q_ref, *refs):
    kv_refs = refs[:RING]
    out_ref = refs[RING]
    qq, kbuf, vbuf, sbuf, mbuf, lbuf, acc, lse = refs[RING + 1 :]
    lane = lax.broadcasted_iota(jnp.int32, (BLK, WIDTH), 1)
    left = lane < HEAD_DIM
    for s in range(RING):
        for b in range(PER):
            rows = pl.ds(b * BLK, BLK)
            kbuf[s * PER + b] = kv_refs[s][rows, :WIDTH]
            vbuf[s * PER + b] = kv_refs[s][rows, WIDTH:]
    zero = jnp.zeros((BLK, WIDTH), bf16)
    for i in range(TEAM):
        for b in range(PER):
            q = q_ref[i, pl.ds(b * BLK, BLK), :]
            qq[i * PER + b, :BLK, :] = jnp.where(left, q, zero)
            qq[i * PER + b, BLK:, :] = jnp.where(left, zero, q)
    qq[QB] = jnp.zeros((2 * BLK, WIDTH), bf16)
    mbuf[...] = jnp.full(mbuf.shape, masked_score, f32)
    lbuf[...] = jnp.zeros(lbuf.shape, f32)
    acc[...] = jnp.zeros(acc.shape, f32)
    trips = count_ref[0]

    def score(it, carry):
        for u in range(UNROLL):
            i = it * UNROLL + u
            code = pairs_ref[i]
            qi = code >> 6
            ki = code & 63
            st = lax.dot_general(
                kbuf[ki], qq[qi], (((1,), (1,)), ((), ())), preferred_element_type=f32
            )
            sbuf[i] = st
            m8 = jnp.max(st.reshape(8, 8, WIDTH), axis=0)
            mbuf[qi] = jnp.maximum(mbuf[qi], m8)
        return carry

    lax.fori_loop(0, trips, score, 0)
    for i in range(QB + 1):
        mbuf[i] = jnp.broadcast_to(jnp.max(mbuf[i], axis=0, keepdims=True), (8, WIDTH))

    def weigh(it, carry):
        for u in range(UNROLL):
            i = it * UNROLL + u
            code = pairs_ref[i]
            qi = code >> 6
            ki = code & 63
            p = jnp.exp(sbuf[i].reshape(8, 8, WIDTH) - mbuf[qi][None])
            lbuf[qi] = lbuf[qi] + jnp.sum(p, axis=0)
            pb = p.reshape(BLK, WIDTH).astype(bf16)
            ot = lax.dot_general(
                vbuf[ki], pb, (((0,), (0,)), ((), ())), preferred_element_type=f32
            )
            acc[qi] = acc[qi] + jnp.where(left, ot[:HEAD_DIM], ot[HEAD_DIM:])
        return carry

    lax.fori_loop(0, trips, weigh, 0)
    for i in range(QB):
        total = jnp.sum(lbuf[i], axis=0, keepdims=True)
        some = total > 0.0
        safe = jnp.where(some, total, 1.0)
        out_ref[i // PER, pl.ds((i % PER) * BLK, BLK), :] = (acc[i] * (1.0 / safe)).astype(bf16)
        lse[pl.ds(i, 1), :] = jnp.where(some, mbuf[i, :1, :] + jnp.log(safe), masked_score)
    for i in range(TEAM):
        value = lse[pl.ds(i * PER, PER), :]
        hi = value.astype(bf16).astype(f32)
        rest = value - hi
        mid = rest.astype(bf16).astype(f32)
        parts = jnp.concatenate([hi, mid, rest - mid, jnp.zeros((PER, WIDTH), f32)], axis=0)
        out_ref[i, pl.ds(ROWS, STATS), :] = parts.astype(bf16)


def attend(pairs, count, q, kvs):
    smem = pl.BlockSpec(memory_space=pltpu.SMEM)
    vmem = pl.BlockSpec(memory_space=pltpu.VMEM)
    return pl.pallas_call(
        attend_kernel,
        out_shape=jax.ShapeDtypeStruct((TEAM, ROWS + STATS, WIDTH), bf16),
        in_specs=[smem, smem] + [vmem] * (1 + RING),
        out_specs=vmem,
        scratch_shapes=[
            pltpu.VMEM((QB + 1, 2 * BLK, WIDTH), bf16),
            pltpu.VMEM((RING * PER, BLK, WIDTH), bf16),
            pltpu.VMEM((RING * PER, BLK, WIDTH), bf16),
            pltpu.VMEM((MAXP, BLK, WIDTH), f32),
            pltpu.VMEM((QB + 1, 8, WIDTH), f32),
            pltpu.VMEM((QB + 1, 8, WIDTH), f32),
            pltpu.VMEM((QB + 1, BLK, WIDTH), f32),
            pltpu.VMEM((QB, WIDTH), f32),
        ],
        name="attend",
    )(pairs, count, q, *kvs)


def merge_kernel(part_ref, att_ref, log_ref):
    values = []
    for i in range(TEAM):
        st = part_ref[i, pl.ds(ROWS, STATS), :].astype(f32)
        values.append(st[:PER] + st[PER : 2 * PER] + st[2 * PER : 3 * PER])
    top = functools.reduce(jnp.maximum, values)
    weights = [jnp.exp(v - top) for v in values]
    total = functools.reduce(jnp.add, weights)
    log_ref[...] = top + jnp.log(total)
    inverse = 1.0 / total
    weights = [w * inverse for w in weights]
    for b in range(PER):
        rows = pl.ds(b * BLK, BLK)
        att = jnp.zeros((BLK, WIDTH), f32)
        for i in range(TEAM):
            att = att + part_ref[i, rows, :].astype(f32) * weights[i][b : b + 1, :]
        turned = att.T
        att_ref[rows, :] = jnp.concatenate([turned[:BLK], turned[BLK:]], axis=1).astype(bf16)


def merge(parts):
    return pl.pallas_call(
        merge_kernel,
        out_shape=(
            jax.ShapeDtypeStruct((ROWS, WIDTH), bf16),
            jax.ShapeDtypeStruct((PER, WIDTH), f32),
        ),
        name="merge",
    )(parts)


def pair_list(chosen, zh, mine):
    lists = lax.dynamic_slice_in_dim(chosen, zh * QB, QB, 0)
    here = (lists >= 0) & (((lists >> 2) & (TEAM - 1)) == mine)
    slot = (zh - (lists >> 5)) & (RING - 1)
    code = jnp.arange(QB, dtype=jnp.int32)[:, None] * 64 + slot * PER + (lists & (PER - 1))
    here = here.reshape(-1)
    code = code.reshape(-1)
    index = jnp.arange(MAXP, dtype=jnp.int32)
    before = jnp.sum(jnp.where(index[:, None] < index[None, :], here[:, None], False).astype(jnp.int32), axis=0)
    place = jnp.where(here, before, -1)
    hit = place[:, None] == index[None, :]
    pairs = jnp.sum(jnp.where(hit, code[:, None], 0), axis=0)
    count = jnp.sum(here.astype(jnp.int32))
    pairs = jnp.where(index < count, pairs, QB * 64)
    return pairs, ((count + UNROLL - 1) // UNROLL).reshape(1)


def shifted(value, step):
    return lax.ppermute(value, "zh", [(i, (i + step) % RING) for i in range(RING)])


def local(tokens, w_query, w_key, w_value, w_out, chosen):
    zh = lax.axis_index("zh")
    mine = lax.axis_index(("zl", "y"))
    device = zh * TEAM + mine
    positions = device * ROWS + jnp.arange(ROWS)
    half = HEAD_DIM // 2
    inverse = rotary_base ** (-jnp.arange(half, dtype=f32) / half)
    angles = positions.astype(f32)[:, None] * jnp.tile(inverse, 2 * WIDTH // HEAD_DIM)[None, :]
    sign = jnp.where((jnp.arange(WIDTH) & (HEAD_DIM - 1)) < half, -1.0, 1.0).astype(f32)
    q8, kv = project(
        tokens, w_query, w_key, w_value, jnp.cos(angles), jnp.sin(angles) * sign[None, :]
    )
    pairs, count = pair_list(chosen, zh, mine)
    q_team = lax.all_to_all(q8, ("zl", "y"), 0, 0, tiled=True)
    w_all = lax.all_to_all(
        jnp.broadcast_to(w_out[None], (8,) + w_out.shape), ("x", "c"), 0, 0, tiled=True
    )
    slots = [kv] + [None] * (RING - 1)
    up = down = kv
    for s in range(1, RING // 2 + 1):
        up = shifted(up, 1)
        slots[s] = up
        if s < RING // 2:
            down = shifted(down, -1)
            slots[RING - s] = down
    parts = attend(pairs, count, q_team, slots)
    parts = lax.all_to_all(parts, ("zl", "y"), 0, 0, tiled=True)
    attended, logs = merge(parts)
    log_sums = jnp.transpose(logs.reshape(PER, 2, BLK), (1, 0, 2)).reshape(2, ROWS)
    rows = lax.all_to_all(attended.reshape(8, ROWS // 8, WIDTH), ("x", "c"), 0, 0, tiled=True)
    output = jnp.einsum("trc,tcn->rn", rows, w_all, preferred_element_type=f32)
    return (output.astype(bf16), log_sums)


def solution(mesh):
    fine = Mesh(mesh.devices.reshape(8, 2, 4, 4, 2), ("zh", "zl", "y", "x", "c"))
    kv = ("zh", "zl", "y")
    tp = ("x", "c")
    placed = (P(kv, None), P(None, tp), P(None, tp), P(None, tp), P(tp, None), P())
    return jax.shard_map(
        local,
        mesh=fine,
        in_specs=placed,
        out_specs=(P(kv + tp, None), P(tp, kv)),
        check_vma=False,
    )
```

time: 271 us -> 158 us (0.58)
  waiting for transfers between devices: 196 us -> 62 us
  starting transfers between devices: 31.1 us -> 55.9 us
  local copies, waits for them, and re-layouts: 22.2 us -> 5.17 us
  Pallas kernels: 0 us -> 13.6 us
  blocking collectives: 0 us -> 12.1 us
  matrix products: 12.3 us -> 3.67 us
  other arithmetic: 7.6 us -> 3.45 us
    all_to_all x2 -> x3, waiting for transfers between devices: 196 us -> 50.3 us  [the longest x1 46.8 us: local(): lax.all_to_all(jnp.broadcast_to(w_out[None], (8,) + w_out.shape), ('x', '...]
    ppermute x0 -> x7, starting transfers between devices: none -> 29.7 us  [shifted(): lax.ppermute(value, 'zh', [(i, (i + step) % RING) for i in range(RING)])]
    pallas_call x0 -> x3, Pallas kernels: none -> 13.6 us  [the longest x1 7.99 us: attend(): pl.pallas_call(attend_kernel, out_shape=jax.ShapeDtypeStruct((TEAM, ROWS...]
    reshape x6 -> x3, local copies, waits for them, and re-layouts: 14.8 us -> 1.51 us  [the longest x1 0.76 us: local(): logs.reshape(PER, 2, BLK)]
    all_to_all x0 -> x1, blocking collectives: none -> 12.1 us  [local(): parts = lax.all_to_all(parts, ('zl', 'y'), 0, 0, tiled=True)]
    ppermute x0 -> x7, waiting for transfers between devices: none -> 11.7 us  [shifted(): lax.ppermute(value, 'zh', [(i, (i + step) % RING) for i in range(RING)])]
    dot_general x7 -> x1, matrix products: 12.3 us -> 3.67 us  [local(): output = jnp.einsum('trc,tcn->rn', rows, w_all, preferred_element_type=f32)]
    all_to_all x2 -> x3, starting transfers between devices: 31.1 us -> 26.2 us  [the longest x1 15.6 us: local(): lax.all_to_all(jnp.broadcast_to(w_out[None], (8,) + w_out.shape), ('x', '...]
  transfers between devices with their start and end apart: 2 -> 10, of which waited for: 2 -> 6; matrix products, arithmetic and copies ran while one was open for 1% -> 3% of each run, Pallas kernels for 0% -> 1%
where the time goes in v1:
time: 158 us; the launch traced here: 157 us
  waiting for transfers between devices  62 us (39%)
  starting transfers between devices  55.9 us (35%)
  Pallas kernels  13.6 us (9%)
  blocking collectives  12.1 us (8%)
  local copies, waits for them, and re-layouts  5.17 us (3%)
  matrix products  3.67 us (2%)
  other arithmetic  3.45 us (2%)
    all_to_all x1, waiting for transfers between devices, local(): lax.all_to_all(jnp.broadcast_to(w_out[None], (8,) + w_out.shape), ('x', '...  46.8 us
    ppermute x7, starting transfers between devices, shifted(): lax.ppermute(value, 'zh', [(i, (i + step) % RING) for i in range(RING)])  29.7 us
    all_to_all x1, starting transfers between devices, local(): lax.all_to_all(jnp.broadcast_to(w_out[None], (8,) + w_out.shape), ('x', '...  15.6 us
    all_to_all x1, blocking collectives, local(): parts = lax.all_to_all(parts, ('zl', 'y'), 0, 0, tiled=True)  12.1 us
    ppermute x7, waiting for transfers between devices, shifted(): lax.ppermute(value, 'zh', [(i, (i + step) % RING) for i in range(RING)])  11.7 us
    pallas_call x1, Pallas kernels, attend(): pl.pallas_call(attend_kernel, out_shape=jax.ShapeDtypeStruct((TEAM, ROWS...  7.99 us
    all_to_all x1, starting transfers between devices, local(): q_team = lax.all_to_all(q8, ('zl', 'y'), 0, 0, tiled=True)  6.36 us
    all_to_all x1, starting transfers between devices, local(): lax.all_to_all(attended.reshape(8, ROWS // 8, WIDTH), ('x', 'c'), 0, 0, t...  4.22 us
  transfers between devices with their start and end apart: 10, of which 6 were waited for; matrix products, arithmetic and copies ran while one was open for 3% of the time, Pallas kernels for 1%

profile of v1, /device:TPU:1, one launch (start us, length us, event | category | flops | bytes accessed | tf_op | source)
XLA Modules:
  0.0 157.2 jit_solution(6483290334426369720)
XLA Ops:
  0.8 1.2 fusion.2
  2.0 3.6 %project.1 = (bf16[8,256,128]{2,1,0:T(8,128)(2,1)}, bf16[256,256]{1,0:T(8,128)(2,1)}) custom-call(bf16[256,2048]{1,0:T(8,128)(2,1)} %x_ref.1, bf16[2048,128]{1,0:T(8,128)(2,1)} %wq_ref.1, bf16[2048,128]{1,0:T(8,128)(2,1)} %wk_ref.1, bf16[2048,128]{1,0:T(8,128)(2,1)} %wv_ref.1, f32[256,128]{1,0:T(8,128)} %get-tuple-element.14.cos_ref, ...), custom_call_target="tpu_custom_call" | custom-call | tf_op jit(solution)/shard_map/project/pallas_call | solution.py:52
  5.6 6.4 %all-to-all-start = ((bf16[8,256,128]{2,1,0:T(8,128)(2,1)}), bf16[8,256,128]{2,1,0:T(8,128)(2,1)S(1)}, u32[]{:S(2)}, u32[]{:S(2)}) async-start(bf16[8,256,128]{2,1,0:T(8,128)(2,1)} %get-tuple-element.6), calls=%async_computation | async-start | bytes 1048576 | tf_op jit(solution)/shard_map/all_to_all | solution.py:221
  12.0 10.7 %collective-permute-start.4 = (bf16[256,256]{1,0:T(8,128)(2,1)}, bf16[256,256]{1,0:T(8,128)(2,1)S(1)}, u32[]{:S(2)}, u32[]{:S(2)}) collective-permute-start(bf16[256,256]{1,0:T(8,128)(2,1)} %get-tuple-element.7.refs_0_), channel_id=1, source_target_pairs={{0,448},{64,0},{128,64},{192,128},{256,192},{320,256},{384,320},{4... | collective-permute-start | bytes 393224 | tf_op jit(solution)/shard_map/ppermute | solution.py:205
  22.7 1.9 %collective-permute-start = (bf16[256,256]{1,0:T(8,128)(2,1)}, bf16[256,256]{1,0:T(8,128)(2,1)S(1)}, u32[]{:S(2)}, u32[]{:S(2)}) collective-permute-start(bf16[256,256]{1,0:T(8,128)(2,1)} %get-tuple-element.7.refs_0_), channel_id=1, source_target_pairs={{0,64},{64,128},{128,192},{192,256},{256,320},{320,384},{384,448},... | collective-permute-start | bytes 393224 | tf_op jit(solution)/shard_map/ppermute | solution.py:205
  24.6 0.7 convert_reduce_fusion.1
  25.9 0.1 copy.12
  26.2 0.2 convert_reduce_fusion
  26.4 4.6 %collective-permute-done.refs_1_ = bf16[256,256]{1,0:T(8,128)(2,1)S(1)} collective-permute-done((bf16[256,256]{1,0:T(8,128)(2,1)}, bf16[256,256]{1,0:T(8,128)(2,1)S(1)}, u32[]{:S(2)}, u32[]{:S(2)}) %collective-permute-start) | collective-permute-done | bytes 131104 | tf_op jit(solution)/shard_map/ppermute | solution.py:205
  30.9 1.9 %collective-permute-start.1 = (bf16[256,256]{1,0:T(8,128)(2,1)S(1)}, bf16[256,256]{1,0:T(8,128)(2,1)S(1)}, u32[]{:S(2)}, u32[]{:S(2)}) collective-permute-start(bf16[256,256]{1,0:T(8,128)(2,1)S(1)} %collective-permute-done.refs_1_), channel_id=1, source_target_pairs={{0,64},{64,128},{128,192},{192,256},{256,320},{320,384},{384,448},... | collective-permute-start | bytes 393224 | tf_op jit(solution)/shard_map/ppermute | solution.py:205
  32.9 5.5 %collective-permute-start.5 = (bf16[256,256]{1,0:T(8,128)(2,1)S(1)}, bf16[256,256]{1,0:T(8,128)(2,1)S(1)}, u32[]{:S(2)}, u32[]{:S(2)}) collective-permute-start(bf16[256,256]{1,0:T(8,128)(2,1)S(1)} %collective-permute-done.4.refs_7_), channel_id=1, source_target_pairs={{0,448},{64,0},{128,64},{192,128},{256,192},{320,256},{384,320},{4... | collective-permute-start | bytes 393224 | tf_op jit(solution)/shard_map/ppermute | solution.py:205
  38.4 0.4 collective-permute-done.1.refs_2_
  38.8 1.9 %collective-permute-start.2 = (bf16[256,256]{1,0:T(8,128)(2,1)S(1)}, bf16[256,256]{1,0:T(8,128)(2,1)S(1)}, u32[]{:S(2)}, u32[]{:S(2)}) collective-permute-start(bf16[256,256]{1,0:T(8,128)(2,1)S(1)} %collective-permute-done.1.refs_2_), channel_id=1, source_target_pairs={{0,64},{64,128},{128,192},{192,256},{256,320},{320,384},{384,448},... | collective-permute-start | bytes 393224 | tf_op jit(solution)/shard_map/ppermute | solution.py:205
  40.7 0.2 select_reduce_fusion
  40.9 5.5 %collective-permute-start.6 = (bf16[256,256]{1,0:T(8,128)(2,1)S(1)}, bf16[256,256]{1,0:T(8,128)(2,1)S(1)}, u32[]{:S(2)}, u32[]{:S(2)}) collective-permute-start(bf16[256,256]{1,0:T(8,128)(2,1)S(1)} %collective-permute-done.5.refs_6_), channel_id=1, source_target_pairs={{0,448},{64,0},{128,64},{192,128},{256,192},{320,256},{384,320},{4... | collective-permute-start | bytes 393224 | tf_op jit(solution)/shard_map/ppermute | solution.py:205
  46.4 0.2 collective-permute-done.2.refs_3_
  46.6 2.4 %collective-permute-start.3 = (bf16[256,256]{1,0:T(8,128)(2,1)S(1)}, bf16[256,256]{1,0:T(8,128)(2,1)S(1)}, u32[]{:S(2)}, u32[]{:S(2)}) collective-permute-start(bf16[256,256]{1,0:T(8,128)(2,1)S(1)} %collective-permute-done.2.refs_3_), channel_id=1, source_target_pairs={{0,64},{64,128},{128,192},{192,256},{256,320},{320,384},{384,448},... | collective-permute-start | bytes 393224 | tf_op jit(solution)/shard_map/ppermute | solution.py:205
  49.0 1.1 fusion.4.pairs_ref
  50.1 6.5 %collective-permute-done.3.refs_4_ = bf16[256,256]{1,0:T(8,128)(2,1)S(1)} collective-permute-done((bf16[256,256]{1,0:T(8,128)(2,1)S(1)}, bf16[256,256]{1,0:T(8,128)(2,1)S(1)}, u32[]{:S(2)}, u32[]{:S(2)}) %collective-permute-start.3) | collective-permute-done | bytes 131104 | tf_op jit(solution)/shard_map/ppermute | solution.py:205
  56.7 0.6 copy-done.8
  57.3 0.2 copy-done
  57.5 8.0 %attend.1 = bf16[8,272,128]{2,1,0:T(8,128)(2,1)} custom-call(s32[512]{0:T(512)} %fusion.4.pairs_ref, s32[1]{0:T(128)} %bitcast.count_ref, bf16[8,256,128]{2,1,0:T(8,128)(2,1)} %copy-done, bf16[256,256]{1,0:T(8,128)(2,1)} %get-tuple-element.7.refs_0_, bf16[256,256]{1,0:T(8,128)(2,1)} %copy-done.3, bf16[256,256]{1,0:T(8,128)(2,1)} %copy-done.4, ...), custom_call_target="tpu_custom_call" | custom-call | tf_op jit(solution)/shard_map/attend/pallas_call | solution.py:137
  65.5 12.1 %all_to_all.20.part_ref = bf16[8,272,128]{2,1,0:T(8,128)(2,1)} all-to-all(bf16[8,272,128]{2,1,0:T(8,128)(2,1)} %attend.1), channel_id=1, replica_groups=mesh['zh'=8,'zl'=2,'y'=4,'x'=4,'c'=2] {'zl','y'}, dimensions={0} | all-to-all | bytes 1114112 | tf_op jit(solution)/shard_map/all_to_all | solution.py:234
  77.6 2.5 %broadcast_in_dim.63 = bf16[8,128,2048]{2,1,0:T(8,128)(2,1)} broadcast(bf16[128,2048]{1,0:T(8,128)(2,1)S(1)} %copy-done.1), dimensions={1,2} | broadcast | bytes 4718592 | tf_op jit(solution)/shard_map/broadcast_in_dim | solution.py:223
  80.1 15.6 %all-to-all-start.3 = ((bf16[8,128,2048]{2,1,0:T(8,128)(2,1)}), bf16[8,128,2048]{2,1,0:T(8,128)(2,1)}, u32[]{:S(2)}, u32[]{:S(2)}) async-start(bf16[8,128,2048]{2,1,0:T(8,128)(2,1)} %broadcast_in_dim.63), calls=%async_computation.3 | async-start | bytes 8388608 | tf_op jit(solution)/shard_map/all_to_all | solution.py:222
  95.6 2.0 %merge.1 = (bf16[256,128]{1,0:T(8,128)(2,1)}, f32[4,128]{1,0:T(4,128)}) custom-call(bf16[8,272,128]{2,1,0:T(8,128)(2,1)} %all_to_all.20.part_ref), custom_call_target="tpu_custom_call" | custom-call | tf_op jit(solution)/shard_map/merge/pallas_call | solution.py:177
  97.6 46.8 %all-to-all-done.3 = bf16[8,128,2048]{2,1,0:T(8,128)(2,1)} async-done(((bf16[8,128,2048]{2,1,0:T(8,128)(2,1)}), bf16[8,128,2048]{2,1,0:T(8,128)(2,1)}, u32[]{:S(2)}, u32[]{:S(2)}) %all-to-all-start.3) | async-done | bytes 4194336 | tf_op jit(solution)/shard_map/all_to_all | solution.py:222
  144.5 4.2 %all-to-all-start.2 = ((bf16[8,32,128]{2,1,0:T(8,128)(2,1)}), bf16[8,32,128]{2,1,0:T(8,128)(2,1)S(1)}, u32[]{:S(2)}, u32[]{:S(2)}) async-start(bf16[8,32,128]{2,1,0:T(8,128)(2,1)} %bitcast.9), calls=%async_computation.2 | async-start | bytes 131072 | tf_op jit(solution)/shard_map/all_to_all | solution.py:237
  148.7 0.8 reshape.55
  149.4 0.7 reshape.56
  150.1 3.4 %all-to-all-done.2 = bf16[8,32,128]{2,1,0:T(8,128)(2,1)S(1)} async-done(((bf16[8,32,128]{2,1,0:T(8,128)(2,1)}), bf16[8,32,128]{2,1,0:T(8,128)(2,1)S(1)}, u32[]{:S(2)}, u32[]{:S(2)}) %all-to-all-start.2) | async-done | bytes 65568 | tf_op jit(solution)/shard_map/all_to_all | solution.py:237
  153.5 3.7 %fusion = bf16[32,2048]{1,0:T(8,128)(2,1)} fusion(bf16[8,32,128]{2,1,0:T(8,128)(2,1)S(1)} %all-to-all-done.2, bf16[8,128,2048]{2,1,0:T(8,128)(2,1)} %all-to-all-done.3), kind=kOutput, calls=%fused_computation.1 | convolution fusion | flops 134283264 | bytes 4390912 | tf_op jit(solution)/shard_map/trc,tcn->rn/dot_general | solution.py:238
  (33 shorter events, 0.4 us)
Async XLA Ops:
  0.6 24.0 %copy-start.9 = (s32[256,16]{0,1:T(8,128)S(1)}, s32[256,16]{0,1:T(8,128)}, u32[]{:S(2)}) copy-start(s32[256,16]{0,1:T(8,128)} %param.11) | copy-start | bytes 49156
  0.6 76.9 %copy-start.1 = (bf16[128,2048]{1,0:T(8,128)(2,1)S(1)}, bf16[128,2048]{1,0:T(8,128)(2,1)}, u32[]{:S(2)}) copy-start(bf16[128,2048]{1,0:T(8,128)(2,1)} %param.10) | copy-start | bytes 1572868
  5.6 51.0 %all-to-all-start = ((bf16[8,256,128]{2,1,0:T(8,128)(2,1)}), bf16[8,256,128]{2,1,0:T(8,128)(2,1)S(1)}, u32[]{:S(2)}, u32[]{:S(2)}) async-start(bf16[8,256,128]{2,1,0:T(8,128)(2,1)} %get-tuple-element.6), calls=%async_computation | async-start | bytes 1048576 | tf_op jit(solution)/shard_map/all_to_all | solution.py:221
  12.0 20.9 %collective-permute-start.4 = (bf16[256,256]{1,0:T(8,128)(2,1)}, bf16[256,256]{1,0:T(8,128)(2,1)S(1)}, u32[]{:S(2)}, u32[]{:S(2)}) collective-permute-start(bf16[256,256]{1,0:T(8,128)(2,1)} %get-tuple-element.7.refs_0_), channel_id=1, source_target_pairs={{0,448},{64,0},{128,64},{192,128},{256,192},{320,256},{384,320},{4... | collective-permute-start | bytes 393224 | tf_op jit(solution)/shard_map/ppermute | solution.py:205
  22.7 8.3 %collective-permute-start = (bf16[256,256]{1,0:T(8,128)(2,1)}, bf16[256,256]{1,0:T(8,128)(2,1)S(1)}, u32[]{:S(2)}, u32[]{:S(2)}) collective-permute-start(bf16[256,256]{1,0:T(8,128)(2,1)} %get-tuple-element.7.refs_0_), channel_id=1, source_target_pairs={{0,64},{64,128},{128,192},{192,256},{256,320},{320,384},{384,448},... | collective-permute-start | bytes 393224 | tf_op jit(solution)/shard_map/ppermute | solution.py:205
  30.9 25.7 %copy-start.3 = (bf16[256,256]{1,0:T(8,128)(2,1)}, bf16[256,256]{1,0:T(8,128)(2,1)S(1)}, u32[]{:S(2)}) copy-start(bf16[256,256]{1,0:T(8,128)(2,1)S(1)} %collective-permute-done.refs_1_) | copy-start | bytes 393220
  30.9 7.8 %collective-permute-start.1 = (bf16[256,256]{1,0:T(8,128)(2,1)S(1)}, bf16[256,256]{1,0:T(8,128)(2,1)S(1)}, u32[]{:S(2)}, u32[]{:S(2)}) collective-permute-start(bf16[256,256]{1,0:T(8,128)(2,1)S(1)} %collective-permute-done.refs_1_), channel_id=1, source_target_pairs={{0,64},{64,128},{128,192},{192,256},{256,320},{320,384},{384,448},... | collective-permute-start | bytes 393224 | tf_op jit(solution)/shard_map/ppermute | solution.py:205
  32.9 23.8 %copy-start.2 = (bf16[256,256]{1,0:T(8,128)(2,1)}, bf16[256,256]{1,0:T(8,128)(2,1)S(1)}, u32[]{:S(2)}) copy-start(bf16[256,256]{1,0:T(8,128)(2,1)S(1)} %collective-permute-done.4.refs_7_) | copy-start | bytes 393220
  32.9 8.0 %collective-permute-start.5 = (bf16[256,256]{1,0:T(8,128)(2,1)S(1)}, bf16[256,256]{1,0:T(8,128)(2,1)S(1)}, u32[]{:S(2)}, u32[]{:S(2)}) collective-permute-start(bf16[256,256]{1,0:T(8,128)(2,1)S(1)} %collective-permute-done.4.refs_7_), channel_id=1, source_target_pairs={{0,448},{64,0},{128,64},{192,128},{256,192},{320,256},{384,320},{4... | collective-permute-start | bytes 393224 | tf_op jit(solution)/shard_map/ppermute | solution.py:205
  38.8 17.9 %copy-start.4 = (bf16[256,256]{1,0:T(8,128)(2,1)}, bf16[256,256]{1,0:T(8,128)(2,1)S(1)}, u32[]{:S(2)}) copy-start(bf16[256,256]{1,0:T(8,128)(2,1)S(1)} %collective-permute-done.1.refs_2_) | copy-start | bytes 393220
  38.8 7.8 %collective-permute-start.2 = (bf16[256,256]{1,0:T(8,128)(2,1)S(1)}, bf16[256,256]{1,0:T(8,128)(2,1)S(1)}, u32[]{:S(2)}, u32[]{:S(2)}) collective-permute-start(bf16[256,256]{1,0:T(8,128)(2,1)S(1)} %collective-permute-done.1.refs_2_), channel_id=1, source_target_pairs={{0,64},{64,128},{128,192},{192,256},{256,320},{320,384},{384,448},... | collective-permute-start | bytes 393224 | tf_op jit(solution)/shard_map/ppermute | solution.py:205
  40.9 15.8 %copy-start.5 = (bf16[256,256]{1,0:T(8,128)(2,1)}, bf16[256,256]{1,0:T(8,128)(2,1)S(1)}, u32[]{:S(2)}) copy-start(bf16[256,256]{1,0:T(8,128)(2,1)S(1)} %collective-permute-done.5.refs_6_) | copy-start | bytes 393220
  40.9 9.2 %collective-permute-start.6 = (bf16[256,256]{1,0:T(8,128)(2,1)S(1)}, bf16[256,256]{1,0:T(8,128)(2,1)S(1)}, u32[]{:S(2)}, u32[]{:S(2)}) collective-permute-start(bf16[256,256]{1,0:T(8,128)(2,1)S(1)} %collective-permute-done.5.refs_6_), channel_id=1, source_target_pairs={{0,448},{64,0},{128,64},{192,128},{256,192},{320,256},{384,320},{4... | collective-permute-start | bytes 393224 | tf_op jit(solution)/shard_map/ppermute | solution.py:205
  46.6 10.1 %copy-start.6 = (bf16[256,256]{1,0:T(8,128)(2,1)}, bf16[256,256]{1,0:T(8,128)(2,1)S(1)}, u32[]{:S(2)}) copy-start(bf16[256,256]{1,0:T(8,128)(2,1)S(1)} %collective-permute-done.2.refs_3_) | copy-start | bytes 393220
  46.6 10.1 %collective-permute-start.3 = (bf16[256,256]{1,0:T(8,128)(2,1)S(1)}, bf16[256,256]{1,0:T(8,128)(2,1)S(1)}, u32[]{:S(2)}, u32[]{:S(2)}) collective-permute-start(bf16[256,256]{1,0:T(8,128)(2,1)S(1)} %collective-permute-done.2.refs_3_), channel_id=1, source_target_pairs={{0,64},{64,128},{128,192},{192,256},{256,320},{320,384},{384,448},... | collective-permute-start | bytes 393224 | tf_op jit(solution)/shard_map/ppermute | solution.py:205
  50.1 6.6 %copy-start.7 = (bf16[256,256]{1,0:T(8,128)(2,1)}, bf16[256,256]{1,0:T(8,128)(2,1)S(1)}, u32[]{:S(2)}) copy-start(bf16[256,256]{1,0:T(8,128)(2,1)S(1)} %collective-permute-done.6.refs_5_) | copy-start | bytes 393220
  56.6 0.7 copy-start.8
  56.6 0.8 copy-start
  80.1 64.4 %all-to-all-start.3 = ((bf16[8,128,2048]{2,1,0:T(8,128)(2,1)}), bf16[8,128,2048]{2,1,0:T(8,128)(2,1)}, u32[]{:S(2)}, u32[]{:S(2)}) async-start(bf16[8,128,2048]{2,1,0:T(8,128)(2,1)} %broadcast_in_dim.63), calls=%async_computation.3 | async-start | bytes 8388608 | tf_op jit(solution)/shard_map/all_to_all | solution.py:222
  144.5 9.1 %all-to-all-start.2 = ((bf16[8,32,128]{2,1,0:T(8,128)(2,1)}), bf16[8,32,128]{2,1,0:T(8,128)(2,1)S(1)}, u32[]{:S(2)}, u32[]{:S(2)}) async-start(bf16[8,32,128]{2,1,0:T(8,128)(2,1)} %bitcast.9), calls=%async_computation.2 | async-start | bytes 131072 | tf_op jit(solution)/shard_map/all_to_all | solution.py:237

commit v2 on v1

--- a/solution.py
+++ b/solution.py
@@ -55,6 +55,7 @@
             jax.ShapeDtypeStruct((TEAM, ROWS, WIDTH), bf16),
             jax.ShapeDtypeStruct((ROWS, 2 * WIDTH), bf16),
         ),
+        compiler_params=pltpu.CompilerParams(vmem_limit_bytes=12 << 20),
         name="project",
     )(x, wq, wk, wv, cos, sin)
 
@@ -149,6 +150,7 @@
             pltpu.VMEM((QB + 1, BLK, WIDTH), f32),
             pltpu.VMEM((QB, WIDTH), f32),
         ],
+        compiler_params=pltpu.CompilerParams(vmem_limit_bytes=28 << 20),
         name="attend",
     )(pairs, count, q, *kvs)
 
@@ -180,6 +182,7 @@
             jax.ShapeDtypeStruct((ROWS, WIDTH), bf16),
             jax.ShapeDtypeStruct((PER, WIDTH), f32),
         ),
+        compiler_params=pltpu.CompilerParams(vmem_limit_bytes=4 << 20),
         name="merge",
     )(parts)
 
@@ -201,8 +204,13 @@
     return pairs, ((count + UNROLL - 1) // UNROLL).reshape(1)
 
 
-def shifted(value, step):
-    return lax.ppermute(value, "zh", [(i, (i + step) % RING) for i in range(RING)])
+def up_pairs(step):
+    return [(i, i + 1) for i in range(step - 1, RING - 1)]
+
+
+def down_pairs(step):
+    far = RING // 2 - 1
+    return [((r - step + 1) % RING, (r - step) % RING) for r in range(far)]
 
 
 def local(tokens, w_query, w_key, w_value, w_out, chosen):
@@ -218,24 +226,30 @@
         tokens, w_query, w_key, w_value, jnp.cos(angles), jnp.sin(angles) * sign[None, :]
     )
     pairs, count = pair_list(chosen, zh, mine)
-    q_team = lax.all_to_all(q8, ("zl", "y"), 0, 0, tiled=True)
-    w_all = lax.all_to_all(
-        jnp.broadcast_to(w_out[None], (8,) + w_out.shape), ("x", "c"), 0, 0, tiled=True
-    )
     slots = [kv] + [None] * (RING - 1)
     up = down = kv
     for s in range(1, RING // 2 + 1):
-        up = shifted(up, 1)
+        up = lax.ppermute(up, "zh", up_pairs(s))
         slots[s] = up
         if s < RING // 2:
-            down = shifted(down, -1)
+            down = lax.ppermute(down, "zh", down_pairs(s))
             slots[RING - s] = down
+    q_team = lax.all_to_all(q8, ("zl", "y"), 0, 0, tiled=True)
+    w_same = lax.all_to_all(
+        jnp.broadcast_to(w_out[None], (4,) + w_out.shape), "x", 0, 0, tiled=True
+    )
+    w_other = lax.ppermute(w_same, "c", [(0, 1), (1, 0)])
     parts = attend(pairs, count, q_team, slots)
     parts = lax.all_to_all(parts, ("zl", "y"), 0, 0, tiled=True)
     attended, logs = merge(parts)
     log_sums = jnp.transpose(logs.reshape(PER, 2, BLK), (1, 0, 2)).reshape(2, ROWS)
     rows = lax.all_to_all(attended.reshape(8, ROWS // 8, WIDTH), ("x", "c"), 0, 0, tiled=True)
-    output = jnp.einsum("trc,tcn->rn", rows, w_all, preferred_element_type=f32)
+    rows = rows.reshape(4, 2, ROWS // 8, WIDTH)
+    core = lax.axis_index("c")
+    rows_same = lax.dynamic_index_in_dim(rows, core, 1, keepdims=False)
+    rows_other = lax.dynamic_index_in_dim(rows, 1 - core, 1, keepdims=False)
+    output = jnp.einsum("trc,tcn->rn", rows_same, w_same, preferred_element_type=f32)
+    output = output + jnp.einsum("trc,tcn->rn", rows_other, w_other, preferred_element_type=f32)
     return (output.astype(bf16), log_sums)
 
 

time: 158 us -> 110 us (0.70)
  the two profiles are of different devices: /device:TPU:1 before, /device:TPU:288 now
where the time goes in v2:
time: 110 us
  waiting for transfers between devices  39.7 us (36%)
  starting transfers between devices  24.3 us (22%)
  Pallas kernels  17.1 us (16%)
  blocking collectives  14.4 us (13%)
  local copies, waits for them, and re-layouts  7.12 us (6%)
  matrix products  3.2 us (3%)
  other arithmetic  2.3 us (2%)
  between operations  1.52 us (1%)
    ppermute x4, waiting for transfers between devices, local(): up = lax.ppermute(up, 'zh', up_pairs(s))  29.6 us
    pallas_call x1, Pallas kernels, attend(): pl.pallas_call(attend_kernel, out_shape=jax.ShapeDtypeStruct((TEAM, ROWS...  15.1 us
    all_to_all x1, blocking collectives, local(): q_team = lax.all_to_all(q8, ('zl', 'y'), 0, 0, tiled=True)  14.4 us
    ppermute x4, starting transfers between devices, local(): up = lax.ppermute(up, 'zh', up_pairs(s))  9.11 us
    all_to_all x1, waiting for transfers between devices, local(): parts = lax.all_to_all(parts, ('zl', 'y'), 0, 0, tiled=True)  5.28 us
    all_to_all x1, waiting for transfers between devices, local(): lax.all_to_all(attended.reshape(8, ROWS // 8, WIDTH), ('x', 'c'), 0, 0, t...  4.79 us
    all_to_all x1, starting transfers between devices, local(): lax.all_to_all(jnp.broadcast_to(w_out[None], (4,) + w_out.shape), 'x', 0,...  4.43 us
    unnamed x12, local copies, waits for them, and re-layouts  4.35 us
  transfers between devices with their start and end apart: 11, of which 6 were waited for; matrix products, arithmetic and copies ran while one was open for 3% of the time, Pallas kernels for 15%

profile of v2, /device:TPU:288, one launch (start us, length us, event | category | flops | bytes accessed | tf_op | source)
XLA Modules:
  0.0 109.6 jit_solution(15146060254653937245)
XLA Ops:
  0.8 0.5 fusion.3
  1.3 1.2 %copy-done = bf16[256,2048]{1,0:T(8,128)(2,1)S(1)} copy-done((bf16[256,2048]{1,0:T(8,128)(2,1)S(1)}, bf16[256,2048]{1,0:T(8,128)(2,1)}, u32[]{:S(2)}) %copy-start) | copy-done | bytes 1048600
  2.5 1.0 copy-done.1
  3.6 1.0 copy-done.2
  4.6 1.0 copy-done.3
  5.7 1.0 project.1
  6.7 14.4 %all_to_all.20.q_ref = bf16[8,256,128]{2,1,0:T(8,128)(2,1)S(1)} all-to-all(bf16[8,256,128]{2,1,0:T(8,128)(2,1)S(1)} %get-tuple-element.6), channel_id=1, replica_groups=mesh['zh'=8,'zl'=2,'y'=4,'x'=4,'c'=2] {'zl','y'}, dimensions={0} | all-to-all | bytes 1048576 | tf_op jit(solution)/shard_map/all_to_all | solution.py:237
  21.1 1.6 %broadcast_in_dim.63 = bf16[4,128,2048]{2,1,0:T(8,128)(2,1)} broadcast(bf16[128,2048]{1,0:T(8,128)(2,1)S(1)} %copy-done.4), dimensions={1,2} | broadcast | bytes 2621440 | tf_op jit(solution)/shard_map/broadcast_in_dim | solution.py:239
  22.7 4.4 %all-to-all-start.3 = ((bf16[4,128,2048]{2,1,0:T(8,128)(2,1)}), bf16[4,128,2048]{2,1,0:T(8,128)(2,1)S(1)}, u32[]{:S(2)}, u32[]{:S(2)}) async-start(bf16[4,128,2048]{2,1,0:T(8,128)(2,1)} %broadcast_in_dim.63), calls=%async_computation.3 | async-start | bytes 4194304 | tf_op jit(solution)/shard_map/all_to_all | solution.py:238
  27.1 0.7 collective-permute-start.4
  27.8 3.4 %collective-permute-start = (bf16[256,256]{1,0:T(8,128)(2,1)S(1)}, bf16[256,256]{1,0:T(8,128)(2,1)S(1)}, u32[]{:S(2)}, u32[]{:S(2)}) collective-permute-start(bf16[256,256]{1,0:T(8,128)(2,1)S(1)} %get-tuple-element.7.refs_0_), channel_id=1, source_target_pairs={{0,64},{64,128},{128,192},{192,256},{256,320},{320,384},{384,448},... | collective-permute-start | bytes 393224 | tf_op jit(solution)/shard_map/ppermute | solution.py:232
  31.2 0.7 convert_reduce_fusion.1
  33.1 5.8 %collective-permute-done.refs_1_ = bf16[256,256]{1,0:T(8,128)(2,1)S(1)} collective-permute-done((bf16[256,256]{1,0:T(8,128)(2,1)S(1)}, bf16[256,256]{1,0:T(8,128)(2,1)S(1)}, u32[]{:S(2)}, u32[]{:S(2)}) %collective-permute-start) | collective-permute-done | bytes 131104 | tf_op jit(solution)/shard_map/ppermute | solution.py:232
  38.9 1.9 %collective-permute-start.1 = (bf16[256,256]{1,0:T(8,128)(2,1)S(1)}, bf16[256,256]{1,0:T(8,128)(2,1)S(1)}, u32[]{:S(2)}, u32[]{:S(2)}) collective-permute-start(bf16[256,256]{1,0:T(8,128)(2,1)S(1)} %collective-permute-done.refs_1_), channel_id=1, source_target_pairs={{64,128},{128,192},{192,256},{256,320},{320,384},{384,448},{65,129... | collective-permute-start | bytes 393224 | tf_op jit(solution)/shard_map/ppermute | solution.py:232
  40.8 0.7 collective-permute-start.5
  41.5 7.3 %collective-permute-done.1.refs_2_ = bf16[256,256]{1,0:T(8,128)(2,1)S(1)} collective-permute-done((bf16[256,256]{1,0:T(8,128)(2,1)S(1)}, bf16[256,256]{1,0:T(8,128)(2,1)S(1)}, u32[]{:S(2)}, u32[]{:S(2)}) %collective-permute-start.1) | collective-permute-done | bytes 131104 | tf_op jit(solution)/shard_map/ppermute | solution.py:232
  48.8 1.9 %collective-permute-start.2 = (bf16[256,256]{1,0:T(8,128)(2,1)S(1)}, bf16[256,256]{1,0:T(8,128)(2,1)S(1)}, u32[]{:S(2)}, u32[]{:S(2)}) collective-permute-start(bf16[256,256]{1,0:T(8,128)(2,1)S(1)} %collective-permute-done.1.refs_2_), channel_id=1, source_target_pairs={{128,192},{192,256},{256,320},{320,384},{384,448},{129,193},{193,2... | collective-permute-start | bytes 393224 | tf_op jit(solution)/shard_map/ppermute | solution.py:232
  50.9 0.7 collective-permute-start.6
  51.6 10.1 %collective-permute-done.2.refs_3_ = bf16[256,256]{1,0:T(8,128)(2,1)S(1)} collective-permute-done((bf16[256,256]{1,0:T(8,128)(2,1)S(1)}, bf16[256,256]{1,0:T(8,128)(2,1)S(1)}, u32[]{:S(2)}, u32[]{:S(2)}) %collective-permute-start.2) | collective-permute-done | bytes 131104 | tf_op jit(solution)/shard_map/ppermute | solution.py:232
  61.7 1.9 %collective-permute-start.3 = (bf16[256,256]{1,0:T(8,128)(2,1)S(1)}, bf16[256,256]{1,0:T(8,128)(2,1)S(1)}, u32[]{:S(2)}, u32[]{:S(2)}) collective-permute-start(bf16[256,256]{1,0:T(8,128)(2,1)S(1)} %collective-permute-done.2.refs_3_), channel_id=1, source_target_pairs={{192,256},{256,320},{320,384},{384,448},{193,257},{257,321},{321,3... | collective-permute-start | bytes 393224 | tf_op jit(solution)/shard_map/ppermute | solution.py:232
  63.7 0.7 fusion.9.pairs_ref
  64.3 6.4 %collective-permute-done.3.refs_4_ = bf16[256,256]{1,0:T(8,128)(2,1)S(1)} collective-permute-done((bf16[256,256]{1,0:T(8,128)(2,1)S(1)}, bf16[256,256]{1,0:T(8,128)(2,1)S(1)}, u32[]{:S(2)}, u32[]{:S(2)}) %collective-permute-start.3) | collective-permute-done | bytes 131104 | tf_op jit(solution)/shard_map/ppermute | solution.py:232
  70.7 15.1 %attend.1 = bf16[8,272,128]{2,1,0:T(8,128)(2,1)} custom-call(s32[512]{0:T(512)S(1)} %fusion.9.pairs_ref, s32[1]{0:T(128)} %bitcast.count_ref, bf16[8,256,128]{2,1,0:T(8,128)(2,1)S(1)} %all_to_all.20.q_ref, bf16[256,256]{1,0:T(8,128)(2,1)S(1)} %get-tuple-element.7.refs_0_, bf16[256,256]{1,0:T(8,128)(2,1)S(1)} %collective-permute-done.refs_1_, ...), custom_call_target="tpu_custom_call" | custom-call | tf_op jit(solution)/shard_map/attend/pallas_call | solution.py:138
  85.8 3.5 %all-to-all-start.1 = ((bf16[8,272,128]{2,1,0:T(8,128)(2,1)}), bf16[8,272,128]{2,1,0:T(8,128)(2,1)S(1)}, u32[]{:S(2)}, u32[]{:S(2)}) async-start(bf16[8,272,128]{2,1,0:T(8,128)(2,1)} %attend.1), calls=%async_computation.1 | async-start | bytes 1114112 | tf_op jit(solution)/shard_map/all_to_all | solution.py:243
  89.3 1.9 %collective-permute-start.7 = (bf16[4,128,2048]{2,1,0:T(8,128)(2,1)S(1)}, bf16[4,128,2048]{2,1,0:T(8,128)(2,1)}, u32[]{:S(2)}, u32[]{:S(2)}) collective-permute-start(bf16[4,128,2048]{2,1,0:T(8,128)(2,1)S(1)} %all-to-all-done.3), channel_id=1, source_target_pairs={{0,1},{1,0},{2,3},{3,2},{4,5},{5,4},{6,7},{7,6},{8,9},{9,8},{10,11... | collective-permute-start | bytes 6291464 | tf_op jit(solution)/shard_map/ppermute | solution.py:241
  91.2 5.3 %all-to-all-done.1.part_ref = bf16[8,272,128]{2,1,0:T(8,128)(2,1)S(1)} async-done(((bf16[8,272,128]{2,1,0:T(8,128)(2,1)}), bf16[8,272,128]{2,1,0:T(8,128)(2,1)S(1)}, u32[]{:S(2)}, u32[]{:S(2)}) %all-to-all-start.1) | async-done | bytes 557088 | tf_op jit(solution)/shard_map/all_to_all | solution.py:243
  96.5 0.9 merge.1
  97.4 3.4 %all-to-all-start.2 = ((bf16[8,32,128]{2,1,0:T(8,128)(2,1)}), bf16[8,32,128]{2,1,0:T(8,128)(2,1)S(1)}, u32[]{:S(2)}, u32[]{:S(2)}) async-start(bf16[8,32,128]{2,1,0:T(8,128)(2,1)} %bitcast.1), calls=%async_computation.2 | async-start | bytes 131072 | tf_op jit(solution)/shard_map/all_to_all | solution.py:246
  100.9 0.7 reshape.60
  101.6 4.8 %all-to-all-done.2 = bf16[8,32,128]{2,1,0:T(8,128)(2,1)S(1)} async-done(((bf16[8,32,128]{2,1,0:T(8,128)(2,1)}), bf16[8,32,128]{2,1,0:T(8,128)(2,1)S(1)}, u32[]{:S(2)}, u32[]{:S(2)}) %all-to-all-start.2) | async-done | bytes 65568 | tf_op jit(solution)/shard_map/all_to_all | solution.py:246
  106.3 0.5 convolution_bitcast_fusion.1
  106.8 2.7 %fusion.1 = bf16[32,2048]{1,0:T(8,128)(2,1)} fusion(f32[32,2048]{1,0:T(8,128)S(1)} %convolution_bitcast_fusion.1, bf16[4,128,2048]{2,1,0:T(8,128)(2,1)} %collective-permute-done.7, bf16[4,2,32,128]{3,2,1,0:T(8,128)(2,1)S(1)} %bitcast.25, s32[]{:T(128)S(6)} %select_n.50), kind=kOutput, calls=%fused_computation.3 | convolution fusion | flops 67239936 | bytes 2523140 | tf_op jit(solution)/shard_map/trc,tcn->rn/dot_general | solution.py:252
  (28 shorter events, 0.9 us)
Async XLA Ops:
  1.3 1.2 %copy-start = (bf16[256,2048]{1,0:T(8,128)(2,1)S(1)}, bf16[256,2048]{1,0:T(8,128)(2,1)}, u32[]{:S(2)}) copy-start(bf16[256,2048]{1,0:T(8,128)(2,1)} %x_ref.1) | copy-start | bytes 3145732
  2.5 1.0 copy-start.1
  3.6 1.0 copy-start.2
  4.6 1.0 copy-start.3
  5.7 15.4 %copy-start.4 = (bf16[128,2048]{1,0:T(8,128)(2,1)S(1)}, bf16[128,2048]{1,0:T(8,128)(2,1)}, u32[]{:S(2)}) copy-start(bf16[128,2048]{1,0:T(8,128)(2,1)} %param.10) | copy-start | bytes 1572868
  22.7 8.5 %copy-start.5 = (s32[256,16]{0,1:T(8,128)S(1)}, s32[256,16]{0,1:T(8,128)}, u32[]{:S(2)}) copy-start(s32[256,16]{0,1:T(8,128)} %param.11) | copy-start | bytes 49156
  22.7 63.1 %all-to-all-start.3 = ((bf16[4,128,2048]{2,1,0:T(8,128)(2,1)}), bf16[4,128,2048]{2,1,0:T(8,128)(2,1)S(1)}, u32[]{:S(2)}, u32[]{:S(2)}) async-start(bf16[4,128,2048]{2,1,0:T(8,128)(2,1)} %broadcast_in_dim.63), calls=%async_computation.3 | async-start | bytes 4194304 | tf_op jit(solution)/shard_map/all_to_all | solution.py:238
  27.1 13.7 %collective-permute-start.4 = (bf16[256,256]{1,0:T(8,128)(2,1)S(1)}, bf16[256,256]{1,0:T(8,128)(2,1)S(1)}, u32[]{:S(2)}, u32[]{:S(2)}) collective-permute-start(bf16[256,256]{1,0:T(8,128)(2,1)S(1)} %get-tuple-element.7.refs_0_), channel_id=1, source_target_pairs={{0,448},{64,0},{128,64},{1,449},{65,1},{129,65},{2,450},{66,2},{13... | collective-permute-start | bytes 393224 | tf_op jit(solution)/shard_map/ppermute | solution.py:235
  27.8 11.1 %collective-permute-start = (bf16[256,256]{1,0:T(8,128)(2,1)S(1)}, bf16[256,256]{1,0:T(8,128)(2,1)S(1)}, u32[]{:S(2)}, u32[]{:S(2)}) collective-permute-start(bf16[256,256]{1,0:T(8,128)(2,1)S(1)} %get-tuple-element.7.refs_0_), channel_id=1, source_target_pairs={{0,64},{64,128},{128,192},{192,256},{256,320},{320,384},{384,448},... | collective-permute-start | bytes 393224 | tf_op jit(solution)/shard_map/ppermute | solution.py:232
  38.9 9.9 %collective-permute-start.1 = (bf16[256,256]{1,0:T(8,128)(2,1)S(1)}, bf16[256,256]{1,0:T(8,128)(2,1)S(1)}, u32[]{:S(2)}, u32[]{:S(2)}) collective-permute-start(bf16[256,256]{1,0:T(8,128)(2,1)S(1)} %collective-permute-done.refs_1_), channel_id=1, source_target_pairs={{64,128},{128,192},{192,256},{256,320},{320,384},{384,448},{65,129... | collective-permute-start | bytes 393224 | tf_op jit(solution)/shard_map/ppermute | solution.py:232
  40.8 10.1 %collective-permute-start.5 = (bf16[256,256]{1,0:T(8,128)(2,1)S(1)}, bf16[256,256]{1,0:T(8,128)(2,1)S(1)}, u32[]{:S(2)}, u32[]{:S(2)}) collective-permute-start(bf16[256,256]{1,0:T(8,128)(2,1)S(1)} %collective-permute-done.4.refs_7_), channel_id=1, source_target_pairs={{448,384},{0,448},{64,0},{449,385},{1,449},{65,1},{450,386},{2,450... | collective-permute-start | bytes 393224 | tf_op jit(solution)/shard_map/ppermute | solution.py:235
  48.8 12.9 %collective-permute-start.2 = (bf16[256,256]{1,0:T(8,128)(2,1)S(1)}, bf16[256,256]{1,0:T(8,128)(2,1)S(1)}, u32[]{:S(2)}, u32[]{:S(2)}) collective-permute-start(bf16[256,256]{1,0:T(8,128)(2,1)S(1)} %collective-permute-done.1.refs_2_), channel_id=1, source_target_pairs={{128,192},{192,256},{256,320},{320,384},{384,448},{129,193},{193,2... | collective-permute-start | bytes 393224 | tf_op jit(solution)/shard_map/ppermute | solution.py:232
  50.9 13.4 %collective-permute-start.6 = (bf16[256,256]{1,0:T(8,128)(2,1)S(1)}, bf16[256,256]{1,0:T(8,128)(2,1)S(1)}, u32[]{:S(2)}, u32[]{:S(2)}) collective-permute-start(bf16[256,256]{1,0:T(8,128)(2,1)S(1)} %collective-permute-done.5.refs_6_), channel_id=1, source_target_pairs={{384,320},{448,384},{0,448},{385,321},{449,385},{1,449},{386,322},... | collective-permute-start | bytes 393224 | tf_op jit(solution)/shard_map/ppermute | solution.py:235
  61.7 9.0 %collective-permute-start.3 = (bf16[256,256]{1,0:T(8,128)(2,1)S(1)}, bf16[256,256]{1,0:T(8,128)(2,1)S(1)}, u32[]{:S(2)}, u32[]{:S(2)}) collective-permute-start(bf16[256,256]{1,0:T(8,128)(2,1)S(1)} %collective-permute-done.2.refs_3_), channel_id=1, source_target_pairs={{192,256},{256,320},{320,384},{384,448},{193,257},{257,321},{321,3... | collective-permute-start | bytes 393224 | tf_op jit(solution)/shard_map/ppermute | solution.py:232
  85.8 10.7 %all-to-all-start.1 = ((bf16[8,272,128]{2,1,0:T(8,128)(2,1)}), bf16[8,272,128]{2,1,0:T(8,128)(2,1)S(1)}, u32[]{:S(2)}, u32[]{:S(2)}) async-start(bf16[8,272,128]{2,1,0:T(8,128)(2,1)} %attend.1), calls=%async_computation.1 | async-start | bytes 1114112 | tf_op jit(solution)/shard_map/all_to_all | solution.py:243
  89.3 17.5 %collective-permute-start.7 = (bf16[4,128,2048]{2,1,0:T(8,128)(2,1)S(1)}, bf16[4,128,2048]{2,1,0:T(8,128)(2,1)}, u32[]{:S(2)}, u32[]{:S(2)}) collective-permute-start(bf16[4,128,2048]{2,1,0:T(8,128)(2,1)S(1)} %all-to-all-done.3), channel_id=1, source_target_pairs={{0,1},{1,0},{2,3},{3,2},{4,5},{5,4},{6,7},{7,6},{8,9},{9,8},{10,11... | collective-permute-start | bytes 6291464 | tf_op jit(solution)/shard_map/ppermute | solution.py:241
  97.4 8.9 %all-to-all-start.2 = ((bf16[8,32,128]{2,1,0:T(8,128)(2,1)}), bf16[8,32,128]{2,1,0:T(8,128)(2,1)S(1)}, u32[]{:S(2)}, u32[]{:S(2)}) async-start(bf16[8,32,128]{2,1,0:T(8,128)(2,1)} %bitcast.1), calls=%async_computation.2 | async-start | bytes 131072 | tf_op jit(solution)/shard_map/all_to_all | solution.py:246

commit v3 on v2

--- a/solution.py
+++ b/solution.py
@@ -27,8 +27,12 @@
 bf16 = jnp.bfloat16
 
 
-def project_kernel(x_ref, wq_ref, wk_ref, wv_ref, cos_ref, sin_ref, q_ref, kv_ref):
-    x = x_ref[...]
+def project_kernel(x_hbm, wq_hbm, wk_hbm, wv_hbm, cos_ref, sin_ref, q_ref, kv_ref, x_buf, w_buf, sems):
+    copies = [pltpu.make_async_copy(x_hbm, x_buf, sems.at[0])]
+    for i, w in enumerate((wk_hbm, wv_hbm, wq_hbm)):
+        copies.append(pltpu.make_async_copy(w, w_buf.at[i], sems.at[i + 1]))
+    for copy in copies:
+        copy.start()
     cos = cos_ref[...]
     sin = sin_ref[...]
     lane = lax.broadcasted_iota(jnp.int32, (ROWS, WIDTH), 1)
@@ -38,24 +42,37 @@
         partner = jnp.where(first, pltpu.roll(t, WIDTH - HEAD_DIM // 2, 1), pltpu.roll(t, HEAD_DIM // 2, 1))
         return t * cos + partner * sin
 
-    k = jnp.dot(x, wk_ref[...], preferred_element_type=f32)
+    copies[0].wait()
+    copies[1].wait()
+    x = x_buf[...]
+    k = jnp.dot(x, w_buf[0], preferred_element_type=f32)
     kv_ref[:, :WIDTH] = turned(k).astype(bf16)
-    v = jnp.dot(x, wv_ref[...], preferred_element_type=f32)
+    copies[2].wait()
+    v = jnp.dot(x, w_buf[1], preferred_element_type=f32)
     kv_ref[:, WIDTH:] = v.astype(bf16)
-    q = jnp.dot(x, wq_ref[...], preferred_element_type=f32)
+    copies[3].wait()
+    q = jnp.dot(x, w_buf[2], preferred_element_type=f32)
     q = (turned(q) * (HEAD_DIM**-0.5)).astype(bf16)
     for i in range(TEAM):
         q_ref[i] = q
 
 
 def project(x, wq, wk, wv, cos, sin):
+    hbm = pl.BlockSpec(memory_space=pltpu.HBM)
+    vmem = pl.BlockSpec(memory_space=pltpu.VMEM)
     return pl.pallas_call(
         project_kernel,
         out_shape=(
             jax.ShapeDtypeStruct((TEAM, ROWS, WIDTH), bf16),
             jax.ShapeDtypeStruct((ROWS, 2 * WIDTH), bf16),
         ),
-        compiler_params=pltpu.CompilerParams(vmem_limit_bytes=12 << 20),
+        in_specs=[hbm] * 4 + [vmem] * 2,
+        out_specs=(vmem, vmem),
+        scratch_shapes=[
+            pltpu.VMEM(x.shape, bf16),
+            pltpu.VMEM((3,) + wq.shape, bf16),
+            pltpu.SemaphoreType.DMA((4,)),
+        ],
         name="project",
     )(x, wq, wk, wv, cos, sin)
 
@@ -63,20 +80,24 @@
 def attend_kernel(pairs_ref, count_ref, q_ref, *refs):
     kv_refs = refs[:RING]
     out_ref = refs[RING]
-    qq, kbuf, vbuf, sbuf, mbuf, lbuf, acc, lse = refs[RING + 1 :]
+    qq, kbuf, vbuf, sbuf, mbuf, lbuf, acc = refs[RING + 1 :]
     lane = lax.broadcasted_iota(jnp.int32, (BLK, WIDTH), 1)
     left = lane < HEAD_DIM
+    even = (lane & (HEAD_DIM // 2)) == 0
     for s in range(RING):
         for b in range(PER):
             rows = pl.ds(b * BLK, BLK)
             kbuf[s * PER + b] = kv_refs[s][rows, :WIDTH]
             vbuf[s * PER + b] = kv_refs[s][rows, WIDTH:]
-    zero = jnp.zeros((BLK, WIDTH), bf16)
+    half = BLK // 2
+    left_half = left[:half]
+    zero = jnp.zeros((half, WIDTH), bf16)
     for i in range(TEAM):
         for b in range(PER):
-            q = q_ref[i, pl.ds(b * BLK, BLK), :]
-            qq[i * PER + b, :BLK, :] = jnp.where(left, q, zero)
-            qq[i * PER + b, BLK:, :] = jnp.where(left, zero, q)
+            for h in range(2):
+                q = q_ref[i, pl.ds(b * BLK + h * half, half), :]
+                qq[i * PER + b, pl.ds(h * BLK, half), :] = jnp.where(left_half, q, zero)
+                qq[i * PER + b, pl.ds(h * BLK + half, half), :] = jnp.where(left_half, zero, q)
     qq[QB] = jnp.zeros((2 * BLK, WIDTH), bf16)
     mbuf[...] = jnp.full(mbuf.shape, masked_score, f32)
     lbuf[...] = jnp.zeros(lbuf.shape, f32)
@@ -113,23 +134,40 @@
             ot = lax.dot_general(
                 vbuf[ki], pb, (((0,), (0,)), ((), ())), preferred_element_type=f32
             )
-            acc[qi] = acc[qi] + jnp.where(left, ot[:HEAD_DIM], ot[HEAD_DIM:])
+            acc[qi] = acc[qi] + jnp.where(even, ot[:HEAD_DIM], ot[HEAD_DIM:])
         return carry
 
     lax.fori_loop(0, trips, weigh, 0)
-    for i in range(QB):
+    left_row = left[:1]
+
+    def finished(i):
         total = jnp.sum(lbuf[i], axis=0, keepdims=True)
         some = total > 0.0
         safe = jnp.where(some, total, 1.0)
-        out_ref[i // PER, pl.ds((i % PER) * BLK, BLK), :] = (acc[i] * (1.0 / safe)).astype(bf16)
-        lse[pl.ds(i, 1), :] = jnp.where(some, mbuf[i, :1, :] + jnp.log(safe), masked_score)
+        return acc[i] * (1.0 / safe), jnp.where(some, mbuf[i, :1, :] + jnp.log(safe), masked_score)
+
     for i in range(TEAM):
-        value = lse[pl.ds(i * PER, PER), :]
-        hi = value.astype(bf16).astype(f32)
-        rest = value - hi
-        mid = rest.astype(bf16).astype(f32)
-        parts = jnp.concatenate([hi, mid, rest - mid, jnp.zeros((PER, WIDTH), f32)], axis=0)
-        out_ref[i, pl.ds(ROWS, STATS), :] = parts.astype(bf16)
+        logs = []
+        for pair in range(PER // 2):
+            one, one_log = finished(i * PER + 2 * pair)
+            two, two_log = finished(i * PER + 2 * pair + 1)
+            rows = pl.ds(pair * BLK, BLK)
+            out_ref[2 * i, rows, :] = jnp.where(left, one, pltpu.roll(two, BLK, 1)).astype(bf16)
+            out_ref[2 * i + 1, rows, :] = jnp.where(left, pltpu.roll(one, BLK, 1), two).astype(bf16)
+            logs.append(
+                (
+                    jnp.where(left_row, one_log, pltpu.roll(two_log, BLK, 1)),
+                    jnp.where(left_row, pltpu.roll(one_log, BLK, 1), two_log),
+                )
+            )
+        for c in range(2):
+            value = jnp.concatenate([logs[0][c], logs[1][c]], axis=0)
+            hi = value.astype(bf16).astype(f32)
+            rest = value - hi
+            mid = rest.astype(bf16).astype(f32)
+            empty = jnp.zeros((STATS - 6, WIDTH), f32)
+            stats = jnp.concatenate([hi, mid, rest - mid, empty], axis=0)
+            out_ref[2 * i + c, pl.ds(2 * BLK, STATS), :] = stats.astype(bf16)
 
 
 def attend(pairs, count, q, kvs):
@@ -137,7 +175,7 @@
     vmem = pl.BlockSpec(memory_space=pltpu.VMEM)
     return pl.pallas_call(
         attend_kernel,
-        out_shape=jax.ShapeDtypeStruct((TEAM, ROWS + STATS, WIDTH), bf16),
+        out_shape=jax.ShapeDtypeStruct((2 * TEAM, 2 * BLK + STATS, WIDTH), bf16),
         in_specs=[smem, smem] + [vmem] * (1 + RING),
         out_specs=vmem,
         scratch_shapes=[
@@ -148,43 +186,56 @@
             pltpu.VMEM((QB + 1, 8, WIDTH), f32),
             pltpu.VMEM((QB + 1, 8, WIDTH), f32),
             pltpu.VMEM((QB + 1, BLK, WIDTH), f32),
-            pltpu.VMEM((QB, WIDTH), f32),
         ],
         compiler_params=pltpu.CompilerParams(vmem_limit_bytes=28 << 20),
         name="attend",
     )(pairs, count, q, *kvs)
 
 
-def merge_kernel(part_ref, att_ref, log_ref):
-    values = []
-    for i in range(TEAM):
-        st = part_ref[i, pl.ds(ROWS, STATS), :].astype(f32)
-        values.append(st[:PER] + st[PER : 2 * PER] + st[2 * PER : 3 * PER])
-    top = functools.reduce(jnp.maximum, values)
-    weights = [jnp.exp(v - top) for v in values]
-    total = functools.reduce(jnp.add, weights)
-    log_ref[...] = top + jnp.log(total)
-    inverse = 1.0 / total
-    weights = [w * inverse for w in weights]
-    for b in range(PER):
-        rows = pl.ds(b * BLK, BLK)
-        att = jnp.zeros((BLK, WIDTH), f32)
+def merge_kernel(core_ref, part_ref, same_ref, other_ref, out_ref, log_ref, att):
+    half = BLK // 2
+    for c in range(2):
+        values = []
         for i in range(TEAM):
-            att = att + part_ref[i, rows, :].astype(f32) * weights[i][b : b + 1, :]
-        turned = att.T
-        att_ref[rows, :] = jnp.concatenate([turned[:BLK], turned[BLK:]], axis=1).astype(bf16)
-
-
-def merge(parts):
+            st = part_ref[2 * i + c, pl.ds(2 * BLK, STATS), :].astype(f32)
+            values.append(st[:2] + st[2:4] + st[4:6])
+        top = functools.reduce(jnp.maximum, values)
+        weights = [jnp.exp(v - top) for v in values]
+        total = functools.reduce(jnp.add, weights)
+        log_ref[pl.ds(2 * c, 2), :] = top + jnp.log(total)
+        inverse = 1.0 / total
+        weights = [w * inverse for w in weights]
+        for pair in range(PER // 2):
+            mixed = jnp.zeros((BLK, WIDTH), f32)
+            for i in range(TEAM):
+                part = part_ref[2 * i + c, pl.ds(pair * BLK, BLK), :].astype(f32)
+                mixed = mixed + part * weights[i][pair : pair + 1, :]
+            turned = mixed.T
+            for b in range(2):
+                heads = [turned[b * BLK + h * half : b * BLK + (h + 1) * half] for h in range(2)]
+                rows = pl.ds((2 * pair + b) * half, half)
+                att[c, rows, :] = jnp.concatenate(heads, axis=1).astype(bf16)
+    core = core_ref[0]
+    y = jnp.dot(att[core], same_ref[...], preferred_element_type=f32)
+    y = y + jnp.dot(att[1 - core], other_ref[...], preferred_element_type=f32)
+    out_ref[...] = y.astype(bf16).reshape(out_ref.shape)
+
+
+def merge(core, parts, w_same, w_other):
+    smem = pl.BlockSpec(memory_space=pltpu.SMEM)
+    vmem = pl.BlockSpec(memory_space=pltpu.VMEM)
     return pl.pallas_call(
         merge_kernel,
         out_shape=(
-            jax.ShapeDtypeStruct((ROWS, WIDTH), bf16),
-            jax.ShapeDtypeStruct((PER, WIDTH), f32),
+            jax.ShapeDtypeStruct((PER, BLK // 2, w_same.shape[1]), bf16),
+            jax.ShapeDtypeStruct((4, WIDTH), f32),
         ),
-        compiler_params=pltpu.CompilerParams(vmem_limit_bytes=4 << 20),
+        in_specs=[smem, vmem, vmem, vmem],
+        out_specs=(vmem, vmem),
+        scratch_shapes=[pltpu.VMEM((2, 2 * BLK, WIDTH), bf16)],
+        compiler_params=pltpu.CompilerParams(vmem_limit_bytes=12 << 20),
         name="merge",
-    )(parts)
+    )(core.reshape(1), parts, w_same, w_other)
 
 
 def pair_list(chosen, zh, mine):
@@ -235,21 +286,22 @@
             down = lax.ppermute(down, "zh", down_pairs(s))
             slots[RING - s] = down
     q_team = lax.all_to_all(q8, ("zl", "y"), 0, 0, tiled=True)
-    w_same = lax.all_to_all(
-        jnp.broadcast_to(w_out[None], (4,) + w_out.shape), "x", 0, 0, tiled=True
+    core = lax.axis_index("c")
+    w_other = lax.ppermute(w_out, "c", [(0, 1), (1, 0)])
+    parts = attend(pairs, count, q_team, slots)
+    parts = lax.all_to_all(parts, ("zl", "y", "c"), 0, 0, tiled=True)
+    partial, logs = merge(core, parts, w_out, w_other)
+    tiles = lax.all_to_all(partial, "x", 0, 0, tiled=True)
+    logs = logs.reshape(2, 2, 2, 2, BLK // 2)
+    mine_logs = lax.dynamic_index_in_dim(logs, core, 0, keepdims=False)
+    other_logs = lax.ppermute(
+        lax.dynamic_index_in_dim(logs, 1 - core, 0, keepdims=False), "c", [(0, 1), (1, 0)]
     )
-    w_other = lax.ppermute(w_same, "c", [(0, 1), (1, 0)])
-    parts = attend(pairs, count, q_team, slots)
-    parts = lax.all_to_all(parts, ("zl", "y"), 0, 0, tiled=True)
-    attended, logs = merge(parts)
-    log_sums = jnp.transpose(logs.reshape(PER, 2, BLK), (1, 0, 2)).reshape(2, ROWS)
-    rows = lax.all_to_all(attended.reshape(8, ROWS // 8, WIDTH), ("x", "c"), 0, 0, tiled=True)
-    rows = rows.reshape(4, 2, ROWS // 8, WIDTH)
-    core = lax.axis_index("c")
-    rows_same = lax.dynamic_index_in_dim(rows, core, 1, keepdims=False)
-    rows_other = lax.dynamic_index_in_dim(rows, 1 - core, 1, keepdims=False)
-    output = jnp.einsum("trc,tcn->rn", rows_same, w_same, preferred_element_type=f32)
-    output = output + jnp.einsum("trc,tcn->rn", rows_other, w_other, preferred_element_type=f32)
+    ordered = jnp.where(
+        core == 0, jnp.stack([mine_logs, other_logs]), jnp.stack([other_logs, mine_logs])
+    )
+    log_sums = jnp.transpose(ordered, (3, 1, 2, 0, 4)).reshape(2, ROWS)
+    output = jnp.sum(tiles.astype(f32), axis=0)
     return (output.astype(bf16), log_sums)
 
 

time: 110 us -> 101 us (0.918)
  blocking collectives: 14.4 us -> 0 us
  local copies, waits for them, and re-layouts: 7.12 us -> 1.19 us
  starting transfers between devices: 24.3 us -> 29.4 us
  Pallas kernels: 17.1 us -> 21.3 us
  matrix products: 3.2 us -> 0 us
  waiting for transfers between devices: 39.7 us -> 42.8 us
  other arithmetic: 2.3 us -> 3.76 us
    all_to_all x1 -> x0, blocking collectives: 14.4 us -> none  [local(): q_team = lax.all_to_all(q8, ('zl', 'y'), 0, 0, tiled=True)]
    unnamed x12 -> x6, local copies, waits for them, and re-layouts: 4.35 us -> 0.01 us
    pallas_call x1, Pallas kernels: 1.04 us -> 4.57 us  [project(): pl.pallas_call(project_kernel, out_shape=(jax.ShapeDtypeStruct((TEAM, ROW...]
    all_to_all x3, starting transfers between devices: 11.3 us -> 14.5 us  [the longest x1 6.07 us: local(): q_team = lax.all_to_all(q8, ('zl', 'y'), 0, 0, tiled=True)]
    dot_general x2 -> x0, matrix products: 3.2 us -> none  [the longest x1 2.73 us: local(): jnp.einsum('trc,tcn->rn', rows_other, w_other, preferred_element_type=f32)]
    ppermute x1 -> x2, waiting for transfers between devices: 0.01 us -> 3 us  [the longest x1 1.87 us: local(): w_other = lax.ppermute(w_out, 'c', [(0, 1), (1, 0)])]
    all_to_all x3, waiting for transfers between devices: 10.1 us -> 12.1 us  [the longest x1 6.17 us: local(): parts = lax.all_to_all(parts, ('zl', 'y', 'c'), 0, 0, tiled=True)]
    ppermute x4, waiting for transfers between devices: 29.6 us -> 27.7 us  [local(): up = lax.ppermute(up, 'zh', up_pairs(s))]
  transfers between devices with their start and end apart: 11 -> 12, of which waited for: 6 -> 8; matrix products, arithmetic and copies ran while one was open for 3% -> 3% of each run, Pallas kernels for 15% -> 0%
where the time goes in v3:
time: 101 us; the launch traced here: 100 us
  waiting for transfers between devices  42.8 us (42%)
  starting transfers between devices  29.4 us (29%)
  Pallas kernels  21.3 us (21%)
  other arithmetic  3.76 us (4%)
  between operations  1.53 us (2%)
  local copies, waits for them, and re-layouts  1.19 us (1%)
    ppermute x4, waiting for transfers between devices, local(): up = lax.ppermute(up, 'zh', up_pairs(s))  27.7 us
    pallas_call x1, Pallas kernels, attend(): pl.pallas_call(attend_kernel, out_shape=jax.ShapeDtypeStruct((2 * TEAM, 2...  15.2 us
    ppermute x4, starting transfers between devices, local(): up = lax.ppermute(up, 'zh', up_pairs(s))  9.1 us
    all_to_all x1, waiting for transfers between devices, local(): parts = lax.all_to_all(parts, ('zl', 'y', 'c'), 0, 0, tiled=True)  6.17 us
    all_to_all x1, starting transfers between devices, local(): q_team = lax.all_to_all(q8, ('zl', 'y'), 0, 0, tiled=True)  6.07 us
    all_to_all x1, waiting for transfers between devices, local(): tiles = lax.all_to_all(partial, 'x', 0, 0, tiled=True)  5.93 us
    all_to_all x1, starting transfers between devices, local(): tiles = lax.all_to_all(partial, 'x', 0, 0, tiled=True)  4.8 us
    pallas_call x1, Pallas kernels, project(): pl.pallas_call(project_kernel, out_shape=(jax.ShapeDtypeStruct((TEAM, ROW...  4.57 us
  transfers between devices with their start and end apart: 12, of which 8 were waited for; matrix products, arithmetic and copies ran while one was open for 3% of the time, Pallas kernels for 0%

profile of v3, /device:TPU:288, one launch (start us, length us, event | category | flops | bytes accessed | tf_op | source)
XLA Modules:
  0.0 100.0 jit_solution(12106357927788045409)
XLA Ops:
  0.8 1.2 %fusion.1 = (f32[256,128]{1,0:T(8,128)}, f32[256,128]{1,0:T(8,128)}) fusion(f32[128]{0:T(128)S(1)} %compare_select_fusion, f32[128]{0:T(128)S(1)} %mul.61, f32[256]{0:T(256)S(1)} %add_convert_fusion), kind=kLoop, calls=%fused_computation.7 | loop fusion | flops 65536 | bytes 264192 | tf_op jit(solution)/shard_map/mul | solution.py:277
  2.0 4.6 %project.1 = (bf16[8,256,128]{2,1,0:T(8,128)(2,1)}, bf16[256,256]{1,0:T(8,128)(2,1)}) custom-call(bf16[256,2048]{1,0:T(8,128)(2,1)} %x_hbm.1, bf16[2048,128]{1,0:T(8,128)(2,1)} %wq_hbm.1, bf16[2048,128]{1,0:T(8,128)(2,1)} %wk_hbm.1, bf16[2048,128]{1,0:T(8,128)(2,1)} %wv_hbm.1, f32[256,128]{1,0:T(8,128)} %get-tuple-element.16.cos_ref, ...), custom_call_target="tpu_custom_call" | custom-call | tf_op jit(solution)/shard_map/project/pallas_call | solution.py:63
  6.6 6.1 %all-to-all-start = ((bf16[8,256,128]{2,1,0:T(8,128)(2,1)}), bf16[8,256,128]{2,1,0:T(8,128)(2,1)S(1)}, u32[]{:S(2)}, u32[]{:S(2)}) async-start(bf16[8,256,128]{2,1,0:T(8,128)(2,1)} %get-tuple-element.6), calls=%async_computation | async-start | bytes 1048576 | tf_op jit(solution)/shard_map/all_to_all | solution.py:288
  12.7 3.4 %collective-permute-start = (bf16[256,256]{1,0:T(8,128)(2,1)S(1)}, bf16[256,256]{1,0:T(8,128)(2,1)S(1)}, u32[]{:S(2)}, u32[]{:S(2)}) collective-permute-start(bf16[256,256]{1,0:T(8,128)(2,1)S(1)} %copy-done.1), channel_id=1, source_target_pairs={{0,64},{64,128},{128,192},{192,256},{256,320},{320,384},{384,448},... | collective-permute-start | bytes 393224 | tf_op jit(solution)/shard_map/ppermute | solution.py:283
  16.1 0.7 collective-permute-start.4
  16.8 0.7 convert_reduce_fusion.1
  18.2 0.1 copy.12
  18.2 0.1 reshape.52
  18.5 0.2 convert_reduce_fusion
  18.7 3.9 %collective-permute-done.refs_1_ = bf16[256,256]{1,0:T(8,128)(2,1)S(1)} collective-permute-done((bf16[256,256]{1,0:T(8,128)(2,1)S(1)}, bf16[256,256]{1,0:T(8,128)(2,1)S(1)}, u32[]{:S(2)}, u32[]{:S(2)}) %collective-permute-start) | collective-permute-done | bytes 131104 | tf_op jit(solution)/shard_map/ppermute | solution.py:283
  22.5 1.9 %collective-permute-start.1 = (bf16[256,256]{1,0:T(8,128)(2,1)S(1)}, bf16[256,256]{1,0:T(8,128)(2,1)S(1)}, u32[]{:S(2)}, u32[]{:S(2)}) collective-permute-start(bf16[256,256]{1,0:T(8,128)(2,1)S(1)} %collective-permute-done.refs_1_), channel_id=1, source_target_pairs={{64,128},{128,192},{192,256},{256,320},{320,384},{384,448},{65,129... | collective-permute-start | bytes 393224 | tf_op jit(solution)/shard_map/ppermute | solution.py:283
  24.5 0.7 collective-permute-start.5
  25.2 8.4 %collective-permute-done.1.refs_2_ = bf16[256,256]{1,0:T(8,128)(2,1)S(1)} collective-permute-done((bf16[256,256]{1,0:T(8,128)(2,1)S(1)}, bf16[256,256]{1,0:T(8,128)(2,1)S(1)}, u32[]{:S(2)}, u32[]{:S(2)}) %collective-permute-start.1) | collective-permute-done | bytes 131104 | tf_op jit(solution)/shard_map/ppermute | solution.py:283
  33.5 1.9 %collective-permute-start.2 = (bf16[256,256]{1,0:T(8,128)(2,1)S(1)}, bf16[256,256]{1,0:T(8,128)(2,1)S(1)}, u32[]{:S(2)}, u32[]{:S(2)}) collective-permute-start(bf16[256,256]{1,0:T(8,128)(2,1)S(1)} %collective-permute-done.1.refs_2_), channel_id=1, source_target_pairs={{128,192},{192,256},{256,320},{320,384},{384,448},{129,193},{193,2... | collective-permute-start | bytes 393224 | tf_op jit(solution)/shard_map/ppermute | solution.py:283
  35.5 0.2 select_reduce_fusion
  35.7 0.7 collective-permute-start.6
  36.4 7.8 %collective-permute-done.2.refs_3_ = bf16[256,256]{1,0:T(8,128)(2,1)S(1)} collective-permute-done((bf16[256,256]{1,0:T(8,128)(2,1)S(1)}, bf16[256,256]{1,0:T(8,128)(2,1)S(1)}, u32[]{:S(2)}, u32[]{:S(2)}) %collective-permute-start.2) | collective-permute-done | bytes 131104 | tf_op jit(solution)/shard_map/ppermute | solution.py:283
  44.2 1.9 %collective-permute-start.3 = (bf16[256,256]{1,0:T(8,128)(2,1)S(1)}, bf16[256,256]{1,0:T(8,128)(2,1)S(1)}, u32[]{:S(2)}, u32[]{:S(2)}) collective-permute-start(bf16[256,256]{1,0:T(8,128)(2,1)S(1)} %collective-permute-done.2.refs_3_), channel_id=1, source_target_pairs={{192,256},{256,320},{320,384},{384,448},{193,257},{257,321},{321,3... | collective-permute-start | bytes 393224 | tf_op jit(solution)/shard_map/ppermute | solution.py:283
  46.1 0.7 fusion.4.pairs_ref
  46.7 7.6 %collective-permute-done.3.refs_4_ = bf16[256,256]{1,0:T(8,128)(2,1)S(1)} collective-permute-done((bf16[256,256]{1,0:T(8,128)(2,1)S(1)}, bf16[256,256]{1,0:T(8,128)(2,1)S(1)}, u32[]{:S(2)}, u32[]{:S(2)}) %collective-permute-start.3) | collective-permute-done | bytes 131104 | tf_op jit(solution)/shard_map/ppermute | solution.py:283
  54.4 15.2 %attend.1 = bf16[16,144,128]{2,1,0:T(8,128)(2,1)} custom-call(s32[512]{0:T(512)S(1)} %fusion.4.pairs_ref, s32[1]{0:T(128)} %bitcast.1.count_ref, bf16[8,256,128]{2,1,0:T(8,128)(2,1)S(1)} %all-to-all-done.q_ref, bf16[256,256]{1,0:T(8,128)(2,1)S(1)} %copy-done.1, bf16[256,256]{1,0:T(8,128)(2,1)S(1)} %collective-permute-done.refs_1_, ...), custom_call_target="tpu_custom_call" | custom-call | tf_op jit(solution)/shard_map/attend/pallas_call | solution.py:176
  69.6 3.6 %all-to-all-start.1 = ((bf16[16,144,128]{2,1,0:T(8,128)(2,1)}), bf16[16,144,128]{2,1,0:T(8,128)(2,1)S(1)}, u32[]{:S(2)}, u32[]{:S(2)}) async-start(bf16[16,144,128]{2,1,0:T(8,128)(2,1)} %attend.1), calls=%async_computation.1 | async-start | bytes 1179648 | tf_op jit(solution)/shard_map/all_to_all | solution.py:292
  73.2 1.9 %collective-permute-start.7 = (bf16[128,2048]{1,0:T(8,128)(2,1)S(1)}, bf16[128,2048]{1,0:T(8,128)(2,1)S(1)}, u32[]{:S(2)}, u32[]{:S(2)}) collective-permute-start(bf16[128,2048]{1,0:T(8,128)(2,1)S(1)} %copy-done), channel_id=1, source_target_pairs={{0,1},{1,0},{2,3},{3,2},{4,5},{5,4},{6,7},{7,6},{8,9},{9,8},{10,11... | collective-permute-start | bytes 1572872 | tf_op jit(solution)/shard_map/ppermute | solution.py:290
  75.1 1.9 %collective-permute-done.7.other_ref = bf16[128,2048]{1,0:T(8,128)(2,1)S(1)} collective-permute-done((bf16[128,2048]{1,0:T(8,128)(2,1)S(1)}, bf16[128,2048]{1,0:T(8,128)(2,1)S(1)}, u32[]{:S(2)}, u32[]{:S(2)}) %collective-permute-start.7) | collective-permute-done | bytes 524320 | tf_op jit(solution)/shard_map/ppermute | solution.py:290
  77.0 6.2 %all-to-all-done.1.part_ref = bf16[16,144,128]{2,1,0:T(8,128)(2,1)S(1)} async-done(((bf16[16,144,128]{2,1,0:T(8,128)(2,1)}), bf16[16,144,128]{2,1,0:T(8,128)(2,1)S(1)}, u32[]{:S(2)}, u32[]{:S(2)}) %all-to-all-start.1) | async-done | bytes 589856 | tf_op jit(solution)/shard_map/all_to_all | solution.py:292
  83.2 1.5 %merge.1 = (bf16[4,32,2048]{2,1,0:T(8,128)(2,1)}, f32[4,128]{1,0:T(4,128)S(1)}) custom-call(s32[1]{0:T(128)} %bitcast.core_ref, bf16[16,144,128]{2,1,0:T(8,128)(2,1)S(1)} %all-to-all-done.1.part_ref, bf16[128,2048]{1,0:T(8,128)(2,1)S(1)} %copy-done, bf16[128,2048]{1,0:T(8,128)(2,1)S(1)} %collective-permute-done.7.other_ref), custom_call_target="tpu_custom_call" | custom-call | tf_op jit(solution)/shard_map/merge/pallas_call | solution.py:227
  84.7 4.8 %all-to-all-start.2 = ((bf16[4,32,2048]{2,1,0:T(8,128)(2,1)}), bf16[4,32,2048]{2,1,0:T(8,128)(2,1)S(1)}, u32[]{:S(2)}, u32[]{:S(2)}) async-start(bf16[4,32,2048]{2,1,0:T(8,128)(2,1)} %get-tuple-element.8), calls=%async_computation.2 | async-start | bytes 1048576 | tf_op jit(solution)/shard_map/all_to_all | solution.py:294
  89.6 1.9 %collective-permute-start.8 = (f32[2,2,2,32]{3,2,1,0:T(2,128)S(1)}, f32[2,2,2,32]{3,2,1,0:T(2,128)S(1)}, u32[]{:S(2)}, u32[]{:S(2)}) collective-permute-start(f32[2,2,2,32]{3,2,1,0:T(2,128)S(1)} %get-tuple-element.14), channel_id=1, source_target_pairs={{0,1},{1,0},{2,3},{3,2},{4,5},{5,4},{6,7},{7,6},{8,9},{9,8},{10,11... | collective-permute-start | bytes 3080 | tf_op jit(solution)/shard_map/ppermute | solution.py:297
  91.5 1.1 %collective-permute-done.8 = f32[2,2,2,32]{3,2,1,0:T(2,128)S(1)} collective-permute-done((f32[2,2,2,32]{3,2,1,0:T(2,128)S(1)}, f32[2,2,2,32]{3,2,1,0:T(2,128)S(1)}, u32[]{:S(2)}, u32[]{:S(2)}) %collective-permute-start.8) | collective-permute-done | bytes 1056 | tf_op jit(solution)/shard_map/ppermute | solution.py:297
  92.6 0.7 reshape.55
  93.3 5.9 %all-to-all-done.2 = bf16[4,32,2048]{2,1,0:T(8,128)(2,1)S(1)} async-done(((bf16[4,32,2048]{2,1,0:T(8,128)(2,1)}), bf16[4,32,2048]{2,1,0:T(8,128)(2,1)S(1)}, u32[]{:S(2)}, u32[]{:S(2)}) %all-to-all-start.2) | async-done | bytes 524320 | tf_op jit(solution)/shard_map/all_to_all | solution.py:294
  99.2 0.7 reduce_sum.42
  (23 shorter events, 0.4 us)
Async XLA Ops:
  6.6 6.1 %copy-start.1 = (bf16[256,256]{1,0:T(8,128)(2,1)S(1)}, bf16[256,256]{1,0:T(8,128)(2,1)}, u32[]{:S(2)}) copy-start(bf16[256,256]{1,0:T(8,128)(2,1)} %get-tuple-element.7.refs_0_) | copy-start | bytes 393220
  6.6 10.2 %copy-start.2 = (s32[256,16]{0,1:T(8,128)S(1)}, s32[256,16]{0,1:T(8,128)}, u32[]{:S(2)}) copy-start(s32[256,16]{0,1:T(8,128)} %param.11) | copy-start | bytes 49156
  6.6 47.7 %all-to-all-start = ((bf16[8,256,128]{2,1,0:T(8,128)(2,1)}), bf16[8,256,128]{2,1,0:T(8,128)(2,1)S(1)}, u32[]{:S(2)}, u32[]{:S(2)}) async-start(bf16[8,256,128]{2,1,0:T(8,128)(2,1)} %get-tuple-element.6), calls=%async_computation | async-start | bytes 1048576 | tf_op jit(solution)/shard_map/all_to_all | solution.py:288
  12.7 9.8 %collective-permute-start = (bf16[256,256]{1,0:T(8,128)(2,1)S(1)}, bf16[256,256]{1,0:T(8,128)(2,1)S(1)}, u32[]{:S(2)}, u32[]{:S(2)}) collective-permute-start(bf16[256,256]{1,0:T(8,128)(2,1)S(1)} %copy-done.1), channel_id=1, source_target_pairs={{0,64},{64,128},{128,192},{192,256},{256,320},{320,384},{384,448},... | collective-permute-start | bytes 393224 | tf_op jit(solution)/shard_map/ppermute | solution.py:283
  16.1 8.4 %collective-permute-start.4 = (bf16[256,256]{1,0:T(8,128)(2,1)S(1)}, bf16[256,256]{1,0:T(8,128)(2,1)S(1)}, u32[]{:S(2)}, u32[]{:S(2)}) collective-permute-start(bf16[256,256]{1,0:T(8,128)(2,1)S(1)} %copy-done.1), channel_id=1, source_target_pairs={{0,448},{64,0},{128,64},{1,449},{65,1},{129,65},{2,450},{66,2},{13... | collective-permute-start | bytes 393224 | tf_op jit(solution)/shard_map/ppermute | solution.py:286
  22.5 11.0 %collective-permute-start.1 = (bf16[256,256]{1,0:T(8,128)(2,1)S(1)}, bf16[256,256]{1,0:T(8,128)(2,1)S(1)}, u32[]{:S(2)}, u32[]{:S(2)}) collective-permute-start(bf16[256,256]{1,0:T(8,128)(2,1)S(1)} %collective-permute-done.refs_1_), channel_id=1, source_target_pairs={{64,128},{128,192},{192,256},{256,320},{320,384},{384,448},{65,129... | collective-permute-start | bytes 393224 | tf_op jit(solution)/shard_map/ppermute | solution.py:283
  24.5 11.2 %collective-permute-start.5 = (bf16[256,256]{1,0:T(8,128)(2,1)S(1)}, bf16[256,256]{1,0:T(8,128)(2,1)S(1)}, u32[]{:S(2)}, u32[]{:S(2)}) collective-permute-start(bf16[256,256]{1,0:T(8,128)(2,1)S(1)} %collective-permute-done.4.refs_7_), channel_id=1, source_target_pairs={{448,384},{0,448},{64,0},{449,385},{1,449},{65,1},{450,386},{2,450... | collective-permute-start | bytes 393224 | tf_op jit(solution)/shard_map/ppermute | solution.py:286
  33.5 10.6 %collective-permute-start.2 = (bf16[256,256]{1,0:T(8,128)(2,1)S(1)}, bf16[256,256]{1,0:T(8,128)(2,1)S(1)}, u32[]{:S(2)}, u32[]{:S(2)}) collective-permute-start(bf16[256,256]{1,0:T(8,128)(2,1)S(1)} %collective-permute-done.1.refs_2_), channel_id=1, source_target_pairs={{128,192},{192,256},{256,320},{320,384},{384,448},{129,193},{193,2... | collective-permute-start | bytes 393224 | tf_op jit(solution)/shard_map/ppermute | solution.py:283
  35.7 11.1 %collective-permute-start.6 = (bf16[256,256]{1,0:T(8,128)(2,1)S(1)}, bf16[256,256]{1,0:T(8,128)(2,1)S(1)}, u32[]{:S(2)}, u32[]{:S(2)}) collective-permute-start(bf16[256,256]{1,0:T(8,128)(2,1)S(1)} %collective-permute-done.5.refs_6_), channel_id=1, source_target_pairs={{384,320},{448,384},{0,448},{385,321},{449,385},{1,449},{386,322},... | collective-permute-start | bytes 393224 | tf_op jit(solution)/shard_map/ppermute | solution.py:286
  44.2 10.2 %collective-permute-start.3 = (bf16[256,256]{1,0:T(8,128)(2,1)S(1)}, bf16[256,256]{1,0:T(8,128)(2,1)S(1)}, u32[]{:S(2)}, u32[]{:S(2)}) collective-permute-start(bf16[256,256]{1,0:T(8,128)(2,1)S(1)} %collective-permute-done.2.refs_3_), channel_id=1, source_target_pairs={{192,256},{256,320},{320,384},{384,448},{193,257},{257,321},{321,3... | collective-permute-start | bytes 393224 | tf_op jit(solution)/shard_map/ppermute | solution.py:283
  69.6 3.6 %copy-start = (bf16[128,2048]{1,0:T(8,128)(2,1)S(1)}, bf16[128,2048]{1,0:T(8,128)(2,1)}, u32[]{:S(2)}) copy-start(bf16[128,2048]{1,0:T(8,128)(2,1)} %same_ref.1) | copy-start | bytes 1572868
  69.6 13.6 %all-to-all-start.1 = ((bf16[16,144,128]{2,1,0:T(8,128)(2,1)}), bf16[16,144,128]{2,1,0:T(8,128)(2,1)S(1)}, u32[]{:S(2)}, u32[]{:S(2)}) async-start(bf16[16,144,128]{2,1,0:T(8,128)(2,1)} %attend.1), calls=%async_computation.1 | async-start | bytes 1179648 | tf_op jit(solution)/shard_map/all_to_all | solution.py:292
  73.2 3.8 %collective-permute-start.7 = (bf16[128,2048]{1,0:T(8,128)(2,1)S(1)}, bf16[128,2048]{1,0:T(8,128)(2,1)S(1)}, u32[]{:S(2)}, u32[]{:S(2)}) collective-permute-start(bf16[128,2048]{1,0:T(8,128)(2,1)S(1)} %copy-done), channel_id=1, source_target_pairs={{0,1},{1,0},{2,3},{3,2},{4,5},{5,4},{6,7},{7,6},{8,9},{9,8},{10,11... | collective-permute-start | bytes 1572872 | tf_op jit(solution)/shard_map/ppermute | solution.py:290
  84.7 14.6 %all-to-all-start.2 = ((bf16[4,32,2048]{2,1,0:T(8,128)(2,1)}), bf16[4,32,2048]{2,1,0:T(8,128)(2,1)S(1)}, u32[]{:S(2)}, u32[]{:S(2)}) async-start(bf16[4,32,2048]{2,1,0:T(8,128)(2,1)} %get-tuple-element.8), calls=%async_computation.2 | async-start | bytes 1048576 | tf_op jit(solution)/shard_map/all_to_all | solution.py:294
  89.6 3.1 %collective-permute-start.8 = (f32[2,2,2,32]{3,2,1,0:T(2,128)S(1)}, f32[2,2,2,32]{3,2,1,0:T(2,128)S(1)}, u32[]{:S(2)}, u32[]{:S(2)}) collective-permute-start(f32[2,2,2,32]{3,2,1,0:T(2,128)S(1)} %get-tuple-element.14), channel_id=1, source_target_pairs={{0,1},{1,0},{2,3},{3,2},{4,5},{5,4},{6,7},{7,6},{8,9},{9,8},{10,11... | collective-permute-start | bytes 3080 | tf_op jit(solution)/shard_map/ppermute | solution.py:297

commit v4 on v3

--- a/solution.py
+++ b/solution.py
@@ -19,6 +19,8 @@
 QB = TEAM * PER
 MAXP = QB * SEL
 UNROLL = 8
+NEAR = (0, 1, 2, 6, 7)
+FAR = (3, 4, 5)
 STATS = 16
 
 rotary_base = 500000.0
@@ -58,6 +60,7 @@
 
 
 def project(x, wq, wk, wv, cos, sin):
+    x, wq, wk, wv = (pltpu.with_memory_space_constraint(a, pltpu.HBM) for a in (x, wq, wk, wv))
     hbm = pl.BlockSpec(memory_space=pltpu.HBM)
     vmem = pl.BlockSpec(memory_space=pltpu.VMEM)
     return pl.pallas_call(
@@ -73,36 +76,34 @@
             pltpu.VMEM((3,) + wq.shape, bf16),
             pltpu.SemaphoreType.DMA((4,)),
         ],
+        compiler_params=pltpu.CompilerParams(vmem_limit_bytes=12 << 20),
         name="project",
     )(x, wq, wk, wv, cos, sin)
 
 
-def attend_kernel(pairs_ref, count_ref, q_ref, *refs):
-    kv_refs = refs[:RING]
-    out_ref = refs[RING]
-    qq, kbuf, vbuf, sbuf, mbuf, lbuf, acc = refs[RING + 1 :]
-    lane = lax.broadcasted_iota(jnp.int32, (BLK, WIDTH), 1)
-    left = lane < HEAD_DIM
-    even = (lane & (HEAD_DIM // 2)) == 0
-    for s in range(RING):
+def fill_keys(kv_refs, kbuf, vbuf):
+    for s, ref in enumerate(kv_refs):
         for b in range(PER):
             rows = pl.ds(b * BLK, BLK)
-            kbuf[s * PER + b] = kv_refs[s][rows, :WIDTH]
-            vbuf[s * PER + b] = kv_refs[s][rows, WIDTH:]
+            kbuf[s * PER + b] = ref[rows, :WIDTH]
+            vbuf[s * PER + b] = ref[rows, WIDTH:]
+
+
+def fill_queries(q_ref, qq):
     half = BLK // 2
-    left_half = left[:half]
+    left = lax.broadcasted_iota(jnp.int32, (half, WIDTH), 1) < HEAD_DIM
     zero = jnp.zeros((half, WIDTH), bf16)
     for i in range(TEAM):
         for b in range(PER):
             for h in range(2):
                 q = q_ref[i, pl.ds(b * BLK + h * half, half), :]
-                qq[i * PER + b, pl.ds(h * BLK, half), :] = jnp.where(left_half, q, zero)
-                qq[i * PER + b, pl.ds(h * BLK + half, half), :] = jnp.where(left_half, zero, q)
+                qq[i * PER + b, pl.ds(h * BLK, half), :] = jnp.where(left, q, zero)
+                qq[i * PER + b, pl.ds(h * BLK + half, half), :] = jnp.where(left, zero, q)
     qq[QB] = jnp.zeros((2 * BLK, WIDTH), bf16)
-    mbuf[...] = jnp.full(mbuf.shape, masked_score, f32)
-    lbuf[...] = jnp.zeros(lbuf.shape, f32)
-    acc[...] = jnp.zeros(acc.shape, f32)
-    trips = count_ref[0]
+
+
+def run_pairs(pairs_ref, trips, qq, kbuf, vbuf, sbuf, mbuf, lbuf, acc, rescale):
+    even = (lax.broadcasted_iota(jnp.int32, (BLK, WIDTH), 1) & (HEAD_DIM // 2)) == 0
 
     def score(it, carry):
         for u in range(UNROLL):
@@ -120,7 +121,12 @@
 
     lax.fori_loop(0, trips, score, 0)
     for i in range(QB + 1):
-        mbuf[i] = jnp.broadcast_to(jnp.max(mbuf[i], axis=0, keepdims=True), (8, WIDTH))
+        top = jnp.broadcast_to(jnp.max(mbuf[i], axis=0, keepdims=True), (8, WIDTH))
+        mbuf[i] = top
+        if rescale is not None:
+            factor = jnp.exp(rescale[i] - top)
+            lbuf[i] = lbuf[i] * factor
+            acc[i] = (acc[i].reshape(8, 8, WIDTH) * factor[None]).reshape(BLK, WIDTH)
 
     def weigh(it, carry):
         for u in range(UNROLL):
@@ -138,6 +144,30 @@
         return carry
 
     lax.fori_loop(0, trips, weigh, 0)
+
+
+def near_kernel(pairs_ref, count_ref, q_ref, *refs):
+    n = len(NEAR)
+    qq, mbuf, lbuf, acc = refs[n : n + 4]
+    kbuf, vbuf, sbuf = refs[n + 4 :]
+    fill_keys(refs[:n], kbuf, vbuf)
+    fill_queries(q_ref, qq)
+    mbuf[...] = jnp.full(mbuf.shape, masked_score, f32)
+    lbuf[...] = jnp.zeros(lbuf.shape, f32)
+    acc[...] = jnp.zeros(acc.shape, f32)
+    run_pairs(pairs_ref, count_ref[0], qq, kbuf, vbuf, sbuf, mbuf, lbuf, acc, None)
+
+
+def far_kernel(pairs_ref, count_ref, qq, m_ref, l_ref, acc_ref, *refs):
+    n = len(FAR)
+    out_ref = refs[n]
+    kbuf, vbuf, sbuf, mbuf, lbuf, acc = refs[n + 1 :]
+    fill_keys(refs[:n], kbuf, vbuf)
+    mbuf[...] = m_ref[...]
+    lbuf[...] = l_ref[...]
+    acc[...] = acc_ref[...]
+    run_pairs(pairs_ref, count_ref[0], qq, kbuf, vbuf, sbuf, mbuf, lbuf, acc, m_ref)
+    left = lax.broadcasted_iota(jnp.int32, (BLK, WIDTH), 1) < HEAD_DIM
     left_row = left[:1]
 
     def finished(i):
@@ -170,26 +200,48 @@
             out_ref[2 * i + c, pl.ds(2 * BLK, STATS), :] = stats.astype(bf16)
 
 
-def attend(pairs, count, q, kvs):
+STATE = (
+    jax.ShapeDtypeStruct((QB + 1, 2 * BLK, WIDTH), bf16),
+    jax.ShapeDtypeStruct((QB + 1, 8, WIDTH), f32),
+    jax.ShapeDtypeStruct((QB + 1, 8, WIDTH), f32),
+    jax.ShapeDtypeStruct((QB + 1, BLK, WIDTH), f32),
+)
+
+
+def key_scratch(n):
+    return [
+        pltpu.VMEM((n * PER, BLK, WIDTH), bf16),
+        pltpu.VMEM((n * PER, BLK, WIDTH), bf16),
+        pltpu.VMEM((MAXP, BLK, WIDTH), f32),
+    ]
+
+
+def attend_near(pairs, count, q, kvs):
     smem = pl.BlockSpec(memory_space=pltpu.SMEM)
     vmem = pl.BlockSpec(memory_space=pltpu.VMEM)
     return pl.pallas_call(
-        attend_kernel,
+        near_kernel,
+        out_shape=STATE,
+        in_specs=[smem, smem] + [vmem] * (1 + len(kvs)),
+        out_specs=(vmem,) * len(STATE),
+        scratch_shapes=key_scratch(len(kvs)),
+        compiler_params=pltpu.CompilerParams(vmem_limit_bytes=26 << 20),
+        name="near",
+    )(pairs, count, q, *kvs)
+
+
+def attend_far(pairs, count, state, kvs):
+    smem = pl.BlockSpec(memory_space=pltpu.SMEM)
+    vmem = pl.BlockSpec(memory_space=pltpu.VMEM)
+    return pl.pallas_call(
+        far_kernel,
         out_shape=jax.ShapeDtypeStruct((2 * TEAM, 2 * BLK + STATS, WIDTH), bf16),
-        in_specs=[smem, smem] + [vmem] * (1 + RING),
+        in_specs=[smem, smem] + [vmem] * (len(state) + len(kvs)),
         out_specs=vmem,
-        scratch_shapes=[
-            pltpu.VMEM((QB + 1, 2 * BLK, WIDTH), bf16),
-            pltpu.VMEM((RING * PER, BLK, WIDTH), bf16),
-            pltpu.VMEM((RING * PER, BLK, WIDTH), bf16),
-            pltpu.VMEM((MAXP, BLK, WIDTH), f32),
-            pltpu.VMEM((QB + 1, 8, WIDTH), f32),
-            pltpu.VMEM((QB + 1, 8, WIDTH), f32),
-            pltpu.VMEM((QB + 1, BLK, WIDTH), f32),
-        ],
-        compiler_params=pltpu.CompilerParams(vmem_limit_bytes=28 << 20),
-        name="attend",
-    )(pairs, count, q, *kvs)
+        scratch_shapes=key_scratch(len(kvs)) + [pltpu.VMEM(s.shape, s.dtype) for s in STATE[1:]],
+        compiler_params=pltpu.CompilerParams(vmem_limit_bytes=26 << 20),
+        name="far",
+    )(pairs, count, *state, *kvs)
 
 
 def merge_kernel(core_ref, part_ref, same_ref, other_ref, out_ref, log_ref, att):
@@ -238,21 +290,26 @@
     )(core.reshape(1), parts, w_same, w_other)
 
 
-def pair_list(chosen, zh, mine):
+def pair_lists(chosen, zh, mine):
     lists = lax.dynamic_slice_in_dim(chosen, zh * QB, QB, 0)
     here = (lists >= 0) & (((lists >> 2) & (TEAM - 1)) == mine)
     slot = (zh - (lists >> 5)) & (RING - 1)
-    code = jnp.arange(QB, dtype=jnp.int32)[:, None] * 64 + slot * PER + (lists & (PER - 1))
-    here = here.reshape(-1)
+    far = (slot >= FAR[0]) & (slot <= FAR[-1])
+    order = jnp.where(far, slot - FAR[0], jnp.where(slot > FAR[-1], slot - len(FAR), slot))
+    code = jnp.arange(QB, dtype=jnp.int32)[:, None] * 64 + order * PER + (lists & (PER - 1))
+    kind = jnp.where(here, jnp.where(far, 1, 0), -1).reshape(-1)
     code = code.reshape(-1)
     index = jnp.arange(MAXP, dtype=jnp.int32)
-    before = jnp.sum(jnp.where(index[:, None] < index[None, :], here[:, None], False).astype(jnp.int32), axis=0)
-    place = jnp.where(here, before, -1)
-    hit = place[:, None] == index[None, :]
-    pairs = jnp.sum(jnp.where(hit, code[:, None], 0), axis=0)
-    count = jnp.sum(here.astype(jnp.int32))
-    pairs = jnp.where(index < count, pairs, QB * 64)
-    return pairs, ((count + UNROLL - 1) // UNROLL).reshape(1)
+    same = kind[:, None] == kind[None, :]
+    before = jnp.sum((same & (index[:, None] < index[None, :])).astype(jnp.int32), axis=0)
+    out = []
+    for k in range(2):
+        place = jnp.where(kind == k, before, -1)
+        pairs = jnp.sum(jnp.where(place[:, None] == index[None, :], code[:, None], 0), axis=0)
+        count = jnp.sum((kind == k).astype(jnp.int32))
+        pairs = jnp.where(index < count, pairs, QB * 64)
+        out.append((pairs, ((count + UNROLL - 1) // UNROLL).reshape(1)))
+    return out
 
 
 def up_pairs(step):
@@ -276,7 +333,7 @@
     q8, kv = project(
         tokens, w_query, w_key, w_value, jnp.cos(angles), jnp.sin(angles) * sign[None, :]
     )
-    pairs, count = pair_list(chosen, zh, mine)
+    near, far = pair_lists(chosen, zh, mine)
     slots = [kv] + [None] * (RING - 1)
     up = down = kv
     for s in range(1, RING // 2 + 1):
@@ -288,7 +345,8 @@
     q_team = lax.all_to_all(q8, ("zl", "y"), 0, 0, tiled=True)
     core = lax.axis_index("c")
     w_other = lax.ppermute(w_out, "c", [(0, 1), (1, 0)])
-    parts = attend(pairs, count, q_team, slots)
+    state = attend_near(*near, q_team, [slots[i] for i in NEAR])
+    parts = attend_far(*far, state, [slots[i] for i in FAR])
     parts = lax.all_to_all(parts, ("zl", "y", "c"), 0, 0, tiled=True)
     partial, logs = merge(core, parts, w_out, w_other)
     tiles = lax.all_to_all(partial, "x", 0, 0, tiled=True)

time: 101 us -> 96.2 us (0.952)
  the two profiles are of different devices: /device:TPU:288 before, /device:TPU:192 now
where the time goes in v4:
time: 96.2 us; the launch traced here: 95.6 us
  starting transfers between devices  52.7 us (55%)
  waiting for transfers between devices  21.5 us (22%)
  Pallas kernels  14.3 us (15%)
  other arithmetic  3.8 us (4%)
  between operations  2.2 us (2%)
  local copies, waits for them, and re-layouts  1.16 us (1%)
    ppermute x4, starting transfers between devices, local(): up = lax.ppermute(up, 'zh', up_pairs(s))  24.9 us
    all_to_all x1, starting transfers between devices, local(): parts = lax.all_to_all(parts, ('zl', 'y', 'c'), 0, 0, tiled=True)  11.4 us
    all_to_all x1, waiting for transfers between devices, local(): parts = lax.all_to_all(parts, ('zl', 'y', 'c'), 0, 0, tiled=True)  7.73 us
    pallas_call x1, Pallas kernels, attend_near(): pl.pallas_call(near_kernel, out_shape=STATE, in_specs=[smem, smem] + [vme...  7.29 us
    ppermute x4, waiting for transfers between devices, local(): up = lax.ppermute(up, 'zh', up_pairs(s))  6.03 us
    all_to_all x1, starting transfers between devices, local(): q_team = lax.all_to_all(q8, ('zl', 'y'), 0, 0, tiled=True)  5.84 us
    all_to_all x1, waiting for transfers between devices, local(): tiles = lax.all_to_all(partial, 'x', 0, 0, tiled=True)  5.05 us
    all_to_all x1, starting transfers between devices, local(): tiles = lax.all_to_all(partial, 'x', 0, 0, tiled=True)  4.29 us
  transfers between devices with their start and end apart: 12, of which 7 were waited for; matrix products, arithmetic and copies ran while one was open for 4% of the time, Pallas kernels for 8%

profile of v4, /device:TPU:192, one launch (start us, length us, event | category | flops | bytes accessed | tf_op | source)
XLA Modules:
  0.0 95.6 jit_solution(11632699054142224974)
XLA Ops:
  0.7 0.1 mul.61
  0.8 0.5 fusion.1
  1.3 3.6 %project.1 = (bf16[8,256,128]{2,1,0:T(8,128)(2,1)}, bf16[256,256]{1,0:T(8,128)(2,1)S(1)}) custom-call(bf16[256,2048]{1,0:T(8,128)(2,1)} %x_hbm.1, bf16[2048,128]{1,0:T(8,128)(2,1)} %wq_hbm.1, bf16[2048,128]{1,0:T(8,128)(2,1)} %wk_hbm.1, bf16[2048,128]{1,0:T(8,128)(2,1)} %wv_hbm.1, f32[256,128]{1,0:T(8,128)S(1)} %get-tuple-element.29.cos_ref, ...), custom_call_target="tpu_custom_call" | custom-call | tf_op jit(solution)/shard_map/project/pallas_call | solution.py:66
  4.9 5.8 %all-to-all-start = ((bf16[8,256,128]{2,1,0:T(8,128)(2,1)}), bf16[8,256,128]{2,1,0:T(8,128)(2,1)S(1)}, u32[]{:S(2)}, u32[]{:S(2)}) async-start(bf16[8,256,128]{2,1,0:T(8,128)(2,1)} %get-tuple-element.10), calls=%async_computation | async-start | bytes 1048576 | tf_op jit(solution)/shard_map/all_to_all | solution.py:345
  10.8 5.5 %collective-permute-start = (bf16[256,256]{1,0:T(8,128)(2,1)S(1)}, bf16[256,256]{1,0:T(8,128)(2,1)S(1)}, u32[]{:S(2)}, u32[]{:S(2)}) collective-permute-start(bf16[256,256]{1,0:T(8,128)(2,1)S(1)} %get-tuple-element.11.refs_0_), channel_id=1, source_target_pairs={{0,64},{64,128},{128,192},{192,256},{256,320},{320,384},{384,448},... | collective-permute-start | bytes 393224 | tf_op jit(solution)/shard_map/ppermute | solution.py:340
  16.3 0.7 collective-permute-start.2
  17.0 0.7 convert_reduce_fusion.1
  19.3 0.2 convert_reduce_fusion
  19.5 2.8 %collective-permute-done.refs_1_ = bf16[256,256]{1,0:T(8,128)(2,1)S(1)} collective-permute-done((bf16[256,256]{1,0:T(8,128)(2,1)S(1)}, bf16[256,256]{1,0:T(8,128)(2,1)S(1)}, u32[]{:S(2)}, u32[]{:S(2)}) %collective-permute-start) | collective-permute-done | bytes 131104 | tf_op jit(solution)/shard_map/ppermute | solution.py:340
  22.3 6.4 %collective-permute-start.1 = (bf16[256,256]{1,0:T(8,128)(2,1)S(1)}, bf16[256,256]{1,0:T(8,128)(2,1)S(1)}, u32[]{:S(2)}, u32[]{:S(2)}) collective-permute-start(bf16[256,256]{1,0:T(8,128)(2,1)S(1)} %collective-permute-done.refs_1_), channel_id=1, source_target_pairs={{64,128},{128,192},{192,256},{256,320},{320,384},{384,448},{65,129... | collective-permute-start | bytes 393224 | tf_op jit(solution)/shard_map/ppermute | solution.py:340
  28.7 0.3 select_reduce_fusion
  29.0 0.7 collective-permute-start.3
  29.6 1.5 %collective-permute-done.1.refs_2_ = bf16[256,256]{1,0:T(8,128)(2,1)S(1)} collective-permute-done((bf16[256,256]{1,0:T(8,128)(2,1)S(1)}, bf16[256,256]{1,0:T(8,128)(2,1)S(1)}, u32[]{:S(2)}, u32[]{:S(2)}) %collective-permute-start.1) | collective-permute-done | bytes 131104 | tf_op jit(solution)/shard_map/ppermute | solution.py:340
  31.2 6.5 %collective-permute-start.4 = (bf16[256,256]{1,0:T(8,128)(2,1)S(1)}, bf16[256,256]{1,0:T(8,128)(2,1)S(1)}, u32[]{:S(2)}, u32[]{:S(2)}) collective-permute-start(bf16[256,256]{1,0:T(8,128)(2,1)S(1)} %collective-permute-done.1.refs_2_), channel_id=1, source_target_pairs={{128,192},{192,256},{256,320},{320,384},{384,448},{129,193},{193,2... | collective-permute-start | bytes 393224 | tf_op jit(solution)/shard_map/ppermute | solution.py:340
  37.6 0.7 fusion.11.pairs_ref
  38.3 0.7 collective-permute-start.6
  39.0 1.7 %collective-permute-done.4.refs_0_ = bf16[256,256]{1,0:T(8,128)(2,1)S(1)} collective-permute-done((bf16[256,256]{1,0:T(8,128)(2,1)S(1)}, bf16[256,256]{1,0:T(8,128)(2,1)S(1)}, u32[]{:S(2)}, u32[]{:S(2)}) %collective-permute-start.4) | collective-permute-done | bytes 131104 | tf_op jit(solution)/shard_map/ppermute | solution.py:340
  40.7 6.6 %collective-permute-start.5 = (bf16[256,256]{1,0:T(8,128)(2,1)S(1)}, bf16[256,256]{1,0:T(8,128)(2,1)S(1)}, u32[]{:S(2)}, u32[]{:S(2)}) collective-permute-start(bf16[256,256]{1,0:T(8,128)(2,1)S(1)} %collective-permute-done.4.refs_0_), channel_id=1, source_target_pairs={{192,256},{256,320},{320,384},{384,448},{193,257},{257,321},{321,3... | collective-permute-start | bytes 393224 | tf_op jit(solution)/shard_map/ppermute | solution.py:340
  47.3 0.7 fusion.12.pairs_ref
  48.0 7.3 %near.1 = (bf16[33,128,128]{2,1,0:T(8,128)(2,1)S(1)}, f32[33,8,128]{2,1,0:T(8,128)S(1)}, f32[33,8,128]{2,1,0:T(8,128)S(1)}, f32[33,64,128]{2,1,0:T(8,128)S(1)}) custom-call(s32[512]{0:T(512)S(1)} %fusion.12.pairs_ref, s32[1]{0:T(128)} %bitcast.2.count_ref, bf16[8,256,128]{2,1,0:T(8,128)(2,1)S(1)} %all-to-all-done.q_ref, ...), custom_call_target="tpu_custom_call" | custom-call | tf_op jit(solution)/shard_map/near/pallas_call | solution.py:222
  55.3 1.9 %far.1 = bf16[16,144,128]{2,1,0:T(8,128)(2,1)} custom-call(s32[512]{0:T(512)S(1)} %fusion.11.pairs_ref, s32[1]{0:T(128)} %bitcast.1.count_ref, bf16[33,128,128]{2,1,0:T(8,128)(2,1)S(1)} %get-tuple-element.12.qq, f32[33,8,128]{2,1,0:T(8,128)S(1)} %get-tuple-element.13.m_ref, f32[33,8,128]{2,1,0:T(8,128)S(1)} %get-tuple-element.14.l_ref, ...), custom_call_target="tpu_custom_call" | custom-call | tf_op jit(solution)/shard_map/far/pallas_call | solution.py:236
  57.2 11.4 %all-to-all-start.1 = ((bf16[16,144,128]{2,1,0:T(8,128)(2,1)}), bf16[16,144,128]{2,1,0:T(8,128)(2,1)S(1)}, u32[]{:S(2)}, u32[]{:S(2)}) async-start(bf16[16,144,128]{2,1,0:T(8,128)(2,1)} %far.1), calls=%async_computation.1 | async-start | bytes 1179648 | tf_op jit(solution)/shard_map/all_to_all | solution.py:350
  68.6 2.3 %collective-permute-start.7 = (bf16[128,2048]{1,0:T(8,128)(2,1)S(1)}, bf16[128,2048]{1,0:T(8,128)(2,1)S(1)}, u32[]{:S(2)}, u32[]{:S(2)}) collective-permute-start(bf16[128,2048]{1,0:T(8,128)(2,1)S(1)} %copy-done), channel_id=1, source_target_pairs={{0,1},{1,0},{2,3},{3,2},{4,5},{5,4},{6,7},{7,6},{8,9},{9,8},{10,11... | collective-permute-start | bytes 1572872 | tf_op jit(solution)/shard_map/ppermute | solution.py:347
  71.0 1.5 %collective-permute-done.7.other_ref = bf16[128,2048]{1,0:T(8,128)(2,1)S(1)} collective-permute-done((bf16[128,2048]{1,0:T(8,128)(2,1)S(1)}, bf16[128,2048]{1,0:T(8,128)(2,1)S(1)}, u32[]{:S(2)}, u32[]{:S(2)}) %collective-permute-start.7) | collective-permute-done | bytes 524320 | tf_op jit(solution)/shard_map/ppermute | solution.py:347
  72.5 7.7 %all-to-all-done.1.part_ref = bf16[16,144,128]{2,1,0:T(8,128)(2,1)S(1)} async-done(((bf16[16,144,128]{2,1,0:T(8,128)(2,1)}), bf16[16,144,128]{2,1,0:T(8,128)(2,1)S(1)}, u32[]{:S(2)}, u32[]{:S(2)}) %all-to-all-start.1) | async-done | bytes 589856 | tf_op jit(solution)/shard_map/all_to_all | solution.py:350
  80.2 1.5 %merge.1 = (bf16[4,32,2048]{2,1,0:T(8,128)(2,1)}, f32[4,128]{1,0:T(4,128)S(1)}) custom-call(s32[1]{0:T(128)} %bitcast.core_ref, bf16[16,144,128]{2,1,0:T(8,128)(2,1)S(1)} %all-to-all-done.1.part_ref, bf16[128,2048]{1,0:T(8,128)(2,1)S(1)} %copy-done, bf16[128,2048]{1,0:T(8,128)(2,1)S(1)} %collective-permute-done.7.other_ref), custom_call_target="tpu_custom_call" | custom-call | tf_op jit(solution)/shard_map/merge/pallas_call | solution.py:279
  81.7 4.3 %all-to-all-start.2 = ((bf16[4,32,2048]{2,1,0:T(8,128)(2,1)}), bf16[4,32,2048]{2,1,0:T(8,128)(2,1)S(1)}, u32[]{:S(2)}, u32[]{:S(2)}) async-start(bf16[4,32,2048]{2,1,0:T(8,128)(2,1)} %get-tuple-element.16), calls=%async_computation.2 | async-start | bytes 1048576 | tf_op jit(solution)/shard_map/all_to_all | solution.py:352
  86.1 1.9 %collective-permute-start.8 = (f32[2,2,2,32]{3,2,1,0:T(2,128)S(1)}, f32[2,2,2,32]{3,2,1,0:T(2,128)S(1)}, u32[]{:S(2)}, u32[]{:S(2)}) collective-permute-start(f32[2,2,2,32]{3,2,1,0:T(2,128)S(1)} %get-tuple-element.25), channel_id=1, source_target_pairs={{0,1},{1,0},{2,3},{3,2},{4,5},{5,4},{6,7},{7,6},{8,9},{9,8},{10,11... | collective-permute-start | bytes 3080 | tf_op jit(solution)/shard_map/ppermute | solution.py:355
  88.0 1.1 %collective-permute-done.8 = f32[2,2,2,32]{3,2,1,0:T(2,128)S(1)} collective-permute-done((f32[2,2,2,32]{3,2,1,0:T(2,128)S(1)}, f32[2,2,2,32]{3,2,1,0:T(2,128)S(1)}, u32[]{:S(2)}, u32[]{:S(2)}) %collective-permute-start.8) | collective-permute-done | bytes 1056 | tf_op jit(solution)/shard_map/ppermute | solution.py:355
  89.2 0.7 reshape.69
  89.8 5.1 %all-to-all-done.2 = bf16[4,32,2048]{2,1,0:T(8,128)(2,1)S(1)} async-done(((bf16[4,32,2048]{2,1,0:T(8,128)(2,1)}), bf16[4,32,2048]{2,1,0:T(8,128)(2,1)S(1)}, u32[]{:S(2)}, u32[]{:S(2)}) %all-to-all-start.2) | async-done | bytes 524320 | tf_op jit(solution)/shard_map/all_to_all | solution.py:352
  94.9 0.7 reduce_sum.62
  (23 shorter events, 0.5 us)
Async XLA Ops:
  1.3 15.6 %copy-start.1 = (s32[256,16]{0,1:T(8,128)S(1)}, s32[256,16]{0,1:T(8,128)}, u32[]{:S(2)}) copy-start(s32[256,16]{0,1:T(8,128)} %param.11) | copy-start | bytes 49156
  4.9 43.0 %all-to-all-start = ((bf16[8,256,128]{2,1,0:T(8,128)(2,1)}), bf16[8,256,128]{2,1,0:T(8,128)(2,1)S(1)}, u32[]{:S(2)}, u32[]{:S(2)}) async-start(bf16[8,256,128]{2,1,0:T(8,128)(2,1)} %get-tuple-element.10), calls=%async_computation | async-start | bytes 1048576 | tf_op jit(solution)/shard_map/all_to_all | solution.py:345
  10.8 11.5 %collective-permute-start = (bf16[256,256]{1,0:T(8,128)(2,1)S(1)}, bf16[256,256]{1,0:T(8,128)(2,1)S(1)}, u32[]{:S(2)}, u32[]{:S(2)}) collective-permute-start(bf16[256,256]{1,0:T(8,128)(2,1)S(1)} %get-tuple-element.11.refs_0_), channel_id=1, source_target_pairs={{0,64},{64,128},{128,192},{192,256},{256,320},{320,384},{384,448},... | collective-permute-start | bytes 393224 | tf_op jit(solution)/shard_map/ppermute | solution.py:340
  16.3 12.7 %collective-permute-start.2 = (bf16[256,256]{1,0:T(8,128)(2,1)S(1)}, bf16[256,256]{1,0:T(8,128)(2,1)S(1)}, u32[]{:S(2)}, u32[]{:S(2)}) collective-permute-start(bf16[256,256]{1,0:T(8,128)(2,1)S(1)} %get-tuple-element.11.refs_0_), channel_id=1, source_target_pairs={{0,448},{64,0},{128,64},{1,449},{65,1},{129,65},{2,450},{66,2},{13... | collective-permute-start | bytes 393224 | tf_op jit(solution)/shard_map/ppermute | solution.py:343
  22.3 8.9 %collective-permute-start.1 = (bf16[256,256]{1,0:T(8,128)(2,1)S(1)}, bf16[256,256]{1,0:T(8,128)(2,1)S(1)}, u32[]{:S(2)}, u32[]{:S(2)}) collective-permute-start(bf16[256,256]{1,0:T(8,128)(2,1)S(1)} %collective-permute-done.refs_1_), channel_id=1, source_target_pairs={{64,128},{128,192},{192,256},{256,320},{320,384},{384,448},{65,129... | collective-permute-start | bytes 393224 | tf_op jit(solution)/shard_map/ppermute | solution.py:340
  29.0 9.3 %collective-permute-start.3 = (bf16[256,256]{1,0:T(8,128)(2,1)S(1)}, bf16[256,256]{1,0:T(8,128)(2,1)S(1)}, u32[]{:S(2)}, u32[]{:S(2)}) collective-permute-start(bf16[256,256]{1,0:T(8,128)(2,1)S(1)} %collective-permute-done.2.refs_4_), channel_id=1, source_target_pairs={{448,384},{0,448},{64,0},{449,385},{1,449},{65,1},{450,386},{2,450... | collective-permute-start | bytes 393224 | tf_op jit(solution)/shard_map/ppermute | solution.py:343
  31.2 9.5 %collective-permute-start.4 = (bf16[256,256]{1,0:T(8,128)(2,1)S(1)}, bf16[256,256]{1,0:T(8,128)(2,1)S(1)}, u32[]{:S(2)}, u32[]{:S(2)}) collective-permute-start(bf16[256,256]{1,0:T(8,128)(2,1)S(1)} %collective-permute-done.1.refs_2_), channel_id=1, source_target_pairs={{128,192},{192,256},{256,320},{320,384},{384,448},{129,193},{193,2... | collective-permute-start | bytes 393224 | tf_op jit(solution)/shard_map/ppermute | solution.py:340
  38.3 17.0 %collective-permute-start.6 = (bf16[256,256]{1,0:T(8,128)(2,1)S(1)}, bf16[256,256]{1,0:T(8,128)(2,1)S(1)}, u32[]{:S(2)}, u32[]{:S(2)}) collective-permute-start(bf16[256,256]{1,0:T(8,128)(2,1)S(1)} %collective-permute-done.3.refs_3_), channel_id=1, source_target_pairs={{384,320},{448,384},{0,448},{385,321},{449,385},{1,449},{386,322},... | collective-permute-start | bytes 393224 | tf_op jit(solution)/shard_map/ppermute | solution.py:343
  40.7 14.6 %collective-permute-start.5 = (bf16[256,256]{1,0:T(8,128)(2,1)S(1)}, bf16[256,256]{1,0:T(8,128)(2,1)S(1)}, u32[]{:S(2)}, u32[]{:S(2)}) collective-permute-start(bf16[256,256]{1,0:T(8,128)(2,1)S(1)} %collective-permute-done.4.refs_0_), channel_id=1, source_target_pairs={{192,256},{256,320},{320,384},{384,448},{193,257},{257,321},{321,3... | collective-permute-start | bytes 393224 | tf_op jit(solution)/shard_map/ppermute | solution.py:340
  57.2 11.4 %copy-start = (bf16[128,2048]{1,0:T(8,128)(2,1)S(1)}, bf16[128,2048]{1,0:T(8,128)(2,1)}, u32[]{:S(2)}) copy-start(bf16[128,2048]{1,0:T(8,128)(2,1)} %same_ref.1) | copy-start | bytes 1572868
  57.2 23.0 %all-to-all-start.1 = ((bf16[16,144,128]{2,1,0:T(8,128)(2,1)}), bf16[16,144,128]{2,1,0:T(8,128)(2,1)S(1)}, u32[]{:S(2)}, u32[]{:S(2)}) async-start(bf16[16,144,128]{2,1,0:T(8,128)(2,1)} %far.1), calls=%async_computation.1 | async-start | bytes 1179648 | tf_op jit(solution)/shard_map/all_to_all | solution.py:350
  68.6 3.8 %collective-permute-start.7 = (bf16[128,2048]{1,0:T(8,128)(2,1)S(1)}, bf16[128,2048]{1,0:T(8,128)(2,1)S(1)}, u32[]{:S(2)}, u32[]{:S(2)}) collective-permute-start(bf16[128,2048]{1,0:T(8,128)(2,1)S(1)} %copy-done), channel_id=1, source_target_pairs={{0,1},{1,0},{2,3},{3,2},{4,5},{5,4},{6,7},{7,6},{8,9},{9,8},{10,11... | collective-permute-start | bytes 1572872 | tf_op jit(solution)/shard_map/ppermute | solution.py:347
  81.7 13.2 %all-to-all-start.2 = ((bf16[4,32,2048]{2,1,0:T(8,128)(2,1)}), bf16[4,32,2048]{2,1,0:T(8,128)(2,1)S(1)}, u32[]{:S(2)}, u32[]{:S(2)}) async-start(bf16[4,32,2048]{2,1,0:T(8,128)(2,1)} %get-tuple-element.16), calls=%async_computation.2 | async-start | bytes 1048576 | tf_op jit(solution)/shard_map/all_to_all | solution.py:352
  86.1 3.1 %collective-permute-start.8 = (f32[2,2,2,32]{3,2,1,0:T(2,128)S(1)}, f32[2,2,2,32]{3,2,1,0:T(2,128)S(1)}, u32[]{:S(2)}, u32[]{:S(2)}) collective-permute-start(f32[2,2,2,32]{3,2,1,0:T(2,128)S(1)} %get-tuple-element.25), channel_id=1, source_target_pairs={{0,1},{1,0},{2,3},{3,2},{4,5},{5,4},{6,7},{7,6},{8,9},{9,8},{10,11... | collective-permute-start | bytes 3080 | tf_op jit(solution)/shard_map/ppermute | solution.py:355

commit v5 on v4

v5 whole, which is shorter than its diff:
```python
import functools

import jax
import jax.numpy as jnp
from jax import lax
from jax.experimental import pallas as pl
from jax.experimental.pallas import tpu as pltpu
from jax.sharding import Mesh
from jax.sharding import PartitionSpec as P

HEAD_DIM = 64
BLK = 64
SEL = 16
ROWS = 256
PER = 4
WIDTH = 128
RING = 8
TEAM = 8
QB = TEAM * PER
MAXP = QB * SEL
UNROLL_BITS = 5
UNROLL = 1 << UNROLL_BITS
NBLK = 256
NEAR = (0, 1, 2, 6, 7)
FAR = (3, 4, 5)
STATS = 16

rotary_base = 500000.0
masked_score = -1e30
f32 = jnp.float32
bf16 = jnp.bfloat16


def pair_lists(chosen_t, zh, mine, pairs_ref):
    i32 = jnp.int32
    rolled = pltpu.roll(chosen_t, (NBLK - zh * QB) & (NBLK - 1), 1)[:, :WIDTH]
    lists = rolled.astype(f32).T[:QB].astype(i32)
    here = (lists >= 0) & (((lists >> 2) & (TEAM - 1)) == mine)
    slot = (zh - (lists >> 5)) & (RING - 1)
    far = (slot >= FAR[0]) & (slot <= FAR[-1])
    order = jnp.where(far, slot - FAR[0], jnp.where(slot > FAR[-1], slot - len(FAR), slot))
    block = lax.broadcasted_iota(i32, (QB, SEL), 0)
    code = (block * 64 + order * PER + (lists & (PER - 1))).astype(f32)
    earlier = lax.broadcasted_iota(i32, (QB, QB), 1) < lax.broadcasted_iota(i32, (QB, QB), 0)
    before = lax.broadcasted_iota(i32, (SEL, SEL), 0) < lax.broadcasted_iota(i32, (SEL, SEL), 1)
    index = lax.broadcasted_iota(i32, (QB, MAXP), 1).astype(f32)
    row = lax.broadcasted_iota(i32, (1, MAXP), 1).astype(f32)
    for k, wanted in enumerate((here & ~far, here & far)):
        one = jnp.where(wanted, 1.0, 0.0)
        inside = jnp.dot(jnp.where(earlier, 1.0, 0.0), one, preferred_element_type=f32)
        sums = jnp.sum(one, axis=0, keepdims=True)
        base = jnp.dot(sums, jnp.where(before, 1.0, 0.0), preferred_element_type=f32)
        place = jnp.where(wanted, inside + base, -1.0)
        picked = jnp.zeros((QB, MAXP), f32)
        for j in range(SEL):
            picked = picked + jnp.where(place[:, j : j + 1] == index, code[:, j : j + 1], 0.0)
        count = jnp.sum(sums, axis=1, keepdims=True)
        pairs = jnp.where(row < count, jnp.sum(picked, axis=0, keepdims=True), float(QB * 64))
        pairs_ref[pl.ds(k, 1), :] = pairs.astype(i32)
        trips = (count.astype(i32) + (UNROLL - 1)) >> UNROLL_BITS
        pairs_ref[pl.ds(2 + k, 1), :] = jnp.broadcast_to(trips, (1, MAXP))


def project_kernel(
    place_ref, x_hbm, wq_hbm, wk_hbm, wv_hbm, chosen_ref, cos_ref, sin_ref, q_ref, kv_ref, pairs_ref, x_buf, w_buf, sems
):
    copies = [pltpu.make_async_copy(x_hbm, x_buf, sems.at[0])]
    for i, w in enumerate((wk_hbm, wv_hbm, wq_hbm)):
        copies.append(pltpu.make_async_copy(w, w_buf.at[i], sems.at[i + 1]))
    for copy in copies:
        copy.start()
    pair_lists(chosen_ref[...], place_ref[0], place_ref[1], pairs_ref)
    cos = cos_ref[...]
    sin = sin_ref[...]
    lane = lax.broadcasted_iota(jnp.int32, (ROWS, WIDTH), 1)
    first = (lane & (HEAD_DIM - 1)) < HEAD_DIM // 2

    def turned(t):
        partner = jnp.where(first, pltpu.roll(t, WIDTH - HEAD_DIM // 2, 1), pltpu.roll(t, HEAD_DIM // 2, 1))
        return t * cos + partner * sin

    copies[0].wait()
    copies[1].wait()
    x = x_buf[...]
    k = jnp.dot(x, w_buf[0], preferred_element_type=f32)
    kv_ref[pl.ds(0, ROWS), :] = turned(k).astype(bf16)
    copies[2].wait()
    v = jnp.dot(x, w_buf[1], preferred_element_type=f32)
    for p in range(ROWS // WIDTH):
        kv_ref[pl.ds(ROWS + p * WIDTH, WIDTH), :] = v[p * WIDTH : (p + 1) * WIDTH].T.astype(bf16)
    copies[3].wait()
    q = jnp.dot(x, w_buf[2], preferred_element_type=f32)
    q = turned(q) * (HEAD_DIM**-0.5)
    for p in range(ROWS // WIDTH):
        flipped = q[p * WIDTH : (p + 1) * WIDTH].T.astype(bf16)
        for i in range(TEAM):
            q_ref[i, pl.ds(p * WIDTH, WIDTH), :] = flipped


def project(place, x, wq, wk, wv, chosen_t, cos, sin):
    x, wq, wk, wv = (pltpu.with_memory_space_constraint(a, pltpu.HBM) for a in (x, wq, wk, wv))
    hbm = pl.BlockSpec(memory_space=pltpu.HBM)
    smem = pl.BlockSpec(memory_space=pltpu.SMEM)
    vmem = pl.BlockSpec(memory_space=pltpu.VMEM)
    return pl.pallas_call(
        project_kernel,
        out_shape=(
            jax.ShapeDtypeStruct((TEAM, ROWS, WIDTH), bf16),
            jax.ShapeDtypeStruct((2 * ROWS, WIDTH), bf16),
            jax.ShapeDtypeStruct((4, MAXP), jnp.int32),
        ),
        in_specs=[smem] + [hbm] * 4 + [vmem] * 3,
        out_specs=(vmem, vmem, vmem),
        scratch_shapes=[
            pltpu.VMEM(x.shape, bf16),
            pltpu.VMEM((3,) + wq.shape, bf16),
            pltpu.SemaphoreType.DMA((4,)),
        ],
        compiler_params=pltpu.CompilerParams(vmem_limit_bytes=12 << 20),
        name="project",
    )(place, x, wq, wk, wv, chosen_t, cos, sin)


def fill_keys(kv_refs, kbuf, vbuf):
    for s, ref in enumerate(kv_refs):
        for b in range(PER):
            kbuf[s * PER + b] = ref[pl.ds(b * BLK, BLK), :]
        for p in range(ROWS // WIDTH):
            both = ref[pl.ds(ROWS + p * WIDTH, WIDTH), :]
            vbuf[s * PER + 2 * p] = both[:, :BLK]
            vbuf[s * PER + 2 * p + 1] = both[:, BLK:]


def fill_queries(q_ref, qq):
    lane = lax.broadcasted_iota(jnp.int32, (WIDTH, WIDTH), 1)
    row = lax.broadcasted_iota(jnp.int32, (WIDTH, WIDTH), 0)
    half = BLK // 2
    own = (row < HEAD_DIM) == ((lane & half) == 0)
    early = lane < half
    late = lane >= 3 * half
    for i in range(TEAM):
        for p in range(ROWS // WIDTH):
            t = q_ref[i, pl.ds(p * WIDTH, WIDTH), :].astype(f32)
            r64 = pltpu.roll(t, 2 * half, 1)
            first = jnp.where(early, t, jnp.where(late, r64, pltpu.roll(t, half, 1)))
            second = jnp.where(early, r64, jnp.where(late, t, pltpu.roll(t, 3 * half, 1)))
            qq[i * PER + 2 * p] = jnp.where(own, first, 0.0).astype(bf16)
            qq[i * PER + 2 * p + 1] = jnp.where(own, second, 0.0).astype(bf16)
    qq[QB] = jnp.zeros((WIDTH, WIDTH), bf16)


def run_pairs(pairs_ref, kind, qq, kbuf, vbuf, sbuf, mbuf, lbuf, acc, rescale):
    even = (lax.broadcasted_iota(jnp.int32, (BLK, WIDTH), 1) & (HEAD_DIM // 2)) == 0
    trips = pairs_ref[2 + kind, 0]

    def score(it, carry):
        for u in range(UNROLL):
            i = it * UNROLL + u
            code = pairs_ref[kind, i]
            qi = code >> 6
            ki = code & 63
            st = jnp.dot(kbuf[ki], qq[qi], preferred_element_type=f32)
            sbuf[i] = st
            m8 = jnp.max(st.reshape(8, 8, WIDTH), axis=0)
            mbuf[qi] = jnp.maximum(mbuf[qi], m8)
        return carry

    lax.fori_loop(0, trips, score, 0)
    for i in range(QB + 1):
        top = jnp.broadcast_to(jnp.max(mbuf[i], axis=0, keepdims=True), (8, WIDTH))
        mbuf[i] = top
        if rescale is not None:
            factor = jnp.exp(rescale[i] - top)
            lbuf[i] = lbuf[i] * factor
            acc[i] = (acc[i].reshape(8, 8, WIDTH) * factor[None]).reshape(BLK, WIDTH)

    def weigh(it, carry):
        for u in range(UNROLL):
            i = it * UNROLL + u
            code = pairs_ref[kind, i]
            qi = code >> 6
            ki = code & 63
            p = jnp.exp(sbuf[i].reshape(8, 8, WIDTH) - mbuf[qi][None])
            lbuf[qi] = lbuf[qi] + jnp.sum(p, axis=0)
            pb = p.reshape(BLK, WIDTH).astype(bf16)
            ot = jnp.dot(vbuf[ki], pb, preferred_element_type=f32)
            acc[qi] = acc[qi] + jnp.where(even, ot[:HEAD_DIM], ot[HEAD_DIM:])
        return carry

    lax.fori_loop(0, trips, weigh, 0)


def near_kernel(pairs_ref, q_ref, *refs):
    n = len(NEAR)
    qq, mbuf, lbuf, acc = refs[n : n + 4]
    kbuf, vbuf, sbuf = refs[n + 4 :]
    fill_keys(refs[:n], kbuf, vbuf)
    fill_queries(q_ref, qq)
    mbuf[...] = jnp.full(mbuf.shape, masked_score, f32)
    lbuf[...] = jnp.zeros(lbuf.shape, f32)
    acc[...] = jnp.zeros(acc.shape, f32)
    run_pairs(pairs_ref, 0, qq, kbuf, vbuf, sbuf, mbuf, lbuf, acc, None)


def far_kernel(pairs_ref, qq, m_ref, l_ref, acc_ref, *refs):
    n = len(FAR)
    out_ref = refs[n]
    kbuf, vbuf, sbuf, mbuf, lbuf, acc = refs[n + 1 :]
    fill_keys(refs[:n], kbuf, vbuf)
    mbuf[...] = m_ref[...]
    lbuf[...] = l_ref[...]
    acc[...] = acc_ref[...]
    run_pairs(pairs_ref, 1, qq, kbuf, vbuf, sbuf, mbuf, lbuf, acc, m_ref)
    for i in range(TEAM):
        logs = []
        for b in range(PER):
            q = i * PER + b
            total = jnp.sum(lbuf[q], axis=0, keepdims=True)
            some = total > 0.0
            safe = jnp.where(some, total, 1.0)
            logs.append(jnp.where(some, mbuf[q, :1, :] + jnp.log(safe), masked_score))
            out_ref[q, pl.ds(0, BLK), :] = (acc[q] * (1.0 / safe)).astype(bf16)
        value = jnp.concatenate(logs, axis=0)
        hi = value.astype(bf16).astype(f32)
        rest = value - hi
        mid = rest.astype(bf16).astype(f32)
        stats = jnp.concatenate([hi, mid, rest - mid, jnp.zeros((PER, WIDTH), f32)], axis=0)
        for b in range(PER):
            out_ref[i * PER + b, pl.ds(BLK, STATS), :] = stats.astype(bf16)


STATE = (
    jax.ShapeDtypeStruct((QB + 1, WIDTH, WIDTH), bf16),
    jax.ShapeDtypeStruct((QB + 1, 8, WIDTH), f32),
    jax.ShapeDtypeStruct((QB + 1, 8, WIDTH), f32),
    jax.ShapeDtypeStruct((QB + 1, BLK, WIDTH), f32),
)


def key_scratch(n):
    return [
        pltpu.VMEM((n * PER, BLK, WIDTH), bf16),
        pltpu.VMEM((n * PER, WIDTH, BLK), bf16),
        pltpu.VMEM((MAXP, BLK, WIDTH), f32),
    ]


def attend_near(pairs, q, kvs):
    smem = pl.BlockSpec(memory_space=pltpu.SMEM)
    vmem = pl.BlockSpec(memory_space=pltpu.VMEM)
    return pl.pallas_call(
        near_kernel,
        out_shape=STATE,
        in_specs=[smem] + [vmem] * (1 + len(kvs)),
        out_specs=(vmem,) * len(STATE),
        scratch_shapes=key_scratch(len(kvs)),
        compiler_params=pltpu.CompilerParams(vmem_limit_bytes=20 << 20),
        name="near",
    )(pairs, q, *kvs)


def attend_far(pairs, state, kvs):
    smem = pl.BlockSpec(memory_space=pltpu.SMEM)
    vmem = pl.BlockSpec(memory_space=pltpu.VMEM)
    return pl.pallas_call(
        far_kernel,
        out_shape=jax.ShapeDtypeStruct((QB, BLK + STATS, WIDTH), bf16),
        in_specs=[smem] + [vmem] * (len(state) + len(kvs)),
        out_specs=vmem,
        scratch_shapes=key_scratch(len(kvs)) + [pltpu.VMEM(s.shape, s.dtype) for s in STATE[1:]],
        compiler_params=pltpu.CompilerParams(vmem_limit_bytes=20 << 20),
        name="far",
    )(pairs, *state, *kvs)


def merge_kernel(place_ref, part_ref, *refs):
    w_refs = refs[:PER]
    own_ref, send_ref, log_ref, att = refs[PER:]
    x = place_ref[0]
    core = place_ref[1]
    half = BLK // 2
    row = lax.broadcasted_iota(jnp.int32, (PER, WIDTH), 0)
    for c in range(PER):
        values = []
        for i in range(TEAM):
            st = part_ref[i * PER + c, pl.ds(BLK, STATS), :].astype(f32)
            values.append(st[:PER] + st[PER : 2 * PER] + st[2 * PER : 3 * PER])
        top = functools.reduce(jnp.maximum, values)
        weights = [jnp.exp(v - top) for v in values]
        total = functools.reduce(jnp.add, weights)

        @pl.when(x == c)
        def _():
            log_ref[...] = top + jnp.log(total)

        inverse = 1.0 / total
        mixed = jnp.zeros((BLK, WIDTH), f32)
        for i in range(TEAM):
            mine = jnp.sum(jnp.where(row == x, weights[i] * inverse, 0.0), axis=0, keepdims=True)
            mixed = mixed + part_ref[i * PER + c, pl.ds(0, BLK), :].astype(f32) * mine
        turned = mixed.T
        for h in range(2):
            heads = [turned[h * BLK + k * half : h * BLK + (k + 1) * half] for k in range(2)]
            att[c, pl.ds(h * half, half), :] = jnp.concatenate(heads, axis=1).astype(bf16)
    y = jnp.dot(att[x], w_refs[0][...], preferred_element_type=f32)
    for k in range(1, PER):
        y = y + jnp.dot(att[(x - k) & (PER - 1)], w_refs[k][...], preferred_element_type=f32)
    own_ref[...] = jnp.where(core == 0, y[:half], y[half:])
    send_ref[...] = jnp.where(core == 0, y[half:], y[:half]).astype(bf16)


def merge(place, parts, w_all):
    smem = pl.BlockSpec(memory_space=pltpu.SMEM)
    vmem = pl.BlockSpec(memory_space=pltpu.VMEM)
    tile = (BLK // 2, w_all[0].shape[-1])
    return pl.pallas_call(
        merge_kernel,
        out_shape=(
            jax.ShapeDtypeStruct(tile, f32),
            jax.ShapeDtypeStruct(tile, bf16),
            jax.ShapeDtypeStruct((PER, WIDTH), f32),
        ),
        in_specs=[smem, vmem] + [vmem] * PER,
        out_specs=(vmem, vmem, vmem),
        scratch_shapes=[pltpu.VMEM((PER, BLK, WIDTH), bf16)],
        compiler_params=pltpu.CompilerParams(vmem_limit_bytes=12 << 20),
        name="merge",
    )(place, parts, *w_all)


def up_pairs(step):
    return [(i, i + 1) for i in range(step - 1, RING - 1)]


def down_pairs(step):
    far = RING // 2 - 1
    return [((r - step + 1) % RING, (r - step) % RING) for r in range(far)]


def local(tokens, w_query, w_key, w_value, w_out, chosen):
    zh = lax.axis_index("zh")
    mine = lax.axis_index(("zl", "y"))
    device = zh * TEAM + mine
    positions = device * ROWS + jnp.arange(ROWS)
    half = HEAD_DIM // 2
    inverse = rotary_base ** (-jnp.arange(half, dtype=f32) / half)
    angles = positions.astype(f32)[:, None] * jnp.tile(inverse, 2 * WIDTH // HEAD_DIM)[None, :]
    sign = jnp.where((jnp.arange(WIDTH) & (HEAD_DIM - 1)) < half, -1.0, 1.0).astype(f32)
    q8, kv, pairs = project(
        jnp.stack([zh, mine]),
        tokens,
        w_query,
        w_key,
        w_value,
        chosen.T,
        jnp.cos(angles),
        jnp.sin(angles) * sign[None, :],
    )
    slots = [kv] + [None] * (RING - 1)
    up = down = kv
    for s in range(1, RING // 2 + 1):
        up = lax.ppermute(up, "zh", up_pairs(s))
        slots[s] = up
        if s < RING // 2:
            down = lax.ppermute(down, "zh", down_pairs(s))
            slots[RING - s] = down
    q_team = lax.all_to_all(q8, ("zl", "y"), 0, 0, tiled=True)
    w_all = [w_out]
    for k in range(1, PER):
        w_all.append(lax.ppermute(w_out, "x", [(i, (i + k) % PER) for i in range(PER)]))
    state = attend_near(pairs, q_team, [slots[i] for i in NEAR])
    parts = attend_far(pairs, state, [slots[i] for i in FAR])
    parts = lax.all_to_all(parts, ("zl", "y", "x"), 0, 0, tiled=True)
    place = jnp.stack([lax.axis_index("x"), lax.axis_index("c")])
    own, send, logs = merge(place, parts, w_all)
    received = lax.ppermute(send, "c", [(0, 1), (1, 0)])
    output = (own + received.astype(f32)).astype(bf16)
    log_sums = jnp.transpose(logs.reshape(PER, 2, 2, BLK // 2), (2, 0, 1, 3)).reshape(2, ROWS)
    return (output, log_sums)


def solution(mesh):
    fine = Mesh(mesh.devices.reshape(8, 2, 4, 4, 2), ("zh", "zl", "y", "x", "c"))
    kv = ("zh", "zl", "y")
    tp = ("x", "c")
    placed = (P(kv, None), P(None, tp), P(None, tp), P(None, tp), P(tp, None), P())
    return jax.shard_map(
        local,
        mesh=fine,
        in_specs=placed,
        out_specs=(P(kv + tp, None), P(tp, kv)),
        check_vma=False,
    )
```

time: 96.2 us -> 102 us (1.060)
  the two profiles are of different devices: /device:TPU:192 before, /device:TPU:1 now
where the time goes in v5:
time: 102 us; the launch traced here: 101 us
  starting transfers between devices  57.1 us (56%)
  waiting for transfers between devices  29.1 us (29%)
  Pallas kernels  11.2 us (11%)
  local copies, waits for them, and re-layouts  1.56 us (2%)
  other arithmetic  1.38 us (1%)
    ppermute x3, starting transfers between devices, local(): down = lax.ppermute(down, 'zh', down_pairs(s))  22.4 us
    ppermute x3, waiting for transfers between devices, local(): lax.ppermute(w_out, 'x', [(i, (i + k) % PER) for i in range(PER)])  21.4 us
    ppermute x3, starting transfers between devices, local(): lax.ppermute(w_out, 'x', [(i, (i + k) % PER) for i in range(PER)])  10.5 us
    ppermute x3, waiting for transfers between devices, local(): down = lax.ppermute(down, 'zh', down_pairs(s))  7.53 us
    all_to_all x1, starting transfers between devices, local(): parts = lax.all_to_all(parts, ('zl', 'y', 'x'), 0, 0, tiled=True)  7.06 us
    ppermute x4, starting transfers between devices, local(): up = lax.ppermute(up, 'zh', up_pairs(s))  6.89 us
    all_to_all x1, starting transfers between devices, local(): q_team = lax.all_to_all(q8, ('zl', 'y'), 0, 0, tiled=True)  6.38 us
    pallas_call x1, Pallas kernels, project(): pl.pallas_call(project_kernel, out_shape=(jax.ShapeDtypeStruct((TEAM, ROW...  4.31 us
  transfers between devices with their start and end apart: 13, of which 5 were waited for; matrix products, arithmetic and copies ran while one was open for 1% of the time, Pallas kernels for 3%

profile of v5, /device:TPU:1, one launch (start us, length us, event | category | flops | bytes accessed | tf_op | source)
XLA Modules:
  0.0 101.3 jit_solution(9119759321973070734)
XLA Ops:
  0.7 0.1 mul.36
  0.8 0.1 pad_add_fusion.1.place_ref
  0.8 0.5 fusion
  1.4 0.0 copy-start.1
  1.4 0.7 copy-done.1
  2.1 4.3 %project.1 = (bf16[8,256,128]{2,1,0:T(8,128)(2,1)}, bf16[512,128]{1,0:T(8,128)(2,1)S(1)}, s32[4,512]{1,0:T(4,128)S(1)}) custom-call(s32[2]{0:T(128)S(1)} %pad_add_fusion.1.place_ref, bf16[256,2048]{1,0:T(8,128)(2,1)} %x_hbm.1, bf16[2048,128]{1,0:T(8,128)(2,1)} %wq_hbm.1, bf16[2048,128]{1,0:T(8,128)(2,1)} %wk_hbm.1, bf16[2048,128]{1,0:T(8,128)(2,1)} %wv_hbm.1, ...), custom_call_target="tpu_custom_call" | custom-call | tf_op jit(solution)/shard_map/project/pallas_call | solution.py:105
  6.4 6.4 %all-to-all-start = ((bf16[8,256,128]{2,1,0:T(8,128)(2,1)}), bf16[8,256,128]{2,1,0:T(8,128)(2,1)S(1)}, u32[]{:S(2)}, u32[]{:S(2)}) async-start(bf16[8,256,128]{2,1,0:T(8,128)(2,1)} %get-tuple-element.13), calls=%async_computation | async-start | bytes 1048576 | tf_op jit(solution)/shard_map/all_to_all | solution.py:367
  12.8 4.9 %collective-permute-start = (bf16[512,128]{1,0:T(8,128)(2,1)S(1)}, bf16[512,128]{1,0:T(8,128)(2,1)S(1)}, u32[]{:S(2)}, u32[]{:S(2)}) collective-permute-start(bf16[512,128]{1,0:T(8,128)(2,1)S(1)} %get-tuple-element.14.refs_0_), channel_id=1, source_target_pairs={{0,64},{64,128},{128,192},{192,256},{256,320},{320,384},{384,448},... | collective-permute-start | bytes 393224 | tf_op jit(solution)/shard_map/ppermute | solution.py:362
  17.7 7.1 %collective-permute-start.2 = (bf16[512,128]{1,0:T(8,128)(2,1)S(1)}, bf16[512,128]{1,0:T(8,128)(2,1)S(1)}, u32[]{:S(2)}, u32[]{:S(2)}) collective-permute-start(bf16[512,128]{1,0:T(8,128)(2,1)S(1)} %get-tuple-element.14.refs_0_), channel_id=1, source_target_pairs={{0,448},{64,0},{128,64},{1,449},{65,1},{129,65},{2,450},{66,2},{13... | collective-permute-start | bytes 393224 | tf_op jit(solution)/shard_map/ppermute | solution.py:365
  24.8 0.7 collective-permute-start.1
  25.5 3.0 %collective-permute-done.2.refs_4_ = bf16[512,128]{1,0:T(8,128)(2,1)S(1)} collective-permute-done((bf16[512,128]{1,0:T(8,128)(2,1)S(1)}, bf16[512,128]{1,0:T(8,128)(2,1)S(1)}, u32[]{:S(2)}, u32[]{:S(2)}) %collective-permute-start.2) | collective-permute-done | bytes 131104 | tf_op jit(solution)/shard_map/ppermute | solution.py:365
  28.5 9.0 %collective-permute-start.3 = (bf16[512,128]{1,0:T(8,128)(2,1)S(1)}, bf16[512,128]{1,0:T(8,128)(2,1)S(1)}, u32[]{:S(2)}, u32[]{:S(2)}) collective-permute-start(bf16[512,128]{1,0:T(8,128)(2,1)S(1)} %collective-permute-done.2.refs_4_), channel_id=1, source_target_pairs={{448,384},{0,448},{64,0},{449,385},{1,449},{65,1},{450,386},{2,450... | collective-permute-start | bytes 393224 | tf_op jit(solution)/shard_map/ppermute | solution.py:365
  37.5 0.7 collective-permute-start.4
  38.2 4.4 %collective-permute-done.3.refs_3_ = bf16[512,128]{1,0:T(8,128)(2,1)S(1)} collective-permute-done((bf16[512,128]{1,0:T(8,128)(2,1)S(1)}, bf16[512,128]{1,0:T(8,128)(2,1)S(1)}, u32[]{:S(2)}, u32[]{:S(2)}) %collective-permute-start.3) | collective-permute-done | bytes 131104 | tf_op jit(solution)/shard_map/ppermute | solution.py:365
  42.6 6.4 %collective-permute-start.6 = (bf16[512,128]{1,0:T(8,128)(2,1)S(1)}, bf16[512,128]{1,0:T(8,128)(2,1)S(1)}, u32[]{:S(2)}, u32[]{:S(2)}) collective-permute-start(bf16[512,128]{1,0:T(8,128)(2,1)S(1)} %collective-permute-done.3.refs_3_), channel_id=1, source_target_pairs={{384,320},{448,384},{0,448},{385,321},{449,385},{1,449},{386,322},... | collective-permute-start | bytes 393224 | tf_op jit(solution)/shard_map/ppermute | solution.py:365
  49.0 0.7 collective-permute-start.5
  49.7 3.2 %near.1 = (bf16[33,128,128]{2,1,0:T(8,128)(2,1)S(1)}, f32[33,8,128]{2,1,0:T(8,128)S(1)}, f32[33,8,128]{2,1,0:T(8,128)S(1)}, f32[33,64,128]{2,1,0:T(8,128)S(1)}) custom-call(s32[4,512]{1,0:T(4,128)S(1)} %get-tuple-element.12.pairs_ref, bf16[8,256,128]{2,1,0:T(8,128)(2,1)S(1)} %all-to-all-done.q_ref, bf16[512,128]{1,0:T(8,128)(2,1)S(1)} %get-tuple-element.14.refs_0_, ...), custom_call_target="tpu_custom_call" | custom-call | tf_op jit(solution)/shard_map/near/pallas_call | solution.py:251
  52.9 0.0 collective-permute-done.6.refs_2_
  52.9 2.0 %far.1 = bf16[32,80,128]{2,1,0:T(8,128)(2,1)} custom-call(s32[4,512]{1,0:T(4,128)S(1)} %get-tuple-element.12.pairs_ref, bf16[33,128,128]{2,1,0:T(8,128)(2,1)S(1)} %get-tuple-element.15.qq, f32[33,8,128]{2,1,0:T(8,128)S(1)} %get-tuple-element.16.m_ref, f32[33,8,128]{2,1,0:T(8,128)S(1)} %get-tuple-element.17.l_ref, ...), custom_call_target="tpu_custom_call" | custom-call | tf_op jit(solution)/shard_map/far/pallas_call | solution.py:265
  54.9 7.1 %all-to-all-start.1 = ((bf16[32,80,128]{2,1,0:T(8,128)(2,1)}), bf16[32,80,128]{2,1,0:T(8,128)(2,1)S(1)}, u32[]{:S(2)}, u32[]{:S(2)}) async-start(bf16[32,80,128]{2,1,0:T(8,128)(2,1)} %far.1), calls=%async_computation.1 | async-start | bytes 1310720 | tf_op jit(solution)/shard_map/all_to_all | solution.py:373
  61.9 3.1 %collective-permute-start.7 = (bf16[128,2048]{1,0:T(8,128)(2,1)S(1)}, bf16[128,2048]{1,0:T(8,128)(2,1)S(1)}, u32[]{:S(2)}, u32[]{:S(2)}) collective-permute-start(bf16[128,2048]{1,0:T(8,128)(2,1)S(1)} %copy-done), channel_id=1, source_target_pairs={{0,2},{2,4},{4,6},{6,0},{1,3},{3,5},{5,7},{7,1},{8,10},{10,12},{12... | collective-permute-start | bytes 1572872 | tf_op jit(solution)/shard_map/ppermute | solution.py:370
  65.1 4.3 %collective-permute-start.8 = (bf16[128,2048]{1,0:T(8,128)(2,1)S(1)}, bf16[128,2048]{1,0:T(8,128)(2,1)S(1)}, u32[]{:S(2)}, u32[]{:S(2)}) collective-permute-start(bf16[128,2048]{1,0:T(8,128)(2,1)S(1)} %copy-done), channel_id=1, source_target_pairs={{0,4},{2,6},{4,0},{6,2},{1,5},{3,7},{5,1},{7,3},{8,12},{10,14},{12... | collective-permute-start | bytes 1572872 | tf_op jit(solution)/shard_map/ppermute | solution.py:370
  69.4 3.1 %collective-permute-start.9 = (bf16[128,2048]{1,0:T(8,128)(2,1)S(1)}, bf16[128,2048]{1,0:T(8,128)(2,1)S(1)}, u32[]{:S(2)}, u32[]{:S(2)}) collective-permute-start(bf16[128,2048]{1,0:T(8,128)(2,1)S(1)} %copy-done), channel_id=1, source_target_pairs={{0,6},{2,0},{4,2},{6,4},{1,7},{3,1},{5,3},{7,5},{8,14},{10,8},{12,... | collective-permute-start | bytes 1572872 | tf_op jit(solution)/shard_map/ppermute | solution.py:370
  72.5 0.1 pad_add_fusion.place_ref
  72.6 11.1 %collective-permute-done.7.refs_1_ = bf16[128,2048]{1,0:T(8,128)(2,1)S(1)} collective-permute-done((bf16[128,2048]{1,0:T(8,128)(2,1)S(1)}, bf16[128,2048]{1,0:T(8,128)(2,1)S(1)}, u32[]{:S(2)}, u32[]{:S(2)}) %collective-permute-start.7) | collective-permute-done | bytes 524320 | tf_op jit(solution)/shard_map/ppermute | solution.py:370
  83.7 10.2 %collective-permute-done.8.refs_2_ = bf16[128,2048]{1,0:T(8,128)(2,1)S(1)} collective-permute-done((bf16[128,2048]{1,0:T(8,128)(2,1)S(1)}, bf16[128,2048]{1,0:T(8,128)(2,1)S(1)}, u32[]{:S(2)}, u32[]{:S(2)}) %collective-permute-start.8) | collective-permute-done | bytes 524320 | tf_op jit(solution)/shard_map/ppermute | solution.py:370
  93.9 1.8 %merge.1 = (f32[32,2048]{1,0:T(8,128)S(1)}, bf16[32,2048]{1,0:T(8,128)(2,1)S(1)}, f32[4,128]{1,0:T(4,128)S(1)}) custom-call(s32[2]{0:T(128)S(1)} %pad_add_fusion.place_ref, bf16[32,80,128]{2,1,0:T(8,128)(2,1)S(1)} %all-to-all-done.1.part_ref, bf16[128,2048]{1,0:T(8,128)(2,1)S(1)} %copy-done, bf16[128,2048]{1,0:T(8,128)(2,1)S(1)} %collective-permute-done.7.refs_1_, ...), custom_call_target="tpu_custom_call" | custom-call | tf_op jit(solution)/shard_map/merge/pallas_call | solution.py:316
  95.7 3.9 %collective-permute-start.10 = (bf16[32,2048]{1,0:T(8,128)(2,1)S(1)}, bf16[32,2048]{1,0:T(8,128)(2,1)S(1)}, u32[]{:S(2)}, u32[]{:S(2)}) collective-permute-start(bf16[32,2048]{1,0:T(8,128)(2,1)S(1)} %get-tuple-element.20), channel_id=1, source_target_pairs={{0,1},{1,0},{2,3},{3,2},{4,5},{5,4},{6,7},{7,6},{8,9},{9,8},{10,11... | collective-permute-start | bytes 393224 | tf_op jit(solution)/shard_map/ppermute | solution.py:376
  99.6 0.1 reshape.28
  99.7 0.7 reshape.29
  100.4 0.2 collective-permute-done.10
  100.6 0.7 add_convert_fusion
  (14 shorter events, 0.1 us)
Async XLA Ops:
  1.4 0.7 copy-start.1
  6.4 43.3 %all-to-all-start = ((bf16[8,256,128]{2,1,0:T(8,128)(2,1)}), bf16[8,256,128]{2,1,0:T(8,128)(2,1)S(1)}, u32[]{:S(2)}, u32[]{:S(2)}) async-start(bf16[8,256,128]{2,1,0:T(8,128)(2,1)} %get-tuple-element.13), calls=%async_computation | async-start | bytes 1048576 | tf_op jit(solution)/shard_map/all_to_all | solution.py:367
  12.8 12.0 %collective-permute-start = (bf16[512,128]{1,0:T(8,128)(2,1)S(1)}, bf16[512,128]{1,0:T(8,128)(2,1)S(1)}, u32[]{:S(2)}, u32[]{:S(2)}) collective-permute-start(bf16[512,128]{1,0:T(8,128)(2,1)S(1)} %get-tuple-element.14.refs_0_), channel_id=1, source_target_pairs={{0,64},{64,128},{128,192},{192,256},{256,320},{320,384},{384,448},... | collective-permute-start | bytes 393224 | tf_op jit(solution)/shard_map/ppermute | solution.py:362
  17.7 10.8 %collective-permute-start.2 = (bf16[512,128]{1,0:T(8,128)(2,1)S(1)}, bf16[512,128]{1,0:T(8,128)(2,1)S(1)}, u32[]{:S(2)}, u32[]{:S(2)}) collective-permute-start(bf16[512,128]{1,0:T(8,128)(2,1)S(1)} %get-tuple-element.14.refs_0_), channel_id=1, source_target_pairs={{0,448},{64,0},{128,64},{1,449},{65,1},{129,65},{2,450},{66,2},{13... | collective-permute-start | bytes 393224 | tf_op jit(solution)/shard_map/ppermute | solution.py:365
  24.8 12.7 %collective-permute-start.1 = (bf16[512,128]{1,0:T(8,128)(2,1)S(1)}, bf16[512,128]{1,0:T(8,128)(2,1)S(1)}, u32[]{:S(2)}, u32[]{:S(2)}) collective-permute-start(bf16[512,128]{1,0:T(8,128)(2,1)S(1)} %collective-permute-done.refs_1_), channel_id=1, source_target_pairs={{64,128},{128,192},{192,256},{256,320},{320,384},{384,448},{65,129... | collective-permute-start | bytes 393224 | tf_op jit(solution)/shard_map/ppermute | solution.py:362
  28.5 14.1 %collective-permute-start.3 = (bf16[512,128]{1,0:T(8,128)(2,1)S(1)}, bf16[512,128]{1,0:T(8,128)(2,1)S(1)}, u32[]{:S(2)}, u32[]{:S(2)}) collective-permute-start(bf16[512,128]{1,0:T(8,128)(2,1)S(1)} %collective-permute-done.2.refs_4_), channel_id=1, source_target_pairs={{448,384},{0,448},{64,0},{449,385},{1,449},{65,1},{450,386},{2,450... | collective-permute-start | bytes 393224 | tf_op jit(solution)/shard_map/ppermute | solution.py:365
  37.5 11.5 %collective-permute-start.4 = (bf16[512,128]{1,0:T(8,128)(2,1)S(1)}, bf16[512,128]{1,0:T(8,128)(2,1)S(1)}, u32[]{:S(2)}, u32[]{:S(2)}) collective-permute-start(bf16[512,128]{1,0:T(8,128)(2,1)S(1)} %collective-permute-done.1.refs_2_), channel_id=1, source_target_pairs={{128,192},{192,256},{256,320},{320,384},{384,448},{129,193},{193,2... | collective-permute-start | bytes 393224 | tf_op jit(solution)/shard_map/ppermute | solution.py:362
  42.6 10.3 %collective-permute-start.6 = (bf16[512,128]{1,0:T(8,128)(2,1)S(1)}, bf16[512,128]{1,0:T(8,128)(2,1)S(1)}, u32[]{:S(2)}, u32[]{:S(2)}) collective-permute-start(bf16[512,128]{1,0:T(8,128)(2,1)S(1)} %collective-permute-done.3.refs_3_), channel_id=1, source_target_pairs={{384,320},{448,384},{0,448},{385,321},{449,385},{1,449},{386,322},... | collective-permute-start | bytes 393224 | tf_op jit(solution)/shard_map/ppermute | solution.py:365
  49.0 3.9 %collective-permute-start.5 = (bf16[512,128]{1,0:T(8,128)(2,1)S(1)}, bf16[512,128]{1,0:T(8,128)(2,1)S(1)}, u32[]{:S(2)}, u32[]{:S(2)}) collective-permute-start(bf16[512,128]{1,0:T(8,128)(2,1)S(1)} %collective-permute-done.4.refs_0_), channel_id=1, source_target_pairs={{192,256},{256,320},{320,384},{384,448},{193,257},{257,321},{321,3... | collective-permute-start | bytes 393224 | tf_op jit(solution)/shard_map/ppermute | solution.py:362
  54.9 7.1 %copy-start = (bf16[128,2048]{1,0:T(8,128)(2,1)S(1)}, bf16[128,2048]{1,0:T(8,128)(2,1)}, u32[]{:S(2)}) copy-start(bf16[128,2048]{1,0:T(8,128)(2,1)} %refs_0_.1) | copy-start | bytes 1572868
  54.9 39.1 %all-to-all-start.1 = ((bf16[32,80,128]{2,1,0:T(8,128)(2,1)}), bf16[32,80,128]{2,1,0:T(8,128)(2,1)S(1)}, u32[]{:S(2)}, u32[]{:S(2)}) async-start(bf16[32,80,128]{2,1,0:T(8,128)(2,1)} %far.1), calls=%async_computation.1 | async-start | bytes 1310720 | tf_op jit(solution)/shard_map/all_to_all | solution.py:373
  61.9 21.8 %collective-permute-start.7 = (bf16[128,2048]{1,0:T(8,128)(2,1)S(1)}, bf16[128,2048]{1,0:T(8,128)(2,1)S(1)}, u32[]{:S(2)}, u32[]{:S(2)}) collective-permute-start(bf16[128,2048]{1,0:T(8,128)(2,1)S(1)} %copy-done), channel_id=1, source_target_pairs={{0,2},{2,4},{4,6},{6,0},{1,3},{3,5},{5,7},{7,1},{8,10},{10,12},{12... | collective-permute-start | bytes 1572872 | tf_op jit(solution)/shard_map/ppermute | solution.py:370
  65.1 28.8 %collective-permute-start.8 = (bf16[128,2048]{1,0:T(8,128)(2,1)S(1)}, bf16[128,2048]{1,0:T(8,128)(2,1)S(1)}, u32[]{:S(2)}, u32[]{:S(2)}) collective-permute-start(bf16[128,2048]{1,0:T(8,128)(2,1)S(1)} %copy-done), channel_id=1, source_target_pairs={{0,4},{2,6},{4,0},{6,2},{1,5},{3,7},{5,1},{7,3},{8,12},{10,14},{12... | collective-permute-start | bytes 1572872 | tf_op jit(solution)/shard_map/ppermute | solution.py:370
  69.4 24.5 %collective-permute-start.9 = (bf16[128,2048]{1,0:T(8,128)(2,1)S(1)}, bf16[128,2048]{1,0:T(8,128)(2,1)S(1)}, u32[]{:S(2)}, u32[]{:S(2)}) collective-permute-start(bf16[128,2048]{1,0:T(8,128)(2,1)S(1)} %copy-done), channel_id=1, source_target_pairs={{0,6},{2,0},{4,2},{6,4},{1,7},{3,1},{5,3},{7,5},{8,14},{10,8},{12,... | collective-permute-start | bytes 1572872 | tf_op jit(solution)/shard_map/ppermute | solution.py:370
  95.7 4.8 %collective-permute-start.10 = (bf16[32,2048]{1,0:T(8,128)(2,1)S(1)}, bf16[32,2048]{1,0:T(8,128)(2,1)S(1)}, u32[]{:S(2)}, u32[]{:S(2)}) collective-permute-start(bf16[32,2048]{1,0:T(8,128)(2,1)S(1)} %get-tuple-element.20), channel_id=1, source_target_pairs={{0,1},{1,0},{2,3},{3,2},{4,5},{5,4},{6,7},{7,6},{8,9},{9,8},{10,11... | collective-permute-start | bytes 393224 | tf_op jit(solution)/shard_map/ppermute | solution.py:376

commit v6 on v5

--- a/solution.py
+++ b/solution.py
@@ -31,7 +31,7 @@
 bf16 = jnp.bfloat16
 
 
-def pair_lists(chosen_t, zh, mine, pairs_ref):
+def split_lists(chosen_t, zh, mine):
     i32 = jnp.int32
     rolled = pltpu.roll(chosen_t, (NBLK - zh * QB) & (NBLK - 1), 1)[:, :WIDTH]
     lists = rolled.astype(f32).T[:QB].astype(i32)
@@ -41,35 +41,46 @@
     order = jnp.where(far, slot - FAR[0], jnp.where(slot > FAR[-1], slot - len(FAR), slot))
     block = lax.broadcasted_iota(i32, (QB, SEL), 0)
     code = (block * 64 + order * PER + (lists & (PER - 1))).astype(f32)
+    return (here & ~far, here & far), code
+
+
+def pair_list(lists, kind, pairs_ref):
+    i32 = jnp.int32
+    wanted, code = lists[0][kind], lists[1]
     earlier = lax.broadcasted_iota(i32, (QB, QB), 1) < lax.broadcasted_iota(i32, (QB, QB), 0)
     before = lax.broadcasted_iota(i32, (SEL, SEL), 0) < lax.broadcasted_iota(i32, (SEL, SEL), 1)
     index = lax.broadcasted_iota(i32, (QB, MAXP), 1).astype(f32)
     row = lax.broadcasted_iota(i32, (1, MAXP), 1).astype(f32)
-    for k, wanted in enumerate((here & ~far, here & far)):
-        one = jnp.where(wanted, 1.0, 0.0)
-        inside = jnp.dot(jnp.where(earlier, 1.0, 0.0), one, preferred_element_type=f32)
-        sums = jnp.sum(one, axis=0, keepdims=True)
-        base = jnp.dot(sums, jnp.where(before, 1.0, 0.0), preferred_element_type=f32)
-        place = jnp.where(wanted, inside + base, -1.0)
-        picked = jnp.zeros((QB, MAXP), f32)
-        for j in range(SEL):
-            picked = picked + jnp.where(place[:, j : j + 1] == index, code[:, j : j + 1], 0.0)
-        count = jnp.sum(sums, axis=1, keepdims=True)
-        pairs = jnp.where(row < count, jnp.sum(picked, axis=0, keepdims=True), float(QB * 64))
-        pairs_ref[pl.ds(k, 1), :] = pairs.astype(i32)
-        trips = (count.astype(i32) + (UNROLL - 1)) >> UNROLL_BITS
-        pairs_ref[pl.ds(2 + k, 1), :] = jnp.broadcast_to(trips, (1, MAXP))
-
-
-def project_kernel(
-    place_ref, x_hbm, wq_hbm, wk_hbm, wv_hbm, chosen_ref, cos_ref, sin_ref, q_ref, kv_ref, pairs_ref, x_buf, w_buf, sems
-):
-    copies = [pltpu.make_async_copy(x_hbm, x_buf, sems.at[0])]
-    for i, w in enumerate((wk_hbm, wv_hbm, wq_hbm)):
-        copies.append(pltpu.make_async_copy(w, w_buf.at[i], sems.at[i + 1]))
+    one = jnp.where(wanted, 1.0, 0.0)
+    inside = jnp.dot(jnp.where(earlier, 1.0, 0.0), one, preferred_element_type=f32)
+    sums = jnp.sum(one, axis=0, keepdims=True)
+    base = jnp.dot(sums, jnp.where(before, 1.0, 0.0), preferred_element_type=f32)
+    place = jnp.where(wanted, inside + base, -1.0)
+    picked = jnp.zeros((QB, MAXP), f32)
+    for j in range(SEL):
+        picked = picked + jnp.where(place[:, j : j + 1] == index, code[:, j : j + 1], 0.0)
+    count = jnp.sum(sums, axis=1, keepdims=True)
+    pairs = jnp.where(row < count, jnp.sum(picked, axis=0, keepdims=True), float(QB * 64))
+    pairs_ref[pl.ds(kind, 1), :] = pairs.astype(i32)
+    trips = (count.astype(i32) + (UNROLL - 1)) >> UNROLL_BITS
+    pairs_ref[pl.ds(2 + kind, 1), :] = jnp.broadcast_to(trips, (1, MAXP))
+
+
+def project_kernel(place_ref, *refs):
+    x_hbm, wq_hbm, wk_hbm, wv_hbm, chosen_hbm, cos_ref, sin_ref = refs[:7]
+    q_hbm, kv_ref, pairs_ref = refs[7:10]
+    x_buf, wq_buf, wkv_buf, chosen_buf, q_buf, sems = refs[10:]
+    sources = (
+        (chosen_hbm, chosen_buf),
+        (x_hbm, x_buf),
+        (wq_hbm, wq_buf),
+        (wk_hbm, wkv_buf.at[:, pl.ds(0, WIDTH)]),
+        (wv_hbm, wkv_buf.at[:, pl.ds(WIDTH, WIDTH)]),
+    )
+    copies = [pltpu.make_async_copy(a, b, sems.at[i]) for i, (a, b) in enumerate(sources)]
+    sends = [pltpu.make_async_copy(q_buf, q_hbm.at[i], sems.at[len(copies) + i]) for i in range(TEAM)]
     for copy in copies:
         copy.start()
-    pair_lists(chosen_ref[...], place_ref[0], place_ref[1], pairs_ref)
     cos = cos_ref[...]
     sin = sin_ref[...]
     lane = lax.broadcasted_iota(jnp.int32, (ROWS, WIDTH), 1)
@@ -80,25 +91,31 @@
         return t * cos + partner * sin
 
     copies[0].wait()
+    lists = split_lists(chosen_buf[...], place_ref[0], place_ref[1])
+    pair_list(lists, 0, pairs_ref)
     copies[1].wait()
-    x = x_buf[...]
-    k = jnp.dot(x, w_buf[0], preferred_element_type=f32)
-    kv_ref[pl.ds(0, ROWS), :] = turned(k).astype(bf16)
     copies[2].wait()
-    v = jnp.dot(x, w_buf[1], preferred_element_type=f32)
-    for p in range(ROWS // WIDTH):
-        kv_ref[pl.ds(ROWS + p * WIDTH, WIDTH), :] = v[p * WIDTH : (p + 1) * WIDTH].T.astype(bf16)
-    copies[3].wait()
-    q = jnp.dot(x, w_buf[2], preferred_element_type=f32)
+    q = jnp.dot(x_buf[...], wq_buf[...], preferred_element_type=f32)
     q = turned(q) * (HEAD_DIM**-0.5)
     for p in range(ROWS // WIDTH):
-        flipped = q[p * WIDTH : (p + 1) * WIDTH].T.astype(bf16)
-        for i in range(TEAM):
-            q_ref[i, pl.ds(p * WIDTH, WIDTH), :] = flipped
+        q_buf[pl.ds(p * WIDTH, WIDTH), :] = q[p * WIDTH : (p + 1) * WIDTH].T.astype(bf16)
+    for send in sends:
+        send.start()
+    copies[3].wait()
+    copies[4].wait()
+    kv = jnp.dot(x_buf[...], wkv_buf[...], preferred_element_type=f32)
+    pair_list(lists, 1, pairs_ref)
+    kv_ref[pl.ds(0, ROWS), :] = turned(kv[:, :WIDTH]).astype(bf16)
+    for p in range(ROWS // WIDTH):
+        kv_ref[pl.ds(ROWS + p * WIDTH, WIDTH), :] = kv[p * WIDTH : (p + 1) * WIDTH, WIDTH:].T.astype(bf16)
+    for send in sends:
+        send.wait()
 
 
 def project(place, x, wq, wk, wv, chosen_t, cos, sin):
-    x, wq, wk, wv = (pltpu.with_memory_space_constraint(a, pltpu.HBM) for a in (x, wq, wk, wv))
+    x, wq, wk, wv, chosen_t = (
+        pltpu.with_memory_space_constraint(a, pltpu.HBM) for a in (x, wq, wk, wv, chosen_t)
+    )
     hbm = pl.BlockSpec(memory_space=pltpu.HBM)
     smem = pl.BlockSpec(memory_space=pltpu.SMEM)
     vmem = pl.BlockSpec(memory_space=pltpu.VMEM)
@@ -109,12 +126,15 @@
             jax.ShapeDtypeStruct((2 * ROWS, WIDTH), bf16),
             jax.ShapeDtypeStruct((4, MAXP), jnp.int32),
         ),
-        in_specs=[smem] + [hbm] * 4 + [vmem] * 3,
-        out_specs=(vmem, vmem, vmem),
+        in_specs=[smem] + [hbm] * 5 + [vmem] * 2,
+        out_specs=(pl.BlockSpec(memory_space=pl.ANY), vmem, vmem),
         scratch_shapes=[
             pltpu.VMEM(x.shape, bf16),
-            pltpu.VMEM((3,) + wq.shape, bf16),
-            pltpu.SemaphoreType.DMA((4,)),
+            pltpu.VMEM(wq.shape, bf16),
+            pltpu.VMEM((wk.shape[0], 2 * WIDTH), bf16),
+            pltpu.VMEM(chosen_t.shape, jnp.int32),
+            pltpu.VMEM((ROWS, WIDTH), bf16),
+            pltpu.SemaphoreType.DMA((5 + TEAM,)),
         ],
         compiler_params=pltpu.CompilerParams(vmem_limit_bytes=12 << 20),
         name="project",
@@ -204,13 +224,14 @@
 
 def far_kernel(pairs_ref, qq, m_ref, l_ref, acc_ref, *refs):
     n = len(FAR)
-    out_ref = refs[n]
-    kbuf, vbuf, sbuf, mbuf, lbuf, acc = refs[n + 1 :]
+    out_hbm = refs[n]
+    kbuf, vbuf, sbuf, mbuf, lbuf, acc, out_buf, sems = refs[n + 1 :]
     fill_keys(refs[:n], kbuf, vbuf)
     mbuf[...] = m_ref[...]
     lbuf[...] = l_ref[...]
     acc[...] = acc_ref[...]
     run_pairs(pairs_ref, 1, qq, kbuf, vbuf, sbuf, mbuf, lbuf, acc, m_ref)
+    sends = []
     for i in range(TEAM):
         logs = []
         for b in range(PER):
@@ -219,14 +240,19 @@
             some = total > 0.0
             safe = jnp.where(some, total, 1.0)
             logs.append(jnp.where(some, mbuf[q, :1, :] + jnp.log(safe), masked_score))
-            out_ref[q, pl.ds(0, BLK), :] = (acc[q] * (1.0 / safe)).astype(bf16)
+            out_buf[q, pl.ds(0, BLK), :] = (acc[q] * (1.0 / safe)).astype(bf16)
         value = jnp.concatenate(logs, axis=0)
         hi = value.astype(bf16).astype(f32)
         rest = value - hi
         mid = rest.astype(bf16).astype(f32)
         stats = jnp.concatenate([hi, mid, rest - mid, jnp.zeros((PER, WIDTH), f32)], axis=0)
         for b in range(PER):
-            out_ref[i * PER + b, pl.ds(BLK, STATS), :] = stats.astype(bf16)
+            out_buf[i * PER + b, pl.ds(BLK, STATS), :] = stats.astype(bf16)
+        span = pl.ds(i * PER, PER)
+        sends.append(pltpu.make_async_copy(out_buf.at[span], out_hbm.at[span], sems.at[i]))
+        sends[-1].start()
+    for send in sends:
+        send.wait()
 
 
 STATE = (
@@ -266,8 +292,10 @@
         far_kernel,
         out_shape=jax.ShapeDtypeStruct((QB, BLK + STATS, WIDTH), bf16),
         in_specs=[smem] + [vmem] * (len(state) + len(kvs)),
-        out_specs=vmem,
-        scratch_shapes=key_scratch(len(kvs)) + [pltpu.VMEM(s.shape, s.dtype) for s in STATE[1:]],
+        out_specs=pl.BlockSpec(memory_space=pl.ANY),
+        scratch_shapes=key_scratch(len(kvs))
+        + [pltpu.VMEM(s.shape, s.dtype) for s in STATE[1:]]
+        + [pltpu.VMEM((QB, BLK + STATS, WIDTH), bf16), pltpu.SemaphoreType.DMA((TEAM,))],
         compiler_params=pltpu.CompilerParams(vmem_limit_bytes=20 << 20),
         name="far",
     )(pairs, *state, *kvs)

time: 102 us -> 100 us (0.980)
  transfers between devices with their start and end apart: 13 -> 13, of which waited for: 5 -> 6; matrix products, arithmetic and copies ran while one was open for 1% -> 1% of each run, Pallas kernels for 3% -> 3%
where the time goes in v6:
time: 100 us; the launch traced here: 99.8 us
  starting transfers between devices  57.1 us (57%)
  waiting for transfers between devices  29.1 us (29%)
  Pallas kernels  10.5 us (10%)
  other arithmetic  1.38 us (1%)
    ppermute x3, starting transfers between devices, local(): down = lax.ppermute(down, 'zh', down_pairs(s))  22.4 us
    ppermute x3, waiting for transfers between devices, local(): lax.ppermute(w_out, 'x', [(i, (i + k) % PER) for i in range(PER)])  21.4 us
    ppermute x3, starting transfers between devices, local(): lax.ppermute(w_out, 'x', [(i, (i + k) % PER) for i in range(PER)])  10.5 us
    ppermute x3, waiting for transfers between devices, local(): down = lax.ppermute(down, 'zh', down_pairs(s))  7.53 us
    all_to_all x1, starting transfers between devices, local(): parts = lax.all_to_all(parts, ('zl', 'y', 'x'), 0, 0, tiled=True)  7.06 us
    ppermute x4, starting transfers between devices, local(): up = lax.ppermute(up, 'zh', up_pairs(s))  6.9 us
    all_to_all x1, starting transfers between devices, local(): q_team = lax.all_to_all(q8, ('zl', 'y'), 0, 0, tiled=True)  6.37 us
    ppermute x1, starting transfers between devices, local(): received = lax.ppermute(send, 'c', [(0, 1), (1, 0)])  3.87 us
  transfers between devices with their start and end apart: 13, of which 6 were waited for; matrix products, arithmetic and copies ran while one was open for 1% of the time, Pallas kernels for 3%

profile of v6, /device:TPU:1, one launch (start us, length us, event | category | flops | bytes accessed | tf_op | source)
XLA Modules:
  0.0 99.8 jit_solution(13378076259331309869)
XLA Ops:
  0.7 0.1 mul.36
  0.8 0.1 pad_add_fusion.1.place_ref
  0.8 0.5 fusion
  1.4 3.6 %project.1 = (bf16[8,256,128]{2,1,0:T(8,128)(2,1)}, bf16[512,128]{1,0:T(8,128)(2,1)S(1)}, s32[4,512]{1,0:T(4,128)S(1)}) custom-call(s32[2]{0:T(128)S(1)} %pad_add_fusion.1.place_ref, bf16[256,2048]{1,0:T(8,128)(2,1)} %refs_0_.2, bf16[2048,128]{1,0:T(8,128)(2,1)} %refs_1_.1, bf16[2048,128]{1,0:T(8,128)(2,1)} %refs_2_.1, bf16[2048,128]{1,0:T(8,128)(2,1)} %refs_3_.1, ...), custom_call_target="tpu_custom_call" | custom-call | tf_op jit(solution)/shard_map/project/pallas_call | solution.py:122
  5.0 6.4 %all-to-all-start = ((bf16[8,256,128]{2,1,0:T(8,128)(2,1)}), bf16[8,256,128]{2,1,0:T(8,128)(2,1)S(1)}, u32[]{:S(2)}, u32[]{:S(2)}) async-start(bf16[8,256,128]{2,1,0:T(8,128)(2,1)} %get-tuple-element.13), calls=%async_computation | async-start | bytes 1048576 | tf_op jit(solution)/shard_map/all_to_all | solution.py:395
  11.4 4.9 %collective-permute-start = (bf16[512,128]{1,0:T(8,128)(2,1)S(1)}, bf16[512,128]{1,0:T(8,128)(2,1)S(1)}, u32[]{:S(2)}, u32[]{:S(2)}) collective-permute-start(bf16[512,128]{1,0:T(8,128)(2,1)S(1)} %get-tuple-element.14.refs_0_), channel_id=1, source_target_pairs={{0,64},{64,128},{128,192},{192,256},{256,320},{320,384},{384,448},... | collective-permute-start | bytes 393224 | tf_op jit(solution)/shard_map/ppermute | solution.py:390
  16.3 7.1 %collective-permute-start.2 = (bf16[512,128]{1,0:T(8,128)(2,1)S(1)}, bf16[512,128]{1,0:T(8,128)(2,1)S(1)}, u32[]{:S(2)}, u32[]{:S(2)}) collective-permute-start(bf16[512,128]{1,0:T(8,128)(2,1)S(1)} %get-tuple-element.14.refs_0_), channel_id=1, source_target_pairs={{0,448},{64,0},{128,64},{1,449},{65,1},{129,65},{2,450},{66,2},{13... | collective-permute-start | bytes 393224 | tf_op jit(solution)/shard_map/ppermute | solution.py:393
  23.3 0.0 collective-permute-done.refs_1_
  23.3 0.7 collective-permute-start.1
  24.0 3.0 %collective-permute-done.2.refs_4_ = bf16[512,128]{1,0:T(8,128)(2,1)S(1)} collective-permute-done((bf16[512,128]{1,0:T(8,128)(2,1)S(1)}, bf16[512,128]{1,0:T(8,128)(2,1)S(1)}, u32[]{:S(2)}, u32[]{:S(2)}) %collective-permute-start.2) | collective-permute-done | bytes 131104 | tf_op jit(solution)/shard_map/ppermute | solution.py:393
  27.1 9.0 %collective-permute-start.3 = (bf16[512,128]{1,0:T(8,128)(2,1)S(1)}, bf16[512,128]{1,0:T(8,128)(2,1)S(1)}, u32[]{:S(2)}, u32[]{:S(2)}) collective-permute-start(bf16[512,128]{1,0:T(8,128)(2,1)S(1)} %collective-permute-done.2.refs_4_), channel_id=1, source_target_pairs={{448,384},{0,448},{64,0},{449,385},{1,449},{65,1},{450,386},{2,450... | collective-permute-start | bytes 393224 | tf_op jit(solution)/shard_map/ppermute | solution.py:393
  36.1 0.7 collective-permute-start.4
  36.8 4.4 %collective-permute-done.3.refs_3_ = bf16[512,128]{1,0:T(8,128)(2,1)S(1)} collective-permute-done((bf16[512,128]{1,0:T(8,128)(2,1)S(1)}, bf16[512,128]{1,0:T(8,128)(2,1)S(1)}, u32[]{:S(2)}, u32[]{:S(2)}) %collective-permute-start.3) | collective-permute-done | bytes 131104 | tf_op jit(solution)/shard_map/ppermute | solution.py:393
  41.2 6.4 %collective-permute-start.6 = (bf16[512,128]{1,0:T(8,128)(2,1)S(1)}, bf16[512,128]{1,0:T(8,128)(2,1)S(1)}, u32[]{:S(2)}, u32[]{:S(2)}) collective-permute-start(bf16[512,128]{1,0:T(8,128)(2,1)S(1)} %collective-permute-done.3.refs_3_), channel_id=1, source_target_pairs={{384,320},{448,384},{0,448},{385,321},{449,385},{1,449},{386,322},... | collective-permute-start | bytes 393224 | tf_op jit(solution)/shard_map/ppermute | solution.py:393
  47.6 0.7 collective-permute-start.5
  48.3 3.2 %near.1 = (bf16[33,128,128]{2,1,0:T(8,128)(2,1)S(1)}, f32[33,8,128]{2,1,0:T(8,128)S(1)}, f32[33,8,128]{2,1,0:T(8,128)S(1)}, f32[33,64,128]{2,1,0:T(8,128)S(1)}) custom-call(s32[4,512]{1,0:T(4,128)S(1)} %get-tuple-element.12.pairs_ref, bf16[8,256,128]{2,1,0:T(8,128)(2,1)S(1)} %all-to-all-done.q_ref, bf16[512,128]{1,0:T(8,128)(2,1)S(1)} %get-tuple-element.14.refs_0_, ...), custom_call_target="tpu_custom_call" | custom-call | tf_op jit(solution)/shard_map/near/pallas_call | solution.py:277
  51.4 0.1 collective-permute-done.6.refs_2_
  51.5 1.9 %far.1 = bf16[32,80,128]{2,1,0:T(8,128)(2,1)} custom-call(s32[4,512]{1,0:T(4,128)S(1)} %get-tuple-element.12.pairs_ref, bf16[33,128,128]{2,1,0:T(8,128)(2,1)S(1)} %get-tuple-element.15.qq, f32[33,8,128]{2,1,0:T(8,128)S(1)} %get-tuple-element.16.m_ref, f32[33,8,128]{2,1,0:T(8,128)S(1)} %get-tuple-element.17.l_ref, ...), custom_call_target="tpu_custom_call" | custom-call | tf_op jit(solution)/shard_map/far/pallas_call | solution.py:291
  53.4 0.0 copy-start
  53.4 7.1 %all-to-all-start.1 = ((bf16[32,80,128]{2,1,0:T(8,128)(2,1)}), bf16[32,80,128]{2,1,0:T(8,128)(2,1)S(1)}, u32[]{:S(2)}, u32[]{:S(2)}) async-start(bf16[32,80,128]{2,1,0:T(8,128)(2,1)} %far.1), calls=%async_computation.1 | async-start | bytes 1310720 | tf_op jit(solution)/shard_map/all_to_all | solution.py:401
  60.5 3.1 %collective-permute-start.7 = (bf16[128,2048]{1,0:T(8,128)(2,1)S(1)}, bf16[128,2048]{1,0:T(8,128)(2,1)S(1)}, u32[]{:S(2)}, u32[]{:S(2)}) collective-permute-start(bf16[128,2048]{1,0:T(8,128)(2,1)S(1)} %copy-done), channel_id=1, source_target_pairs={{0,2},{2,4},{4,6},{6,0},{1,3},{3,5},{5,7},{7,1},{8,10},{10,12},{12... | collective-permute-start | bytes 1572872 | tf_op jit(solution)/shard_map/ppermute | solution.py:398
  63.6 4.3 %collective-permute-start.8 = (bf16[128,2048]{1,0:T(8,128)(2,1)S(1)}, bf16[128,2048]{1,0:T(8,128)(2,1)S(1)}, u32[]{:S(2)}, u32[]{:S(2)}) collective-permute-start(bf16[128,2048]{1,0:T(8,128)(2,1)S(1)} %copy-done), channel_id=1, source_target_pairs={{0,4},{2,6},{4,0},{6,2},{1,5},{3,7},{5,1},{7,3},{8,12},{10,14},{12... | collective-permute-start | bytes 1572872 | tf_op jit(solution)/shard_map/ppermute | solution.py:398
  68.0 3.1 %collective-permute-start.9 = (bf16[128,2048]{1,0:T(8,128)(2,1)S(1)}, bf16[128,2048]{1,0:T(8,128)(2,1)S(1)}, u32[]{:S(2)}, u32[]{:S(2)}) collective-permute-start(bf16[128,2048]{1,0:T(8,128)(2,1)S(1)} %copy-done), channel_id=1, source_target_pairs={{0,6},{2,0},{4,2},{6,4},{1,7},{3,1},{5,3},{7,5},{8,14},{10,8},{12,... | collective-permute-start | bytes 1572872 | tf_op jit(solution)/shard_map/ppermute | solution.py:398
  71.1 0.1 pad_add_fusion.place_ref
  71.1 11.1 %collective-permute-done.7.refs_1_ = bf16[128,2048]{1,0:T(8,128)(2,1)S(1)} collective-permute-done((bf16[128,2048]{1,0:T(8,128)(2,1)S(1)}, bf16[128,2048]{1,0:T(8,128)(2,1)S(1)}, u32[]{:S(2)}, u32[]{:S(2)}) %collective-permute-start.7) | collective-permute-done | bytes 524320 | tf_op jit(solution)/shard_map/ppermute | solution.py:398
  82.3 10.2 %collective-permute-done.8.refs_2_ = bf16[128,2048]{1,0:T(8,128)(2,1)S(1)} collective-permute-done((bf16[128,2048]{1,0:T(8,128)(2,1)S(1)}, bf16[128,2048]{1,0:T(8,128)(2,1)S(1)}, u32[]{:S(2)}, u32[]{:S(2)}) %collective-permute-start.8) | collective-permute-done | bytes 524320 | tf_op jit(solution)/shard_map/ppermute | solution.py:398
  92.5 1.8 %merge.1 = (f32[32,2048]{1,0:T(8,128)S(1)}, bf16[32,2048]{1,0:T(8,128)(2,1)S(1)}, f32[4,128]{1,0:T(4,128)S(1)}) custom-call(s32[2]{0:T(128)S(1)} %pad_add_fusion.place_ref, bf16[32,80,128]{2,1,0:T(8,128)(2,1)S(1)} %all-to-all-done.1.part_ref, bf16[128,2048]{1,0:T(8,128)(2,1)S(1)} %copy-done, bf16[128,2048]{1,0:T(8,128)(2,1)S(1)} %collective-permute-done.7.refs_1_, ...), custom_call_target="tpu_custom_call" | custom-call | tf_op jit(solution)/shard_map/merge/pallas_call | solution.py:344
  94.3 3.9 %collective-permute-start.10 = (bf16[32,2048]{1,0:T(8,128)(2,1)S(1)}, bf16[32,2048]{1,0:T(8,128)(2,1)S(1)}, u32[]{:S(2)}, u32[]{:S(2)}) collective-permute-start(bf16[32,2048]{1,0:T(8,128)(2,1)S(1)} %get-tuple-element.20), channel_id=1, source_target_pairs={{0,1},{1,0},{2,3},{3,2},{4,5},{5,4},{6,7},{7,6},{8,9},{9,8},{10,11... | collective-permute-start | bytes 393224 | tf_op jit(solution)/shard_map/ppermute | solution.py:404
  98.2 0.1 reshape.28
  98.3 0.7 reshape.29
  98.9 0.2 collective-permute-done.10
  99.1 0.7 add_convert_fusion
  (12 shorter events, 0.0 us)
Async XLA Ops:
  5.0 43.3 %all-to-all-start = ((bf16[8,256,128]{2,1,0:T(8,128)(2,1)}), bf16[8,256,128]{2,1,0:T(8,128)(2,1)S(1)}, u32[]{:S(2)}, u32[]{:S(2)}) async-start(bf16[8,256,128]{2,1,0:T(8,128)(2,1)} %get-tuple-element.13), calls=%async_computation | async-start | bytes 1048576 | tf_op jit(solution)/shard_map/all_to_all | solution.py:395
  11.4 12.0 %collective-permute-start = (bf16[512,128]{1,0:T(8,128)(2,1)S(1)}, bf16[512,128]{1,0:T(8,128)(2,1)S(1)}, u32[]{:S(2)}, u32[]{:S(2)}) collective-permute-start(bf16[512,128]{1,0:T(8,128)(2,1)S(1)} %get-tuple-element.14.refs_0_), channel_id=1, source_target_pairs={{0,64},{64,128},{128,192},{192,256},{256,320},{320,384},{384,448},... | collective-permute-start | bytes 393224 | tf_op jit(solution)/shard_map/ppermute | solution.py:390
  16.3 10.8 %collective-permute-start.2 = (bf16[512,128]{1,0:T(8,128)(2,1)S(1)}, bf16[512,128]{1,0:T(8,128)(2,1)S(1)}, u32[]{:S(2)}, u32[]{:S(2)}) collective-permute-start(bf16[512,128]{1,0:T(8,128)(2,1)S(1)} %get-tuple-element.14.refs_0_), channel_id=1, source_target_pairs={{0,448},{64,0},{128,64},{1,449},{65,1},{129,65},{2,450},{66,2},{13... | collective-permute-start | bytes 393224 | tf_op jit(solution)/shard_map/ppermute | solution.py:393
  23.3 12.7 %collective-permute-start.1 = (bf16[512,128]{1,0:T(8,128)(2,1)S(1)}, bf16[512,128]{1,0:T(8,128)(2,1)S(1)}, u32[]{:S(2)}, u32[]{:S(2)}) collective-permute-start(bf16[512,128]{1,0:T(8,128)(2,1)S(1)} %collective-permute-done.refs_1_), channel_id=1, source_target_pairs={{64,128},{128,192},{192,256},{256,320},{320,384},{384,448},{65,129... | collective-permute-start | bytes 393224 | tf_op jit(solution)/shard_map/ppermute | solution.py:390
  27.1 14.1 %collective-permute-start.3 = (bf16[512,128]{1,0:T(8,128)(2,1)S(1)}, bf16[512,128]{1,0:T(8,128)(2,1)S(1)}, u32[]{:S(2)}, u32[]{:S(2)}) collective-permute-start(bf16[512,128]{1,0:T(8,128)(2,1)S(1)} %collective-permute-done.2.refs_4_), channel_id=1, source_target_pairs={{448,384},{0,448},{64,0},{449,385},{1,449},{65,1},{450,386},{2,450... | collective-permute-start | bytes 393224 | tf_op jit(solution)/shard_map/ppermute | solution.py:393
  36.1 11.5 %collective-permute-start.4 = (bf16[512,128]{1,0:T(8,128)(2,1)S(1)}, bf16[512,128]{1,0:T(8,128)(2,1)S(1)}, u32[]{:S(2)}, u32[]{:S(2)}) collective-permute-start(bf16[512,128]{1,0:T(8,128)(2,1)S(1)} %collective-permute-done.1.refs_2_), channel_id=1, source_target_pairs={{128,192},{192,256},{256,320},{320,384},{384,448},{129,193},{193,2... | collective-permute-start | bytes 393224 | tf_op jit(solution)/shard_map/ppermute | solution.py:390
  41.2 10.3 %collective-permute-start.6 = (bf16[512,128]{1,0:T(8,128)(2,1)S(1)}, bf16[512,128]{1,0:T(8,128)(2,1)S(1)}, u32[]{:S(2)}, u32[]{:S(2)}) collective-permute-start(bf16[512,128]{1,0:T(8,128)(2,1)S(1)} %collective-permute-done.3.refs_3_), channel_id=1, source_target_pairs={{384,320},{448,384},{0,448},{385,321},{449,385},{1,449},{386,322},... | collective-permute-start | bytes 393224 | tf_op jit(solution)/shard_map/ppermute | solution.py:393
  47.6 3.9 %collective-permute-start.5 = (bf16[512,128]{1,0:T(8,128)(2,1)S(1)}, bf16[512,128]{1,0:T(8,128)(2,1)S(1)}, u32[]{:S(2)}, u32[]{:S(2)}) collective-permute-start(bf16[512,128]{1,0:T(8,128)(2,1)S(1)} %collective-permute-done.4.refs_0_), channel_id=1, source_target_pairs={{192,256},{256,320},{320,384},{384,448},{193,257},{257,321},{321,3... | collective-permute-start | bytes 393224 | tf_op jit(solution)/shard_map/ppermute | solution.py:390
  53.4 7.1 %copy-start = (bf16[128,2048]{1,0:T(8,128)(2,1)S(1)}, bf16[128,2048]{1,0:T(8,128)(2,1)}, u32[]{:S(2)}) copy-start(bf16[128,2048]{1,0:T(8,128)(2,1)} %refs_0_.3) | copy-start | bytes 1572868
  53.4 39.1 %all-to-all-start.1 = ((bf16[32,80,128]{2,1,0:T(8,128)(2,1)}), bf16[32,80,128]{2,1,0:T(8,128)(2,1)S(1)}, u32[]{:S(2)}, u32[]{:S(2)}) async-start(bf16[32,80,128]{2,1,0:T(8,128)(2,1)} %far.1), calls=%async_computation.1 | async-start | bytes 1310720 | tf_op jit(solution)/shard_map/all_to_all | solution.py:401
  60.5 21.8 %collective-permute-start.7 = (bf16[128,2048]{1,0:T(8,128)(2,1)S(1)}, bf16[128,2048]{1,0:T(8,128)(2,1)S(1)}, u32[]{:S(2)}, u32[]{:S(2)}) collective-permute-start(bf16[128,2048]{1,0:T(8,128)(2,1)S(1)} %copy-done), channel_id=1, source_target_pairs={{0,2},{2,4},{4,6},{6,0},{1,3},{3,5},{5,7},{7,1},{8,10},{10,12},{12... | collective-permute-start | bytes 1572872 | tf_op jit(solution)/shard_map/ppermute | solution.py:398
  63.6 28.8 %collective-permute-start.8 = (bf16[128,2048]{1,0:T(8,128)(2,1)S(1)}, bf16[128,2048]{1,0:T(8,128)(2,1)S(1)}, u32[]{:S(2)}, u32[]{:S(2)}) collective-permute-start(bf16[128,2048]{1,0:T(8,128)(2,1)S(1)} %copy-done), channel_id=1, source_target_pairs={{0,4},{2,6},{4,0},{6,2},{1,5},{3,7},{5,1},{7,3},{8,12},{10,14},{12... | collective-permute-start | bytes 1572872 | tf_op jit(solution)/shard_map/ppermute | solution.py:398
  68.0 24.5 %collective-permute-start.9 = (bf16[128,2048]{1,0:T(8,128)(2,1)S(1)}, bf16[128,2048]{1,0:T(8,128)(2,1)S(1)}, u32[]{:S(2)}, u32[]{:S(2)}) collective-permute-start(bf16[128,2048]{1,0:T(8,128)(2,1)S(1)} %copy-done), channel_id=1, source_target_pairs={{0,6},{2,0},{4,2},{6,4},{1,7},{3,1},{5,3},{7,5},{8,14},{10,8},{12,... | collective-permute-start | bytes 1572872 | tf_op jit(solution)/shard_map/ppermute | solution.py:398
  94.3 4.8 %collective-permute-start.10 = (bf16[32,2048]{1,0:T(8,128)(2,1)S(1)}, bf16[32,2048]{1,0:T(8,128)(2,1)S(1)}, u32[]{:S(2)}, u32[]{:S(2)}) collective-permute-start(bf16[32,2048]{1,0:T(8,128)(2,1)S(1)} %get-tuple-element.20), channel_id=1, source_target_pairs={{0,1},{1,0},{2,3},{3,2},{4,5},{5,4},{6,7},{7,6},{8,9},{9,8},{10,11... | collective-permute-start | bytes 393224 | tf_op jit(solution)/shard_map/ppermute | solution.py:404

commit v7 on v6

--- a/solution.py
+++ b/solution.py
@@ -18,11 +18,10 @@
 TEAM = 8
 QB = TEAM * PER
 MAXP = QB * SEL
-UNROLL_BITS = 5
-UNROLL = 1 << UNROLL_BITS
+UNROLL_BITS = (5, 4)
 NBLK = 256
-NEAR = (0, 1, 2, 6, 7)
-FAR = (3, 4, 5)
+NEAR = (0, 1, 2, 3, 6, 7)
+FAR = (4, 5)
 STATS = 16
 
 rotary_base = 500000.0
@@ -62,7 +61,7 @@
     count = jnp.sum(sums, axis=1, keepdims=True)
     pairs = jnp.where(row < count, jnp.sum(picked, axis=0, keepdims=True), float(QB * 64))
     pairs_ref[pl.ds(kind, 1), :] = pairs.astype(i32)
-    trips = (count.astype(i32) + (UNROLL - 1)) >> UNROLL_BITS
+    trips = (count.astype(i32) + ((1 << UNROLL_BITS[kind]) - 1)) >> UNROLL_BITS[kind]
     pairs_ref[pl.ds(2 + kind, 1), :] = jnp.broadcast_to(trips, (1, MAXP))
 
 
@@ -169,13 +168,14 @@
     qq[QB] = jnp.zeros((WIDTH, WIDTH), bf16)
 
 
-def run_pairs(pairs_ref, kind, qq, kbuf, vbuf, sbuf, mbuf, lbuf, acc, rescale):
+def run_pairs(pairs_ref, kind, qq, kbuf, vbuf, sbuf, mbuf, lbuf, acc, earlier):
     even = (lax.broadcasted_iota(jnp.int32, (BLK, WIDTH), 1) & (HEAD_DIM // 2)) == 0
     trips = pairs_ref[2 + kind, 0]
+    unroll = 1 << UNROLL_BITS[kind]
 
     def score(it, carry):
-        for u in range(UNROLL):
-            i = it * UNROLL + u
+        for u in range(unroll):
+            i = it * unroll + u
             code = pairs_ref[kind, i]
             qi = code >> 6
             ki = code & 63
@@ -189,14 +189,14 @@
     for i in range(QB + 1):
         top = jnp.broadcast_to(jnp.max(mbuf[i], axis=0, keepdims=True), (8, WIDTH))
         mbuf[i] = top
-        if rescale is not None:
-            factor = jnp.exp(rescale[i] - top)
-            lbuf[i] = lbuf[i] * factor
-            acc[i] = (acc[i].reshape(8, 8, WIDTH) * factor[None]).reshape(BLK, WIDTH)
+        if earlier is not None:
+            factor = jnp.exp(earlier[0][i] - top)
+            lbuf[i] = earlier[1][i] * factor
+            acc[i] = (earlier[2][i].reshape(8, 8, WIDTH) * factor[None]).reshape(BLK, WIDTH)
 
     def weigh(it, carry):
-        for u in range(UNROLL):
-            i = it * UNROLL + u
+        for u in range(unroll):
+            i = it * unroll + u
             code = pairs_ref[kind, i]
             qi = code >> 6
             ki = code & 63
@@ -228,9 +228,7 @@
     kbuf, vbuf, sbuf, mbuf, lbuf, acc, out_buf, sems = refs[n + 1 :]
     fill_keys(refs[:n], kbuf, vbuf)
     mbuf[...] = m_ref[...]
-    lbuf[...] = l_ref[...]
-    acc[...] = acc_ref[...]
-    run_pairs(pairs_ref, 1, qq, kbuf, vbuf, sbuf, mbuf, lbuf, acc, m_ref)
+    run_pairs(pairs_ref, 1, qq, kbuf, vbuf, sbuf, mbuf, lbuf, acc, (m_ref, l_ref, acc_ref))
     sends = []
     for i in range(TEAM):
         logs = []

time: 100 us -> 100 us (level)
  transfers between devices with their start and end apart: 13 -> 13, of which waited for: 6 -> 5; matrix products, arithmetic and copies ran while one was open for 1% -> 1% of each run, Pallas kernels for 3% -> 3%
where the time goes in v7:
time: 100 us; the launch traced here: 99.8 us
  starting transfers between devices  57.2 us (57%)
  waiting for transfers between devices  29.1 us (29%)
  Pallas kernels  10.5 us (10%)
  other arithmetic  1.38 us (1%)
    ppermute x3, starting transfers between devices, local(): down = lax.ppermute(down, 'zh', down_pairs(s))  22.4 us
    ppermute x3, waiting for transfers between devices, local(): lax.ppermute(w_out, 'x', [(i, (i + k) % PER) for i in range(PER)])  21.4 us
    ppermute x3, starting transfers between devices, local(): lax.ppermute(w_out, 'x', [(i, (i + k) % PER) for i in range(PER)])  10.5 us
    ppermute x3, waiting for transfers between devices, local(): down = lax.ppermute(down, 'zh', down_pairs(s))  7.49 us
    all_to_all x1, starting transfers between devices, local(): parts = lax.all_to_all(parts, ('zl', 'y', 'x'), 0, 0, tiled=True)  7.08 us
    ppermute x4, starting transfers between devices, local(): up = lax.ppermute(up, 'zh', up_pairs(s))  6.9 us
    all_to_all x1, starting transfers between devices, local(): q_team = lax.all_to_all(q8, ('zl', 'y'), 0, 0, tiled=True)  6.37 us
    ppermute x1, starting transfers between devices, local(): received = lax.ppermute(send, 'c', [(0, 1), (1, 0)])  3.87 us
  transfers between devices with their start and end apart: 13, of which 5 were waited for; matrix products, arithmetic and copies ran while one was open for 1% of the time, Pallas kernels for 3%

profile of v7, /device:TPU:1, one launch (start us, length us, event | category | flops | bytes accessed | tf_op | source)
XLA Modules:
  0.0 99.8 jit_solution(9860244212441477456)
XLA Ops:
  0.7 0.1 mul.36
  0.8 0.1 pad_add_fusion.1.place_ref
  0.8 0.5 fusion
  1.4 3.6 %project.1 = (bf16[8,256,128]{2,1,0:T(8,128)(2,1)}, bf16[512,128]{1,0:T(8,128)(2,1)S(1)}, s32[4,512]{1,0:T(4,128)S(1)}) custom-call(s32[2]{0:T(128)S(1)} %pad_add_fusion.1.place_ref, bf16[256,2048]{1,0:T(8,128)(2,1)} %refs_0_.2, bf16[2048,128]{1,0:T(8,128)(2,1)} %refs_1_.1, bf16[2048,128]{1,0:T(8,128)(2,1)} %refs_2_.1, bf16[2048,128]{1,0:T(8,128)(2,1)} %refs_3_.1, ...), custom_call_target="tpu_custom_call" | custom-call | tf_op jit(solution)/shard_map/project/pallas_call | solution.py:121
  5.0 6.4 %all-to-all-start = ((bf16[8,256,128]{2,1,0:T(8,128)(2,1)}), bf16[8,256,128]{2,1,0:T(8,128)(2,1)S(1)}, u32[]{:S(2)}, u32[]{:S(2)}) async-start(bf16[8,256,128]{2,1,0:T(8,128)(2,1)} %get-tuple-element.13), calls=%async_computation | async-start | bytes 1048576 | tf_op jit(solution)/shard_map/all_to_all | solution.py:393
  11.4 4.9 %collective-permute-start = (bf16[512,128]{1,0:T(8,128)(2,1)S(1)}, bf16[512,128]{1,0:T(8,128)(2,1)S(1)}, u32[]{:S(2)}, u32[]{:S(2)}) collective-permute-start(bf16[512,128]{1,0:T(8,128)(2,1)S(1)} %get-tuple-element.14.refs_0_), channel_id=1, source_target_pairs={{0,64},{64,128},{128,192},{192,256},{256,320},{320,384},{384,448},... | collective-permute-start | bytes 393224 | tf_op jit(solution)/shard_map/ppermute | solution.py:388
  16.3 7.1 %collective-permute-start.3 = (bf16[512,128]{1,0:T(8,128)(2,1)S(1)}, bf16[512,128]{1,0:T(8,128)(2,1)S(1)}, u32[]{:S(2)}, u32[]{:S(2)}) collective-permute-start(bf16[512,128]{1,0:T(8,128)(2,1)S(1)} %get-tuple-element.14.refs_0_), channel_id=1, source_target_pairs={{0,448},{64,0},{128,64},{1,449},{65,1},{129,65},{2,450},{66,2},{13... | collective-permute-start | bytes 393224 | tf_op jit(solution)/shard_map/ppermute | solution.py:391
  23.3 0.0 collective-permute-done.refs_1_
  23.3 0.7 collective-permute-start.1
  24.0 3.0 %collective-permute-done.3.refs_5_ = bf16[512,128]{1,0:T(8,128)(2,1)S(1)} collective-permute-done((bf16[512,128]{1,0:T(8,128)(2,1)S(1)}, bf16[512,128]{1,0:T(8,128)(2,1)S(1)}, u32[]{:S(2)}, u32[]{:S(2)}) %collective-permute-start.3) | collective-permute-done | bytes 131104 | tf_op jit(solution)/shard_map/ppermute | solution.py:391
  27.1 9.0 %collective-permute-start.4 = (bf16[512,128]{1,0:T(8,128)(2,1)S(1)}, bf16[512,128]{1,0:T(8,128)(2,1)S(1)}, u32[]{:S(2)}, u32[]{:S(2)}) collective-permute-start(bf16[512,128]{1,0:T(8,128)(2,1)S(1)} %collective-permute-done.3.refs_5_), channel_id=1, source_target_pairs={{448,384},{0,448},{64,0},{449,385},{1,449},{65,1},{450,386},{2,450... | collective-permute-start | bytes 393224 | tf_op jit(solution)/shard_map/ppermute | solution.py:391
  36.1 0.7 collective-permute-start.2
  36.8 4.4 %collective-permute-done.4.refs_4_ = bf16[512,128]{1,0:T(8,128)(2,1)S(1)} collective-permute-done((bf16[512,128]{1,0:T(8,128)(2,1)S(1)}, bf16[512,128]{1,0:T(8,128)(2,1)S(1)}, u32[]{:S(2)}, u32[]{:S(2)}) %collective-permute-start.4) | collective-permute-done | bytes 131104 | tf_op jit(solution)/shard_map/ppermute | solution.py:391
  41.2 6.4 %collective-permute-start.6 = (bf16[512,128]{1,0:T(8,128)(2,1)S(1)}, bf16[512,128]{1,0:T(8,128)(2,1)S(1)}, u32[]{:S(2)}, u32[]{:S(2)}) collective-permute-start(bf16[512,128]{1,0:T(8,128)(2,1)S(1)} %collective-permute-done.4.refs_4_), channel_id=1, source_target_pairs={{384,320},{448,384},{0,448},{385,321},{449,385},{1,449},{386,322},... | collective-permute-start | bytes 393224 | tf_op jit(solution)/shard_map/ppermute | solution.py:391
  47.6 0.7 collective-permute-start.5
  48.3 3.2 %near.1 = (bf16[33,128,128]{2,1,0:T(8,128)(2,1)S(1)}, f32[33,8,128]{2,1,0:T(8,128)S(1)}, f32[33,8,128]{2,1,0:T(8,128)S(1)}, f32[33,64,128]{2,1,0:T(8,128)S(1)}) custom-call(s32[4,512]{1,0:T(4,128)S(1)} %get-tuple-element.12.pairs_ref, bf16[8,256,128]{2,1,0:T(8,128)(2,1)S(1)} %all-to-all-done.q_ref, bf16[512,128]{1,0:T(8,128)(2,1)S(1)} %get-tuple-element.14.refs_0_, ...), custom_call_target="tpu_custom_call" | custom-call | tf_op jit(solution)/shard_map/near/pallas_call | solution.py:275
  51.5 0.0 collective-permute-done.6.refs_1_
  51.5 1.9 %far.1 = bf16[32,80,128]{2,1,0:T(8,128)(2,1)} custom-call(s32[4,512]{1,0:T(4,128)S(1)} %get-tuple-element.12.pairs_ref, bf16[33,128,128]{2,1,0:T(8,128)(2,1)S(1)} %get-tuple-element.15.qq, f32[33,8,128]{2,1,0:T(8,128)S(1)} %get-tuple-element.16.m_ref, f32[33,8,128]{2,1,0:T(8,128)S(1)} %get-tuple-element.17.l_ref, ...), custom_call_target="tpu_custom_call" | custom-call | tf_op jit(solution)/shard_map/far/pallas_call | solution.py:289
  53.4 0.0 copy-start
  53.4 7.1 %all-to-all-start.1 = ((bf16[32,80,128]{2,1,0:T(8,128)(2,1)}), bf16[32,80,128]{2,1,0:T(8,128)(2,1)S(1)}, u32[]{:S(2)}, u32[]{:S(2)}) async-start(bf16[32,80,128]{2,1,0:T(8,128)(2,1)} %far.1), calls=%async_computation.1 | async-start | bytes 1310720 | tf_op jit(solution)/shard_map/all_to_all | solution.py:399
  60.5 3.1 %collective-permute-start.7 = (bf16[128,2048]{1,0:T(8,128)(2,1)S(1)}, bf16[128,2048]{1,0:T(8,128)(2,1)S(1)}, u32[]{:S(2)}, u32[]{:S(2)}) collective-permute-start(bf16[128,2048]{1,0:T(8,128)(2,1)S(1)} %copy-done), channel_id=1, source_target_pairs={{0,2},{2,4},{4,6},{6,0},{1,3},{3,5},{5,7},{7,1},{8,10},{10,12},{12... | collective-permute-start | bytes 1572872 | tf_op jit(solution)/shard_map/ppermute | solution.py:396
  63.6 4.3 %collective-permute-start.8 = (bf16[128,2048]{1,0:T(8,128)(2,1)S(1)}, bf16[128,2048]{1,0:T(8,128)(2,1)S(1)}, u32[]{:S(2)}, u32[]{:S(2)}) collective-permute-start(bf16[128,2048]{1,0:T(8,128)(2,1)S(1)} %copy-done), channel_id=1, source_target_pairs={{0,4},{2,6},{4,0},{6,2},{1,5},{3,7},{5,1},{7,3},{8,12},{10,14},{12... | collective-permute-start | bytes 1572872 | tf_op jit(solution)/shard_map/ppermute | solution.py:396
  67.9 3.1 %collective-permute-start.9 = (bf16[128,2048]{1,0:T(8,128)(2,1)S(1)}, bf16[128,2048]{1,0:T(8,128)(2,1)S(1)}, u32[]{:S(2)}, u32[]{:S(2)}) collective-permute-start(bf16[128,2048]{1,0:T(8,128)(2,1)S(1)} %copy-done), channel_id=1, source_target_pairs={{0,6},{2,0},{4,2},{6,4},{1,7},{3,1},{5,3},{7,5},{8,14},{10,8},{12,... | collective-permute-start | bytes 1572872 | tf_op jit(solution)/shard_map/ppermute | solution.py:396
  71.0 0.1 pad_add_fusion.place_ref
  71.1 11.1 %collective-permute-done.7.refs_1_ = bf16[128,2048]{1,0:T(8,128)(2,1)S(1)} collective-permute-done((bf16[128,2048]{1,0:T(8,128)(2,1)S(1)}, bf16[128,2048]{1,0:T(8,128)(2,1)S(1)}, u32[]{:S(2)}, u32[]{:S(2)}) %collective-permute-start.7) | collective-permute-done | bytes 524320 | tf_op jit(solution)/shard_map/ppermute | solution.py:396
  82.2 10.2 %collective-permute-done.8.refs_2_ = bf16[128,2048]{1,0:T(8,128)(2,1)S(1)} collective-permute-done((bf16[128,2048]{1,0:T(8,128)(2,1)S(1)}, bf16[128,2048]{1,0:T(8,128)(2,1)S(1)}, u32[]{:S(2)}, u32[]{:S(2)}) %collective-permute-start.8) | collective-permute-done | bytes 524320 | tf_op jit(solution)/shard_map/ppermute | solution.py:396
  92.5 1.8 %merge.1 = (f32[32,2048]{1,0:T(8,128)S(1)}, bf16[32,2048]{1,0:T(8,128)(2,1)S(1)}, f32[4,128]{1,0:T(4,128)S(1)}) custom-call(s32[2]{0:T(128)S(1)} %pad_add_fusion.place_ref, bf16[32,80,128]{2,1,0:T(8,128)(2,1)S(1)} %all-to-all-done.1.part_ref, bf16[128,2048]{1,0:T(8,128)(2,1)S(1)} %copy-done, bf16[128,2048]{1,0:T(8,128)(2,1)S(1)} %collective-permute-done.7.refs_1_, ...), custom_call_target="tpu_custom_call" | custom-call | tf_op jit(solution)/shard_map/merge/pallas_call | solution.py:342
  94.3 3.9 %collective-permute-start.10 = (bf16[32,2048]{1,0:T(8,128)(2,1)S(1)}, bf16[32,2048]{1,0:T(8,128)(2,1)S(1)}, u32[]{:S(2)}, u32[]{:S(2)}) collective-permute-start(bf16[32,2048]{1,0:T(8,128)(2,1)S(1)} %get-tuple-element.20), channel_id=1, source_target_pairs={{0,1},{1,0},{2,3},{3,2},{4,5},{5,4},{6,7},{7,6},{8,9},{9,8},{10,11... | collective-permute-start | bytes 393224 | tf_op jit(solution)/shard_map/ppermute | solution.py:402
  98.2 0.1 reshape.28
  98.3 0.7 reshape.29
  98.9 0.2 collective-permute-done.10
  99.1 0.7 add_convert_fusion
  (12 shorter events, 0.0 us)
Async XLA Ops:
  5.0 43.3 %all-to-all-start = ((bf16[8,256,128]{2,1,0:T(8,128)(2,1)}), bf16[8,256,128]{2,1,0:T(8,128)(2,1)S(1)}, u32[]{:S(2)}, u32[]{:S(2)}) async-start(bf16[8,256,128]{2,1,0:T(8,128)(2,1)} %get-tuple-element.13), calls=%async_computation | async-start | bytes 1048576 | tf_op jit(solution)/shard_map/all_to_all | solution.py:393
  11.4 12.0 %collective-permute-start = (bf16[512,128]{1,0:T(8,128)(2,1)S(1)}, bf16[512,128]{1,0:T(8,128)(2,1)S(1)}, u32[]{:S(2)}, u32[]{:S(2)}) collective-permute-start(bf16[512,128]{1,0:T(8,128)(2,1)S(1)} %get-tuple-element.14.refs_0_), channel_id=1, source_target_pairs={{0,64},{64,128},{128,192},{192,256},{256,320},{320,384},{384,448},... | collective-permute-start | bytes 393224 | tf_op jit(solution)/shard_map/ppermute | solution.py:388
  16.3 10.8 %collective-permute-start.3 = (bf16[512,128]{1,0:T(8,128)(2,1)S(1)}, bf16[512,128]{1,0:T(8,128)(2,1)S(1)}, u32[]{:S(2)}, u32[]{:S(2)}) collective-permute-start(bf16[512,128]{1,0:T(8,128)(2,1)S(1)} %get-tuple-element.14.refs_0_), channel_id=1, source_target_pairs={{0,448},{64,0},{128,64},{1,449},{65,1},{129,65},{2,450},{66,2},{13... | collective-permute-start | bytes 393224 | tf_op jit(solution)/shard_map/ppermute | solution.py:391
  23.3 12.7 %collective-permute-start.1 = (bf16[512,128]{1,0:T(8,128)(2,1)S(1)}, bf16[512,128]{1,0:T(8,128)(2,1)S(1)}, u32[]{:S(2)}, u32[]{:S(2)}) collective-permute-start(bf16[512,128]{1,0:T(8,128)(2,1)S(1)} %collective-permute-done.refs_1_), channel_id=1, source_target_pairs={{64,128},{128,192},{192,256},{256,320},{320,384},{384,448},{65,129... | collective-permute-start | bytes 393224 | tf_op jit(solution)/shard_map/ppermute | solution.py:388
  27.1 14.1 %collective-permute-start.4 = (bf16[512,128]{1,0:T(8,128)(2,1)S(1)}, bf16[512,128]{1,0:T(8,128)(2,1)S(1)}, u32[]{:S(2)}, u32[]{:S(2)}) collective-permute-start(bf16[512,128]{1,0:T(8,128)(2,1)S(1)} %collective-permute-done.3.refs_5_), channel_id=1, source_target_pairs={{448,384},{0,448},{64,0},{449,385},{1,449},{65,1},{450,386},{2,450... | collective-permute-start | bytes 393224 | tf_op jit(solution)/shard_map/ppermute | solution.py:391
  36.1 11.5 %collective-permute-start.2 = (bf16[512,128]{1,0:T(8,128)(2,1)S(1)}, bf16[512,128]{1,0:T(8,128)(2,1)S(1)}, u32[]{:S(2)}, u32[]{:S(2)}) collective-permute-start(bf16[512,128]{1,0:T(8,128)(2,1)S(1)} %collective-permute-done.1.refs_2_), channel_id=1, source_target_pairs={{128,192},{192,256},{256,320},{320,384},{384,448},{129,193},{193,2... | collective-permute-start | bytes 393224 | tf_op jit(solution)/shard_map/ppermute | solution.py:388
  41.2 10.3 %collective-permute-start.6 = (bf16[512,128]{1,0:T(8,128)(2,1)S(1)}, bf16[512,128]{1,0:T(8,128)(2,1)S(1)}, u32[]{:S(2)}, u32[]{:S(2)}) collective-permute-start(bf16[512,128]{1,0:T(8,128)(2,1)S(1)} %collective-permute-done.4.refs_4_), channel_id=1, source_target_pairs={{384,320},{448,384},{0,448},{385,321},{449,385},{1,449},{386,322},... | collective-permute-start | bytes 393224 | tf_op jit(solution)/shard_map/ppermute | solution.py:391
  47.6 3.9 %collective-permute-start.5 = (bf16[512,128]{1,0:T(8,128)(2,1)S(1)}, bf16[512,128]{1,0:T(8,128)(2,1)S(1)}, u32[]{:S(2)}, u32[]{:S(2)}) collective-permute-start(bf16[512,128]{1,0:T(8,128)(2,1)S(1)} %collective-permute-done.2.refs_3_), channel_id=1, source_target_pairs={{192,256},{256,320},{320,384},{384,448},{193,257},{257,321},{321,3... | collective-permute-start | bytes 393224 | tf_op jit(solution)/shard_map/ppermute | solution.py:388
  53.4 7.1 %copy-start = (bf16[128,2048]{1,0:T(8,128)(2,1)S(1)}, bf16[128,2048]{1,0:T(8,128)(2,1)}, u32[]{:S(2)}) copy-start(bf16[128,2048]{1,0:T(8,128)(2,1)} %refs_0_.3) | copy-start | bytes 1572868
  53.4 39.1 %all-to-all-start.1 = ((bf16[32,80,128]{2,1,0:T(8,128)(2,1)}), bf16[32,80,128]{2,1,0:T(8,128)(2,1)S(1)}, u32[]{:S(2)}, u32[]{:S(2)}) async-start(bf16[32,80,128]{2,1,0:T(8,128)(2,1)} %far.1), calls=%async_computation.1 | async-start | bytes 1310720 | tf_op jit(solution)/shard_map/all_to_all | solution.py:399
  60.5 21.8 %collective-permute-start.7 = (bf16[128,2048]{1,0:T(8,128)(2,1)S(1)}, bf16[128,2048]{1,0:T(8,128)(2,1)S(1)}, u32[]{:S(2)}, u32[]{:S(2)}) collective-permute-start(bf16[128,2048]{1,0:T(8,128)(2,1)S(1)} %copy-done), channel_id=1, source_target_pairs={{0,2},{2,4},{4,6},{6,0},{1,3},{3,5},{5,7},{7,1},{8,10},{10,12},{12... | collective-permute-start | bytes 1572872 | tf_op jit(solution)/shard_map/ppermute | solution.py:396
  63.6 28.8 %collective-permute-start.8 = (bf16[128,2048]{1,0:T(8,128)(2,1)S(1)}, bf16[128,2048]{1,0:T(8,128)(2,1)S(1)}, u32[]{:S(2)}, u32[]{:S(2)}) collective-permute-start(bf16[128,2048]{1,0:T(8,128)(2,1)S(1)} %copy-done), channel_id=1, source_target_pairs={{0,4},{2,6},{4,0},{6,2},{1,5},{3,7},{5,1},{7,3},{8,12},{10,14},{12... | collective-permute-start | bytes 1572872 | tf_op jit(solution)/shard_map/ppermute | solution.py:396
  67.9 24.5 %collective-permute-start.9 = (bf16[128,2048]{1,0:T(8,128)(2,1)S(1)}, bf16[128,2048]{1,0:T(8,128)(2,1)S(1)}, u32[]{:S(2)}, u32[]{:S(2)}) collective-permute-start(bf16[128,2048]{1,0:T(8,128)(2,1)S(1)} %copy-done), channel_id=1, source_target_pairs={{0,6},{2,0},{4,2},{6,4},{1,7},{3,1},{5,3},{7,5},{8,14},{10,8},{12,... | collective-permute-start | bytes 1572872 | tf_op jit(solution)/shard_map/ppermute | solution.py:396
  94.3 4.8 %collective-permute-start.10 = (bf16[32,2048]{1,0:T(8,128)(2,1)S(1)}, bf16[32,2048]{1,0:T(8,128)(2,1)S(1)}, u32[]{:S(2)}, u32[]{:S(2)}) collective-permute-start(bf16[32,2048]{1,0:T(8,128)(2,1)S(1)} %get-tuple-element.20), channel_id=1, source_target_pairs={{0,1},{1,0},{2,3},{3,2},{4,5},{5,4},{6,7},{7,6},{8,9},{9,8},{10,11... | collective-permute-start | bytes 393224 | tf_op jit(solution)/shard_map/ppermute | solution.py:402

commit v8 on v7

--- a/solution.py
+++ b/solution.py
@@ -80,10 +80,13 @@
     sends = [pltpu.make_async_copy(q_buf, q_hbm.at[i], sems.at[len(copies) + i]) for i in range(TEAM)]
     for copy in copies:
         copy.start()
-    cos = cos_ref[...]
-    sin = sin_ref[...]
     lane = lax.broadcasted_iota(jnp.int32, (ROWS, WIDTH), 1)
     first = (lane & (HEAD_DIM - 1)) < HEAD_DIM // 2
+    cos_j, sin_j = cos_ref[pl.ds(ROWS // 8, 8), :], sin_ref[pl.ds(ROWS // 8, 8), :]
+    rows = [(cos_ref[pl.ds(i, 1), :], sin_ref[pl.ds(i, 1), :]) for i in range(ROWS // 8)]
+    cos = jnp.concatenate([c * cos_j - s * sin_j for c, s in rows], axis=0)
+    sin = jnp.concatenate([s * cos_j + c * sin_j for c, s in rows], axis=0)
+    sin = jnp.where(first, -sin, sin)
 
     def turned(t):
         partner = jnp.where(first, pltpu.roll(t, WIDTH - HEAD_DIM // 2, 1), pltpu.roll(t, HEAD_DIM // 2, 1))
@@ -367,11 +370,11 @@
     zh = lax.axis_index("zh")
     mine = lax.axis_index(("zl", "y"))
     device = zh * TEAM + mine
-    positions = device * ROWS + jnp.arange(ROWS)
+    step = jnp.arange(ROWS // 8 + 8)
+    positions = jnp.where(step < ROWS // 8, device * ROWS + 8 * step, step - ROWS // 8)
     half = HEAD_DIM // 2
     inverse = rotary_base ** (-jnp.arange(half, dtype=f32) / half)
     angles = positions.astype(f32)[:, None] * jnp.tile(inverse, 2 * WIDTH // HEAD_DIM)[None, :]
-    sign = jnp.where((jnp.arange(WIDTH) & (HEAD_DIM - 1)) < half, -1.0, 1.0).astype(f32)
     q8, kv, pairs = project(
         jnp.stack([zh, mine]),
         tokens,
@@ -380,7 +383,7 @@
         w_value,
         chosen.T,
         jnp.cos(angles),
-        jnp.sin(angles) * sign[None, :],
+        jnp.sin(angles),
     )
     slots = [kv] + [None] * (RING - 1)
     up = down = kv

time: 100 us -> 100 us (level)
  no operation moved by 1% of the time
where the time goes in v8:
time: 100 us; the launch traced here: 99.4 us
  starting transfers between devices  57.2 us (57%)
  waiting for transfers between devices  29.1 us (29%)
  Pallas kernels  10.5 us (10%)
  other arithmetic  1 us (1%)
    ppermute x3, starting transfers between devices, local(): down = lax.ppermute(down, 'zh', down_pairs(s))  22.4 us
    ppermute x3, waiting for transfers between devices, local(): lax.ppermute(w_out, 'x', [(i, (i + k) % PER) for i in range(PER)])  21.4 us
    ppermute x3, starting transfers between devices, local(): lax.ppermute(w_out, 'x', [(i, (i + k) % PER) for i in range(PER)])  10.5 us
    ppermute x3, waiting for transfers between devices, local(): down = lax.ppermute(down, 'zh', down_pairs(s))  7.49 us
    all_to_all x1, starting transfers between devices, local(): parts = lax.all_to_all(parts, ('zl', 'y', 'x'), 0, 0, tiled=True)  7.07 us
    ppermute x4, starting transfers between devices, local(): up = lax.ppermute(up, 'zh', up_pairs(s))  6.9 us
    all_to_all x1, starting transfers between devices, local(): q_team = lax.all_to_all(q8, ('zl', 'y'), 0, 0, tiled=True)  6.37 us
    ppermute x1, starting transfers between devices, local(): received = lax.ppermute(send, 'c', [(0, 1), (1, 0)])  3.87 us
  transfers between devices with their start and end apart: 13, of which 5 were waited for; matrix products, arithmetic and copies ran while one was open for 1% of the time, Pallas kernels for 3%

profile of v8, /device:TPU:1, one launch (start us, length us, event | category | flops | bytes accessed | tf_op | source)
XLA Modules:
  0.0 99.4 jit_solution(10310866727765908475)
XLA Ops:
  0.7 0.1 mul.40
  0.8 0.2 multiply_sine_fusion
  0.9 0.1 pad_add_fusion.1.place_ref
  1.0 3.6 %project.1 = (bf16[8,256,128]{2,1,0:T(8,128)(2,1)}, bf16[512,128]{1,0:T(8,128)(2,1)S(1)}, s32[4,512]{1,0:T(4,128)S(1)}) custom-call(s32[2]{0:T(128)S(1)} %pad_add_fusion.1.place_ref, bf16[256,2048]{1,0:T(8,128)(2,1)} %refs_0_.2, bf16[2048,128]{1,0:T(8,128)(2,1)} %refs_1_.1, bf16[2048,128]{1,0:T(8,128)(2,1)} %refs_2_.1, bf16[2048,128]{1,0:T(8,128)(2,1)} %refs_3_.1, ...), custom_call_target="tpu_custom_call" | custom-call | tf_op jit(solution)/shard_map/project/pallas_call | solution.py:124
  4.6 6.4 %all-to-all-start = ((bf16[8,256,128]{2,1,0:T(8,128)(2,1)}), bf16[8,256,128]{2,1,0:T(8,128)(2,1)S(1)}, u32[]{:S(2)}, u32[]{:S(2)}) async-start(bf16[8,256,128]{2,1,0:T(8,128)(2,1)} %get-tuple-element.13), calls=%async_computation | async-start | bytes 1048576 | tf_op jit(solution)/shard_map/all_to_all | solution.py:396
  11.0 4.9 %collective-permute-start = (bf16[512,128]{1,0:T(8,128)(2,1)S(1)}, bf16[512,128]{1,0:T(8,128)(2,1)S(1)}, u32[]{:S(2)}, u32[]{:S(2)}) collective-permute-start(bf16[512,128]{1,0:T(8,128)(2,1)S(1)} %get-tuple-element.14.refs_0_), channel_id=1, source_target_pairs={{0,64},{64,128},{128,192},{192,256},{256,320},{320,384},{384,448},... | collective-permute-start | bytes 393224 | tf_op jit(solution)/shard_map/ppermute | solution.py:391
  15.9 7.1 %collective-permute-start.3 = (bf16[512,128]{1,0:T(8,128)(2,1)S(1)}, bf16[512,128]{1,0:T(8,128)(2,1)S(1)}, u32[]{:S(2)}, u32[]{:S(2)}) collective-permute-start(bf16[512,128]{1,0:T(8,128)(2,1)S(1)} %get-tuple-element.14.refs_0_), channel_id=1, source_target_pairs={{0,448},{64,0},{128,64},{1,449},{65,1},{129,65},{2,450},{66,2},{13... | collective-permute-start | bytes 393224 | tf_op jit(solution)/shard_map/ppermute | solution.py:394
  22.9 0.7 collective-permute-start.1
  23.6 3.0 %collective-permute-done.3.refs_5_ = bf16[512,128]{1,0:T(8,128)(2,1)S(1)} collective-permute-done((bf16[512,128]{1,0:T(8,128)(2,1)S(1)}, bf16[512,128]{1,0:T(8,128)(2,1)S(1)}, u32[]{:S(2)}, u32[]{:S(2)}) %collective-permute-start.3) | collective-permute-done | bytes 131104 | tf_op jit(solution)/shard_map/ppermute | solution.py:394
  26.7 9.0 %collective-permute-start.4 = (bf16[512,128]{1,0:T(8,128)(2,1)S(1)}, bf16[512,128]{1,0:T(8,128)(2,1)S(1)}, u32[]{:S(2)}, u32[]{:S(2)}) collective-permute-start(bf16[512,128]{1,0:T(8,128)(2,1)S(1)} %collective-permute-done.3.refs_5_), channel_id=1, source_target_pairs={{448,384},{0,448},{64,0},{449,385},{1,449},{65,1},{450,386},{2,450... | collective-permute-start | bytes 393224 | tf_op jit(solution)/shard_map/ppermute | solution.py:394
  35.7 0.0 collective-permute-done.1.refs_2_
  35.7 0.7 collective-permute-start.2
  36.4 4.5 %collective-permute-done.4.refs_4_ = bf16[512,128]{1,0:T(8,128)(2,1)S(1)} collective-permute-done((bf16[512,128]{1,0:T(8,128)(2,1)S(1)}, bf16[512,128]{1,0:T(8,128)(2,1)S(1)}, u32[]{:S(2)}, u32[]{:S(2)}) %collective-permute-start.4) | collective-permute-done | bytes 131104 | tf_op jit(solution)/shard_map/ppermute | solution.py:394
  40.8 6.4 %collective-permute-start.6 = (bf16[512,128]{1,0:T(8,128)(2,1)S(1)}, bf16[512,128]{1,0:T(8,128)(2,1)S(1)}, u32[]{:S(2)}, u32[]{:S(2)}) collective-permute-start(bf16[512,128]{1,0:T(8,128)(2,1)S(1)} %collective-permute-done.4.refs_4_), channel_id=1, source_target_pairs={{384,320},{448,384},{0,448},{385,321},{449,385},{1,449},{386,322},... | collective-permute-start | bytes 393224 | tf_op jit(solution)/shard_map/ppermute | solution.py:394
  47.2 0.7 collective-permute-start.5
  47.9 0.0 all-to-all-done.q_ref
  47.9 3.2 %near.1 = (bf16[33,128,128]{2,1,0:T(8,128)(2,1)S(1)}, f32[33,8,128]{2,1,0:T(8,128)S(1)}, f32[33,8,128]{2,1,0:T(8,128)S(1)}, f32[33,64,128]{2,1,0:T(8,128)S(1)}) custom-call(s32[4,512]{1,0:T(4,128)S(1)} %get-tuple-element.12.pairs_ref, bf16[8,256,128]{2,1,0:T(8,128)(2,1)S(1)} %all-to-all-done.q_ref, bf16[512,128]{1,0:T(8,128)(2,1)S(1)} %get-tuple-element.14.refs_0_, ...), custom_call_target="tpu_custom_call" | custom-call | tf_op jit(solution)/shard_map/near/pallas_call | solution.py:278
  51.1 1.9 %far.1 = bf16[32,80,128]{2,1,0:T(8,128)(2,1)} custom-call(s32[4,512]{1,0:T(4,128)S(1)} %get-tuple-element.12.pairs_ref, bf16[33,128,128]{2,1,0:T(8,128)(2,1)S(1)} %get-tuple-element.15.qq, f32[33,8,128]{2,1,0:T(8,128)S(1)} %get-tuple-element.16.m_ref, f32[33,8,128]{2,1,0:T(8,128)S(1)} %get-tuple-element.17.l_ref, ...), custom_call_target="tpu_custom_call" | custom-call | tf_op jit(solution)/shard_map/far/pallas_call | solution.py:292
  53.0 0.0 copy-start
  53.0 7.1 %all-to-all-start.1 = ((bf16[32,80,128]{2,1,0:T(8,128)(2,1)}), bf16[32,80,128]{2,1,0:T(8,128)(2,1)S(1)}, u32[]{:S(2)}, u32[]{:S(2)}) async-start(bf16[32,80,128]{2,1,0:T(8,128)(2,1)} %far.1), calls=%async_computation.1 | async-start | bytes 1310720 | tf_op jit(solution)/shard_map/all_to_all | solution.py:402
  60.1 3.1 %collective-permute-start.7 = (bf16[128,2048]{1,0:T(8,128)(2,1)S(1)}, bf16[128,2048]{1,0:T(8,128)(2,1)S(1)}, u32[]{:S(2)}, u32[]{:S(2)}) collective-permute-start(bf16[128,2048]{1,0:T(8,128)(2,1)S(1)} %copy-done), channel_id=1, source_target_pairs={{0,2},{2,4},{4,6},{6,0},{1,3},{3,5},{5,7},{7,1},{8,10},{10,12},{12... | collective-permute-start | bytes 1572872 | tf_op jit(solution)/shard_map/ppermute | solution.py:399
  63.2 4.3 %collective-permute-start.8 = (bf16[128,2048]{1,0:T(8,128)(2,1)S(1)}, bf16[128,2048]{1,0:T(8,128)(2,1)S(1)}, u32[]{:S(2)}, u32[]{:S(2)}) collective-permute-start(bf16[128,2048]{1,0:T(8,128)(2,1)S(1)} %copy-done), channel_id=1, source_target_pairs={{0,4},{2,6},{4,0},{6,2},{1,5},{3,7},{5,1},{7,3},{8,12},{10,14},{12... | collective-permute-start | bytes 1572872 | tf_op jit(solution)/shard_map/ppermute | solution.py:399
  67.5 3.1 %collective-permute-start.9 = (bf16[128,2048]{1,0:T(8,128)(2,1)S(1)}, bf16[128,2048]{1,0:T(8,128)(2,1)S(1)}, u32[]{:S(2)}, u32[]{:S(2)}) collective-permute-start(bf16[128,2048]{1,0:T(8,128)(2,1)S(1)} %copy-done), channel_id=1, source_target_pairs={{0,6},{2,0},{4,2},{6,4},{1,7},{3,1},{5,3},{7,5},{8,14},{10,8},{12,... | collective-permute-start | bytes 1572872 | tf_op jit(solution)/shard_map/ppermute | solution.py:399
  70.6 0.1 pad_add_fusion.place_ref
  70.7 11.1 %collective-permute-done.7.refs_1_ = bf16[128,2048]{1,0:T(8,128)(2,1)S(1)} collective-permute-done((bf16[128,2048]{1,0:T(8,128)(2,1)S(1)}, bf16[128,2048]{1,0:T(8,128)(2,1)S(1)}, u32[]{:S(2)}, u32[]{:S(2)}) %collective-permute-start.7) | collective-permute-done | bytes 524320 | tf_op jit(solution)/shard_map/ppermute | solution.py:399
  81.8 10.2 %collective-permute-done.8.refs_2_ = bf16[128,2048]{1,0:T(8,128)(2,1)S(1)} collective-permute-done((bf16[128,2048]{1,0:T(8,128)(2,1)S(1)}, bf16[128,2048]{1,0:T(8,128)(2,1)S(1)}, u32[]{:S(2)}, u32[]{:S(2)}) %collective-permute-start.8) | collective-permute-done | bytes 524320 | tf_op jit(solution)/shard_map/ppermute | solution.py:399
  92.1 1.8 %merge.1 = (f32[32,2048]{1,0:T(8,128)S(1)}, bf16[32,2048]{1,0:T(8,128)(2,1)S(1)}, f32[4,128]{1,0:T(4,128)S(1)}) custom-call(s32[2]{0:T(128)S(1)} %pad_add_fusion.place_ref, bf16[32,80,128]{2,1,0:T(8,128)(2,1)S(1)} %all-to-all-done.1.part_ref, bf16[128,2048]{1,0:T(8,128)(2,1)S(1)} %copy-done, bf16[128,2048]{1,0:T(8,128)(2,1)S(1)} %collective-permute-done.7.refs_1_, ...), custom_call_target="tpu_custom_call" | custom-call | tf_op jit(solution)/shard_map/merge/pallas_call | solution.py:345
  93.9 3.9 %collective-permute-start.10 = (bf16[32,2048]{1,0:T(8,128)(2,1)S(1)}, bf16[32,2048]{1,0:T(8,128)(2,1)S(1)}, u32[]{:S(2)}, u32[]{:S(2)}) collective-permute-start(bf16[32,2048]{1,0:T(8,128)(2,1)S(1)} %get-tuple-element.20), channel_id=1, source_target_pairs={{0,1},{1,0},{2,3},{3,2},{4,5},{5,4},{6,7},{7,6},{8,9},{9,8},{10,11... | collective-permute-start | bytes 393224 | tf_op jit(solution)/shard_map/ppermute | solution.py:405
  97.8 0.1 reshape.28
  97.9 0.7 reshape.29
  98.5 0.2 collective-permute-done.10
  98.7 0.7 add_convert_fusion
  (11 shorter events, 0.0 us)
Async XLA Ops:
  4.6 43.3 %all-to-all-start = ((bf16[8,256,128]{2,1,0:T(8,128)(2,1)}), bf16[8,256,128]{2,1,0:T(8,128)(2,1)S(1)}, u32[]{:S(2)}, u32[]{:S(2)}) async-start(bf16[8,256,128]{2,1,0:T(8,128)(2,1)} %get-tuple-element.13), calls=%async_computation | async-start | bytes 1048576 | tf_op jit(solution)/shard_map/all_to_all | solution.py:396
  11.0 12.0 %collective-permute-start = (bf16[512,128]{1,0:T(8,128)(2,1)S(1)}, bf16[512,128]{1,0:T(8,128)(2,1)S(1)}, u32[]{:S(2)}, u32[]{:S(2)}) collective-permute-start(bf16[512,128]{1,0:T(8,128)(2,1)S(1)} %get-tuple-element.14.refs_0_), channel_id=1, source_target_pairs={{0,64},{64,128},{128,192},{192,256},{256,320},{320,384},{384,448},... | collective-permute-start | bytes 393224 | tf_op jit(solution)/shard_map/ppermute | solution.py:391
  15.9 10.8 %collective-permute-start.3 = (bf16[512,128]{1,0:T(8,128)(2,1)S(1)}, bf16[512,128]{1,0:T(8,128)(2,1)S(1)}, u32[]{:S(2)}, u32[]{:S(2)}) collective-permute-start(bf16[512,128]{1,0:T(8,128)(2,1)S(1)} %get-tuple-element.14.refs_0_), channel_id=1, source_target_pairs={{0,448},{64,0},{128,64},{1,449},{65,1},{129,65},{2,450},{66,2},{13... | collective-permute-start | bytes 393224 | tf_op jit(solution)/shard_map/ppermute | solution.py:394
  22.9 12.7 %collective-permute-start.1 = (bf16[512,128]{1,0:T(8,128)(2,1)S(1)}, bf16[512,128]{1,0:T(8,128)(2,1)S(1)}, u32[]{:S(2)}, u32[]{:S(2)}) collective-permute-start(bf16[512,128]{1,0:T(8,128)(2,1)S(1)} %collective-permute-done.refs_1_), channel_id=1, source_target_pairs={{64,128},{128,192},{192,256},{256,320},{320,384},{384,448},{65,129... | collective-permute-start | bytes 393224 | tf_op jit(solution)/shard_map/ppermute | solution.py:391
  26.7 14.1 %collective-permute-start.4 = (bf16[512,128]{1,0:T(8,128)(2,1)S(1)}, bf16[512,128]{1,0:T(8,128)(2,1)S(1)}, u32[]{:S(2)}, u32[]{:S(2)}) collective-permute-start(bf16[512,128]{1,0:T(8,128)(2,1)S(1)} %collective-permute-done.3.refs_5_), channel_id=1, source_target_pairs={{448,384},{0,448},{64,0},{449,385},{1,449},{65,1},{450,386},{2,450... | collective-permute-start | bytes 393224 | tf_op jit(solution)/shard_map/ppermute | solution.py:394
  35.7 11.5 %collective-permute-start.2 = (bf16[512,128]{1,0:T(8,128)(2,1)S(1)}, bf16[512,128]{1,0:T(8,128)(2,1)S(1)}, u32[]{:S(2)}, u32[]{:S(2)}) collective-permute-start(bf16[512,128]{1,0:T(8,128)(2,1)S(1)} %collective-permute-done.1.refs_2_), channel_id=1, source_target_pairs={{128,192},{192,256},{256,320},{320,384},{384,448},{129,193},{193,2... | collective-permute-start | bytes 393224 | tf_op jit(solution)/shard_map/ppermute | solution.py:391
  40.8 10.3 %collective-permute-start.6 = (bf16[512,128]{1,0:T(8,128)(2,1)S(1)}, bf16[512,128]{1,0:T(8,128)(2,1)S(1)}, u32[]{:S(2)}, u32[]{:S(2)}) collective-permute-start(bf16[512,128]{1,0:T(8,128)(2,1)S(1)} %collective-permute-done.4.refs_4_), channel_id=1, source_target_pairs={{384,320},{448,384},{0,448},{385,321},{449,385},{1,449},{386,322},... | collective-permute-start | bytes 393224 | tf_op jit(solution)/shard_map/ppermute | solution.py:394
  47.2 3.9 %collective-permute-start.5 = (bf16[512,128]{1,0:T(8,128)(2,1)S(1)}, bf16[512,128]{1,0:T(8,128)(2,1)S(1)}, u32[]{:S(2)}, u32[]{:S(2)}) collective-permute-start(bf16[512,128]{1,0:T(8,128)(2,1)S(1)} %collective-permute-done.2.refs_3_), channel_id=1, source_target_pairs={{192,256},{256,320},{320,384},{384,448},{193,257},{257,321},{321,3... | collective-permute-start | bytes 393224 | tf_op jit(solution)/shard_map/ppermute | solution.py:391
  53.0 7.1 %copy-start = (bf16[128,2048]{1,0:T(8,128)(2,1)S(1)}, bf16[128,2048]{1,0:T(8,128)(2,1)}, u32[]{:S(2)}) copy-start(bf16[128,2048]{1,0:T(8,128)(2,1)} %refs_0_.3) | copy-start | bytes 1572868
  53.0 39.1 %all-to-all-start.1 = ((bf16[32,80,128]{2,1,0:T(8,128)(2,1)}), bf16[32,80,128]{2,1,0:T(8,128)(2,1)S(1)}, u32[]{:S(2)}, u32[]{:S(2)}) async-start(bf16[32,80,128]{2,1,0:T(8,128)(2,1)} %far.1), calls=%async_computation.1 | async-start | bytes 1310720 | tf_op jit(solution)/shard_map/all_to_all | solution.py:402
  60.1 21.8 %collective-permute-start.7 = (bf16[128,2048]{1,0:T(8,128)(2,1)S(1)}, bf16[128,2048]{1,0:T(8,128)(2,1)S(1)}, u32[]{:S(2)}, u32[]{:S(2)}) collective-permute-start(bf16[128,2048]{1,0:T(8,128)(2,1)S(1)} %copy-done), channel_id=1, source_target_pairs={{0,2},{2,4},{4,6},{6,0},{1,3},{3,5},{5,7},{7,1},{8,10},{10,12},{12... | collective-permute-start | bytes 1572872 | tf_op jit(solution)/shard_map/ppermute | solution.py:399
  63.2 28.8 %collective-permute-start.8 = (bf16[128,2048]{1,0:T(8,128)(2,1)S(1)}, bf16[128,2048]{1,0:T(8,128)(2,1)S(1)}, u32[]{:S(2)}, u32[]{:S(2)}) collective-permute-start(bf16[128,2048]{1,0:T(8,128)(2,1)S(1)} %copy-done), channel_id=1, source_target_pairs={{0,4},{2,6},{4,0},{6,2},{1,5},{3,7},{5,1},{7,3},{8,12},{10,14},{12... | collective-permute-start | bytes 1572872 | tf_op jit(solution)/shard_map/ppermute | solution.py:399
  67.5 24.5 %collective-permute-start.9 = (bf16[128,2048]{1,0:T(8,128)(2,1)S(1)}, bf16[128,2048]{1,0:T(8,128)(2,1)S(1)}, u32[]{:S(2)}, u32[]{:S(2)}) collective-permute-start(bf16[128,2048]{1,0:T(8,128)(2,1)S(1)} %copy-done), channel_id=1, source_target_pairs={{0,6},{2,0},{4,2},{6,4},{1,7},{3,1},{5,3},{7,5},{8,14},{10,8},{12,... | collective-permute-start | bytes 1572872 | tf_op jit(solution)/shard_map/ppermute | solution.py:399
  93.9 4.8 %collective-permute-start.10 = (bf16[32,2048]{1,0:T(8,128)(2,1)S(1)}, bf16[32,2048]{1,0:T(8,128)(2,1)S(1)}, u32[]{:S(2)}, u32[]{:S(2)}) collective-permute-start(bf16[32,2048]{1,0:T(8,128)(2,1)S(1)} %get-tuple-element.20), channel_id=1, source_target_pairs={{0,1},{1,0},{2,3},{3,2},{4,5},{5,4},{6,7},{7,6},{8,9},{9,8},{10,11... | collective-permute-start | bytes 393224 | tf_op jit(solution)/shard_map/ppermute | solution.py:405
